TPU v7x, 512 devices: a whole 4x4x16 slice. The times are simulated.
512 devices in a mesh: rep: 2 (over z_hi), fs: 32 (over z_lo, y), tp: 8 (over x, core).
Axes of the slice: x: 4, y: 4, z: 16 (z_hi: 2, z_lo: 8; z = z_hi * 8 + z_lo), core: 2. Of those that a mesh axis runs over, the one named last changes fastest.
Arguments:
- tokens: bfloat16 [16384, 2048], P(('rep', 'fs')), may hold values from -6 to 6
- first_gain: float32 [2048], replicated, may hold values from 0.1 to 1.9
- value_weight: float32 [2048, 1024], P('fs', 'tp'), may hold values from -0.125 to 0.125
- gate_weight: float32 [2048, 1024], P('fs', 'tp'), may hold values from -0.125 to 0.125
- value_scale: float32 [1024], P('tp'), may hold values from 0.5 to 2
- gate_scale: float32 [1024], P('tp'), may hold values from 0.5 to 2
- conv_taps: float32 [31, 1024], P(None, 'tp'), may hold values from -7 to 7
- chan_gain: float32 [1024], P('tp'), may hold values from 0.1 to 1.9
- mixout_weight: float32 [1024, 2048], P('tp', 'fs'), may hold values from -0.1875 to 0.1875
- mixout_scale: float32 [2048], P('fs'), may hold values from 0.5 to 2
- second_gain: float32 [2048], replicated, may hold values from 0.1 to 1.9
- up_weight: float32 [2048, 8192], P('fs', 'tp'), may hold values from -0.125 to 0.125
- up_scale: float32 [8192], P('tp'), may hold values from 0.5 to 2
- down_weight: float32 [8192, 2048], P('tp', 'fs'), may hold values from -0.0625 to 0.0625
- down_scale: float32 [2048], P('fs'), may hold values from 0.5 to 2
Outputs:
- layer_out: bfloat16 [16384, 2048], P(('rep', 'fs'))
All inputs are finite; a program needn't handle non-finite values.
Results may differ from a plain program's by a relative error of at most 0.025.
Values may be sent and summed in bfloat16 or wider, within the bound.
No kernel may reach another device: no remote copies, remote signals or barrier semaphores. Data moves between devices by JAX's collectives and lax.ppermute only.
A program may use at most 128 MiB of HBM per device.

v0:
```python
import jax
import jax.numpy as jnp
from jax import lax
from jax.sharding import Mesh
from jax.sharding import PartitionSpec as P

SEQ_LEN = 128
FS = ("fs_0", "fs_1")
REP_FS = ("rep", "fs_0", "fs_1")


def laid_out(blocks, dim):
    blocks = jnp.moveaxis(blocks, 0, dim)
    lengths = blocks.shape
    return blocks.reshape(*lengths[:dim], lengths[dim] * lengths[dim + 1], *lengths[dim + 2 :])


def stacked_from(x, axes, order):
    blocks = x
    for k in order:
        blocks = lax.all_gather(blocks, axes[k])
    done = order[::-1]
    back = [done.index(k) for k in range(len(axes))]
    blocks = blocks.transpose(*back, *range(len(axes), blocks.ndim))
    return blocks.reshape(-1, *x.shape)


def gathered_by_axis(x, axes, order, dim):
    return laid_out(stacked_from(x, axes, order), dim)


def side_by_side(arrays, axis, dim, along):
    ends, at = ([], 0)
    for a in arrays[:-1]:
        at += a.shape[along]
        ends.append(at)
    both = jnp.concatenate(arrays, axis=along)
    return tuple(jnp.split(lax.all_gather(both, axis, axis=dim, tiled=True), ends, axis=along))


def turned_gather(arrays, axis, dims):
    turned = [jnp.moveaxis(a, dim, 0) for a, dim in zip(arrays, dims)]
    both = jnp.concatenate([t.reshape(len(t), -1) for t in turned], axis=1)
    whole, at, gathered = (lax.all_gather(both, axis, axis=0, tiled=True), 0, [])
    for t, dim in zip(turned, dims):
        piece = whole[:, at : at + t[0].size].reshape(-1, *t.shape[1:])
        gathered.append(jnp.moveaxis(piece, 0, dim))
        at += t[0].size
    return tuple(gathered)


def copy_for_each(x, axis):
    copies = jnp.broadcast_to(x, (lax.axis_size(axis), *x.shape))
    return lax.all_to_all(copies, axis, split_axis=0, concat_axis=0, tiled=True)


def over_copies(x, axis):
    return copy_for_each(x, axis).astype(jnp.float32).sum(axis=0)


def rms_rows(rows, gain):
    values = rows.astype(jnp.float32)
    scaled = values * lax.rsqrt(jnp.mean(values * values, axis=-1, keepdims=True) + 1e-05)
    return (scaled * gain).astype(jnp.bfloat16)


def causal_conv(signal, taps):
    width = signal.shape[1]
    seqs = signal.reshape(-1, SEQ_LEN, width)
    result = lax.conv_general_dilated(
        seqs,
        taps[:, None, :],
        (1,),
        [(taps.shape[0] - 1, 0)],
        dimension_numbers=("NWC", "WIO", "NWC"),
        feature_group_count=width,
        precision=lax.Precision.HIGHEST,
    )
    return result.reshape(signal.shape)


def on_device(
    tokens,
    first_gain,
    value_weight,
    gate_weight,
    value_scale,
    gate_scale,
    conv_taps,
    chan_gain,
    mixout_weight,
    mixout_scale,
    second_gain,
    up_weight,
    up_scale,
    down_weight,
    down_scale,
):
    up_whole = gathered_by_axis(up_weight.astype(jnp.bfloat16), FS, (0, 1), 0)
    normed = rms_rows(tokens, first_gain)
    width = value_weight.shape[1]
    pieces = side_by_side(
        (value_weight.astype(jnp.bfloat16), gate_weight.astype(jnp.bfloat16)), FS, 0, 1
    )
    value_sum = jnp.dot(normed, pieces[0], preferred_element_type=jnp.float32)
    gate_sum = jnp.dot(normed, pieces[1], preferred_element_type=jnp.float32)
    value_mult = value_scale.astype(jnp.bfloat16).astype(jnp.float32)
    gate_mult = gate_scale.astype(jnp.bfloat16).astype(jnp.float32)
    glu = value_sum * value_mult * jax.nn.sigmoid(gate_sum * gate_mult)
    conv = causal_conv(glu, conv_taps)
    total = width * lax.axis_size("tp")
    mean = lax.psum(jnp.sum(conv, axis=1), "tp") / total
    centred_local = conv - mean[:, None]
    var = lax.psum(jnp.sum(centred_local * centred_local, axis=1), "tp") / total
    centred = conv - mean[:, None]
    mixed_in = jax.nn.silu(centred * lax.rsqrt(var[:, None] + 1e-05) * chan_gain).astype(
        jnp.bfloat16
    )
    out_whole, out_mult = turned_gather(
        (mixout_weight.astype(jnp.bfloat16), mixout_scale.astype(jnp.bfloat16)), FS, (1, 0)
    )
    out_factor = out_mult.astype(jnp.float32)
    mix_term = jnp.dot(mixed_in, out_whole, preferred_element_type=jnp.float32) * out_factor
    mix_sum = over_copies(mix_term.astype(jnp.bfloat16), "tp").astype(jnp.float32)
    middle = (tokens.astype(jnp.float32) + mix_sum).astype(jnp.bfloat16)
    normed2 = rms_rows(middle, second_gain)
    up_sum = jnp.dot(normed2, up_whole, preferred_element_type=jnp.float32)
    up_mult = up_scale.astype(jnp.bfloat16).astype(jnp.float32)
    hidden = jnp.square(jax.nn.relu(up_sum * up_mult)).astype(jnp.bfloat16)
    down_whole, down_mult = turned_gather(
        (down_weight.astype(jnp.bfloat16), down_scale.astype(jnp.bfloat16)), FS, (1, 0)
    )
    down_factor = down_mult.astype(jnp.float32)
    down_term = jnp.dot(hidden, down_whole, preferred_element_type=jnp.float32) * down_factor
    down_sum = over_copies(down_term.astype(jnp.bfloat16), "tp").astype(jnp.float32)
    return (middle.astype(jnp.float32) + down_sum).astype(jnp.bfloat16)


def solution(mesh):
    torus = Mesh(
        mesh.devices.reshape(mesh.shape["rep"], 8, 4, mesh.shape["tp"]),
        ("rep", "fs_0", "fs_1", "tp"),
    )
    placed = (
        P(REP_FS, None),
        P(),
        P(FS, "tp"),
        P(FS, "tp"),
        P("tp"),
        P("tp"),
        P(None, "tp"),
        P("tp"),
        P("tp", FS),
        P(FS),
        P(),
        P(FS, "tp"),
        P("tp"),
        P("tp", FS),
        P(FS),
    )
    return jax.shard_map(
        on_device, mesh=torus, in_specs=placed, out_specs=P(REP_FS, None), check_vma=False
    )
```

profile of v0, /device:TPU:1, one launch (start us, length us, event | category | flops | bytes accessed | tf_op | source)
XLA Modules:
  0.0 708.7 jit_solution(6526058363183108744)
XLA Ops:
  6.6 1.7 convert_element_type.115
  8.4 0.8 convert_element_type.100
  9.1 0.8 convert_element_type.99
  10.6 64.9 %all-gather.11.cloned.1.call-done = bf16[512,1024]{1,0:T(8,128)(2,1)} async-done(((bf16[64,1024]{1,0:T(8,128)(2,1)}), bf16[512,1024]{1,0:T(8,128)(2,1)}) %all-gather.11.cloned.1.call-update) | async-done | bytes 1048592 | tf_op jit(solution)/shard_map/all_gather | solution.py:21
  75.5 0.7 convert_bitcast_fusion.2
  76.3 1.0 convert_bitcast_fusion
  77.3 0.7 pad_maximum_fusion
  78.5 110.2 %all_gather.22 = bf16[2048,129]{1,0:T(8,128)(2,1)S(1)} all-gather(bf16[64,129]{1,0:T(8,128)(2,1)S(1)} %pad_maximum_fusion.2), channel_id=1, replica_groups=mesh['rep'=2,'fs_0'=8,'fs_1'=4,'tp'=8] {'fs_0','fs_1'}, dimensions={0}, use_global_device_ids=true | all-gather | bytes 544896 | tf_op jit(solution)/shard_map/all_gather | solution.py:44
  188.9 88.8 %all-gather.7.cloned.1.call-done = bf16[2048,256]{1,0:T(8,128)(2,1)} async-done(((bf16[64,256]{1,0:T(8,128)(2,1)}), bf16[2048,256]{1,0:T(8,128)(2,1)}) %all-gather.7.cloned.1.call-update) | async-done | bytes 1048592 | tf_op jit(solution)/shard_map/all_gather | solution.py:38
  277.7 1.6 convolution_multiply_fusion.3
  280.4 35.0 %psum.14 = f32[256]{0:T(256)S(1)} all-reduce(f32[256]{0:T(256)S(1)} %bitcast.33), channel_id=1, replica_groups=mesh['rep'=2,'fs_0'=8,'fs_1'=4,'tp'=8] {'tp'}, use_global_device_ids=true, to_apply=%region_2.0 | all-reduce | flops 256 | bytes 2048 | tf_op jit(solution)/shard_map/psum | solution.py:112
  316.0 12.8 %psum.15 = f32[256]{0:T(256)S(1)} all-reduce(f32[256]{0:T(256)S(1)} %bitcast.34), channel_id=1, replica_groups=mesh['rep'=2,'fs_0'=8,'fs_1'=4,'tp'=8] {'tp'}, use_global_device_ids=true, to_apply=%region_4.0 | all-reduce | flops 256 | bytes 2048 | tf_op jit(solution)/shard_map/psum | solution.py:114
  329.5 4.3 broadcast_in_dim.7
  333.8 5.6 all-to-all-start
  339.4 16.5 %all-gather.13.cloned.1.call-done = bf16[32,64,1024]{2,1,0:T(8,128)(2,1)} async-done(((bf16[8,64,1024]{2,1,0:T(8,128)(2,1)}), bf16[32,64,1024]{2,1,0:T(8,128)(2,1)}) %all-gather.13.cloned.1.call-update) | async-done | bytes 4194320 | tf_op jit(solution)/shard_map/all_gather | solution.py:21
  355.9 4.9 copy.57
  360.8 204.9 %all-gather.9.cloned.1.call-done = bf16[2048,1025]{1,0:T(8,128)(2,1)} async-done(((bf16[64,1025]{1,0:T(8,128)(2,1)}), bf16[2048,1025]{1,0:T(8,128)(2,1)}) %all-gather.9.cloned.1.call-update) | async-done | bytes 4198416 | tf_op jit(solution)/shard_map/all_gather | solution.py:44
  565.8 1.3 convert_reduce_fusion.2
  567.0 5.4 convert_reduce_fusion.1
  573.1 5.9 fusion.5
  579.0 1.1 broadcast_in_dim.8
  580.2 118.9 %all_to_all.10 = bf16[8,256,2048]{2,1,0:T(8,128)(2,1)S(1)} all-to-all(bf16[8,256,2048]{2,1,0:T(8,128)(2,1)S(1)} %broadcast_in_dim.8), channel_id=1, replica_groups=mesh['rep'=2,'fs_0'=8,'fs_1'=4,'tp'=8] {'tp'}, dimensions={0} | all-to-all | bytes 16777216 | tf_op jit(solution)/shard_map/all_to_all | solution.py:54
  699.1 1.8 convert_reduce_fusion
  700.9 1.3 fusion.16
  (56 shorter events, 4.6 us)
Async XLA Ops:
  6.5 273.3 %copy-start = (f32[31,128]{1,0:T(8,128)S(1)}, f32[31,128]{1,0:T(8,128)}, u32[]{:S(2)}) copy-start(f32[31,128]{1,0:T(8,128)} %param.21) | copy-start | bytes 47620
  6.5 71.4 %copy-start.1 = (bf16[256,2048]{1,0:T(8,128)(2,1)S(1)}, bf16[256,2048]{1,0:T(8,128)(2,1)}, u32[]{:S(2)}) copy-start(bf16[256,2048]{1,0:T(8,128)(2,1)} %param.15) | copy-start | bytes 3145732
  6.5 71.7 %copy-start.8 = (f32[128]{0:T(128)S(1)}, f32[128]{0:T(128)}, u32[]{:S(2)}) copy-start(f32[128]{0:T(128)} %param.19) | copy-start | bytes 1540
  6.5 71.8 %copy-start.9 = (f32[128]{0:T(128)S(1)}, f32[128]{0:T(128)}, u32[]{:S(2)}) copy-start(f32[128]{0:T(128)} %param.20) | copy-start | bytes 1540
  6.5 71.8 %copy-start.10 = (f32[64]{0:T(128)S(1)}, f32[64]{0:T(128)}, u32[]{:S(2)}) copy-start(f32[64]{0:T(128)} %param.24) | copy-start | bytes 772
  6.5 71.9 %copy-start.2 = (f32[128,64]{0,1:T(8,128)S(1)}, f32[128,64]{0,1:T(8,128)}, u32[]{:S(2)}) copy-start(f32[128,64]{0,1:T(8,128)} %param.23) | copy-start | bytes 98308
  6.6 68.9 %all-gather.11.cloned.1.call-start = ((), (), s32[]{:S(2)}) async-start(), calls=%async_computation.4 | async-start | bytes 1179648 | tf_op jit(solution)/shard_map/all_gather | solution.py:21
  8.3 269.3 %all-gather.7.cloned.1.call-start = ((), (), s32[]{:S(2)}) async-start(), calls=%async_computation.2 | async-start | bytes 1081344 | tf_op jit(solution)/shard_map/all_gather | solution.py:38
  10.5 345.4 %all-gather.13.cloned.1.call-start = ((), (), s32[]{:S(2)}) async-start(), calls=%async_computation.5 | async-start | bytes 5242880 | tf_op jit(solution)/shard_map/all_gather | solution.py:21
  75.4 202.2 %copy-start.6 = (f32[2048]{0:T(1024)S(1)}, f32[2048]{0:T(1024)}, u32[]{:S(2)}) copy-start(f32[2048]{0:T(1024)} %param.16) | copy-start | bytes 24580
  75.5 490.3 %all-gather.9.cloned.1.call-start = ((), (), s32[]{:S(2)}) async-start(), calls=%async_computation.3 | async-start | bytes 4866048 | tf_op jit(solution)/shard_map/all_gather | solution.py:44
  277.7 1.6 copy-start.5
  279.8 49.0 %copy-start.4 = (f32[128]{0:T(128)S(1)}, f32[128]{0:T(128)}, u32[]{:S(2)}) copy-start(f32[128]{0:T(128)} %param.22) | copy-start | bytes 1540
  333.8 5.6 copy-start.3
  333.8 233.3 %all-to-all-start = ((bf16[8,256,2048]{2,1,0:T(8,128)(2,1)}), bf16[8,256,2048]{2,1,0:T(8,128)(2,1)}, u32[]{:S(2)}, u32[]{:S(2)}) async-start(bf16[8,256,2048]{2,1,0:T(8,128)(2,1)} %broadcast_in_dim.7), calls=%async_computation | async-start | bytes 16777216 | tf_op jit(solution)/shard_map/all_to_all | solution.py:54
  572.4 0.7 copy-start.7
Sparse Core Ops, SparseCore 0:
  9.4 65.9 all-gather.10
  77.5 200.0 all-gather.6
  279.8 76.1 all-gather.12
  357.9 207.8 all-gather.8
where the time goes:
time: 709 us
  waiting for transfers between devices  375 us (53%)
  blocking collectives  277 us (39%)
  other arithmetic  17.3 us (2%)
  between operations  13.3 us (2%)
  local copies, waits for them, and re-layouts  11.1 us (2%)
  matrix products  8.98 us (1%)
    all_gather x1, waiting for transfers between devices, turned_gather(): lax.all_gather(both, axis, axis=0, tiled=True)  205 us
    all_to_all x1, blocking collectives, copy_for_each(): return lax.all_to_all(copies, axis, split_axis=0, concat_axis=0, tiled=True)  119 us
    all_gather x1, blocking collectives, turned_gather(): lax.all_gather(both, axis, axis=0, tiled=True)  110 us
    all_gather x1, waiting for transfers between devices, side_by_side(): lax.all_gather(both, axis, axis=dim, tiled=True)  88.8 us
    all_gather x2, waiting for transfers between devices, stacked_from(): blocks = lax.all_gather(blocks, axes[k])  81.4 us
    psum x1, blocking collectives, on_device(): mean = lax.psum(jnp.sum(conv, axis=1), 'tp') / total  35 us
  transfers between devices with their start and end apart: 5, of which 4 were waited for; matrix products, arithmetic and copies ran while one was open for 3% of the time, Pallas kernels for 0%

commit v1 on v0

v1 whole, which is shorter than its diff:
```python
import jax
import jax.numpy as jnp
from jax import lax
from jax.sharding import Mesh
from jax.sharding import PartitionSpec as P

SEQ_LEN = 128
FS = ("z", "y")
REP_FS = ("rep", "z", "y")
TP = ("x", "core")
RING = ("rep", "z")
F32 = jnp.float32
BF16 = jnp.bfloat16


def rounded(scale):
    return scale.astype(BF16).astype(F32)


def exchange(x, axis):
    return lax.all_to_all(x, axis, split_axis=0, concat_axis=0, tiled=True)


def copies_from(x, axis):
    return exchange(jnp.broadcast_to(x, (lax.axis_size(axis), *x.shape)), axis)


def shifted(x, distance):
    n = lax.axis_size(RING)
    return lax.ppermute(x, RING, [((i + distance) % n, i) for i in range(n)])


def ring_window(block):
    n = lax.axis_size("z")
    at = lax.axis_index("z")
    whole = jnp.zeros((n, *block.shape), block.dtype)
    whole = lax.dynamic_update_index_in_dim(whole, block, at, 0)
    for d in (4, -3, 3, -2, 2, -1, 1):
        whole = lax.dynamic_update_index_in_dim(whole, shifted(block, d), (at + d) % n, 0)
    return whole


def summed(x, axis):
    n = lax.axis_size(axis)
    blocks = exchange(x.reshape(n, x.shape[0] // n, x.shape[1]), axis)
    return blocks.astype(F32).sum(axis=0)


def tp_scattered(x):
    part = summed(x.astype(BF16), "core").astype(BF16)
    return summed(part, "x")


def tp_gathered(rows):
    part = copies_from(rows, "x")
    part = part.reshape(-1, rows.shape[1])
    return copies_from(part, "core").reshape(-1, rows.shape[1])


def own_rows(x):
    n = x.shape[0] // lax.axis_size(TP)
    block = lax.axis_index("core") * lax.axis_size("x") + lax.axis_index("x")
    return lax.dynamic_slice_in_dim(x, block * n, n, 0)


def rms_rows(rows, gain):
    values = rows.astype(F32)
    scaled = values * lax.rsqrt(jnp.mean(values * values, axis=-1, keepdims=True) + 1e-05)
    return (scaled * gain).astype(BF16)


def causal_conv(signal, taps):
    width = signal.shape[1]
    seqs = signal.reshape(-1, SEQ_LEN, width)
    result = lax.conv_general_dilated(
        seqs,
        taps[:, None, :],
        (1,),
        [(taps.shape[0] - 1, 0)],
        dimension_numbers=("NWC", "WIO", "NWC"),
        feature_group_count=width,
        precision=lax.Precision.HIGHEST,
    )
    return result.reshape(signal.shape)


def channel_stats(conv):
    width = conv.shape[1]
    total = jnp.sum(conv, axis=1)
    centred = conv - (total / width)[:, None]
    spread = jnp.sum(centred * centred, axis=1)
    both = lax.all_gather(jnp.stack([total, spread]), TP)
    n = both.shape[0]
    mean = both[:, 0].sum(axis=0) / (n * width)
    off = both[:, 0] / width - mean
    var = (both[:, 1].sum(axis=0) + width * (off * off).sum(axis=0)) / (n * width)
    return mean, var


def dot_t(a, b):
    return lax.dot_general(a, b, (((1,), (1,)), ((), ())), preferred_element_type=F32)


def on_device(
    tokens,
    first_gain,
    value_weight,
    gate_weight,
    value_scale,
    gate_scale,
    conv_taps,
    chan_gain,
    mixout_weight,
    mixout_scale,
    second_gain,
    up_weight,
    up_scale,
    down_weight,
    down_scale,
):
    rep = lax.axis_index("rep")
    reps = lax.axis_size("rep")
    width = value_weight.shape[1]
    mix_t = (mixout_weight.astype(BF16).astype(F32) * rounded(mixout_scale)).astype(BF16).T
    down_t = (down_weight.astype(BF16).astype(F32) * rounded(down_scale)).astype(BF16).T
    half = up_weight.shape[1] // reps
    up_half = lax.dynamic_slice_in_dim(up_weight, rep * half, half, 1).astype(BF16)
    down_half = lax.dynamic_slice_in_dim(down_t, rep * half, half, 1)
    ffn = lax.all_gather(jnp.concatenate([up_half, down_half], axis=1), REP_FS, axis=0, tiled=True)

    glu_local = jnp.concatenate([value_weight.astype(BF16), gate_weight.astype(BF16)], axis=1)
    glu_whole = ring_window(copies_from(glu_local, "y")).reshape(-1, 2 * width)
    mix_whole = ring_window(copies_from(mix_t, "y")).reshape(-1, width)

    normed = rms_rows(tokens, first_gain)
    sums = jnp.dot(normed, glu_whole, preferred_element_type=F32)
    glu = sums[:, :width] * rounded(value_scale) * jax.nn.sigmoid(sums[:, width:] * rounded(gate_scale))
    conv = causal_conv(glu, conv_taps)
    mean, var = channel_stats(conv)
    mixed_in = jax.nn.silu((conv - mean[:, None]) * lax.rsqrt(var[:, None] + 1e-05) * chan_gain).astype(BF16)
    mix_sum = tp_scattered(dot_t(mixed_in, mix_whole))
    middle = (own_rows(tokens).astype(F32) + mix_sum).astype(BF16)
    normed2 = tp_gathered(rms_rows(middle, second_gain))

    rows = ffn.shape[0] // reps
    up_mult = rounded(up_scale)
    down_sum = 0.0
    for r in range(reps):
        part = ffn[r * rows : (r + 1) * rows]
        up_sum = jnp.dot(normed2, part[:, :half], preferred_element_type=F32)
        hidden = jnp.square(jax.nn.relu(up_sum * up_mult[r * half : (r + 1) * half])).astype(BF16)
        down_sum = down_sum + dot_t(hidden, part[:, half:])
    layer_out = (middle.astype(F32) + tp_scattered(down_sum)).astype(BF16)
    return tp_gathered(layer_out)


def solution(mesh):
    torus = Mesh(
        mesh.devices.reshape(mesh.shape["rep"], 8, 4, 4, 2),
        ("rep", "z", "y", "x", "core"),
    )
    placed = (
        P(REP_FS, None),
        P(),
        P(FS, TP),
        P(FS, TP),
        P(TP),
        P(TP),
        P(None, TP),
        P(TP),
        P(TP, FS),
        P(FS),
        P(),
        P(FS, TP),
        P(TP),
        P(TP, FS),
        P(FS),
    )
    return jax.shard_map(
        on_device, mesh=torus, in_specs=placed, out_specs=P(REP_FS, None), check_vma=False
    )
```

time: 709 us -> 240 us (0.34)
  waiting for transfers between devices: 375 us -> 47.7 us
  blocking collectives: 277 us -> 69 us
  starting transfers between devices: 5.77 us -> 81.2 us
  other arithmetic: 17.3 us -> 10.1 us
    all_gather x4 -> x1, waiting for transfers between devices: 375 us -> 0.01 us  [on_device(): lax.all_gather(jnp.concatenate([up_half, down_half], axis=1), REP_FS, axi...]
    all_gather x1, blocking collectives: 110 us -> 24.8 us  [channel_stats(): both = lax.all_gather(jnp.stack([total, spread]), TP)]
    all_to_all x1 -> x6, blocking collectives: 119 us -> 44.2 us  [exchange(): return lax.all_to_all(x, axis, split_axis=0, concat_axis=0, tiled=True)]
    ppermute x0 -> x14, starting transfers between devices: none -> 65.6 us  [shifted(): return lax.ppermute(x, RING, [((i + distance) % n, i) for i in range(n)])]
    psum x2 -> x0, blocking collectives: 47.9 us -> none  [the longest x1 35 us: on_device(): mean = lax.psum(jnp.sum(conv, axis=1), 'tp') / total]
    ppermute x0 -> x14, waiting for transfers between devices: none -> 29.8 us  [shifted(): return lax.ppermute(x, RING, [((i + distance) % n, i) for i in range(n)])]
    all_to_all x1 -> x4, waiting for transfers between devices: 0.01 us -> 17.9 us  [exchange(): return lax.all_to_all(x, axis, split_axis=0, concat_axis=0, tiled=True)]
    all_to_all x1 -> x4, starting transfers between devices: 5.61 us -> 15.6 us  [exchange(): return lax.all_to_all(x, axis, split_axis=0, concat_axis=0, tiled=True)]
  transfers between devices with their start and end apart: 5 -> 19, of which waited for: 4 -> 9; matrix products, arithmetic and copies ran while one was open for 3% -> 5% of each run, Pallas kernels for 0% -> 0%
where the time goes in v1:
time: 240 us; the launch traced here: 237 us
  starting transfers between devices  81.2 us (34%)
  blocking collectives  69 us (29%)
  waiting for transfers between devices  47.7 us (20%)
  between operations  13.9 us (6%)
  matrix products  10.6 us (4%)
  other arithmetic  10.1 us (4%)
  local copies, waits for them, and re-layouts  4.38 us (2%)
    ppermute x14, starting transfers between devices, shifted(): return lax.ppermute(x, RING, [((i + distance) % n, i) for i in range(n)])  65.6 us
    all_to_all x6, blocking collectives, exchange(): return lax.all_to_all(x, axis, split_axis=0, concat_axis=0, tiled=True)  44.2 us
    ppermute x14, waiting for transfers between devices, shifted(): return lax.ppermute(x, RING, [((i + distance) % n, i) for i in range(n)])  29.8 us
    all_gather x1, blocking collectives, channel_stats(): both = lax.all_gather(jnp.stack([total, spread]), TP)  24.8 us
    all_to_all x4, waiting for transfers between devices, exchange(): return lax.all_to_all(x, axis, split_axis=0, concat_axis=0, tiled=True)  17.9 us
    all_to_all x4, starting transfers between devices, exchange(): return lax.all_to_all(x, axis, split_axis=0, concat_axis=0, tiled=True)  15.6 us
    dot_general x3, matrix products, dot_t(): lax.dot_general(a, b, (((1,), (1,)), ((), ())), preferred_element_type=F32)  9.55 us
  transfers between devices with their start and end apart: 19, of which 9 were waited for; matrix products, arithmetic and copies ran while one was open for 5% of the time, Pallas kernels for 0%

profile of v1, /device:TPU:1, one launch (start us, length us, event | category | flops | bytes accessed | tf_op | source)
XLA Modules:
  0.0 236.8 jit_solution(3951435594730297037)
XLA Ops:
  11.3 5.0 %all-to-all-start.1 = ((bf16[4,64,128]{2,1,0:T(8,128)(2,1)}), bf16[4,64,128]{2,1,0:T(8,128)(2,1)S(1)}, u32[]{:S(2)}, u32[]{:S(2)}) async-start(bf16[4,64,128]{2,1,0:T(8,128)(2,1)} %broadcast_in_dim.104), calls=%async_computation.1 | async-start | bytes 131072 | tf_op jit(solution)/shard_map/all_to_all | solution.py:21
  25.0 11.1 %collective-permute-start.13 = (bf16[4,64,128]{2,1,0:T(8,128)(2,1)S(1)}, bf16[4,64,128]{2,1,0:T(8,128)(2,1)S(1)}, u32[]{:S(2)}, u32[]{:S(2)}) collective-permute-start(bf16[4,64,128]{2,1,0:T(8,128)(2,1)S(1)} %all-to-all-done.1), channel_id=1, source_target_pairs={{32,0},{64,32},{96,64},{128,96},{160,128},{192,160},{224,192},{256... | collective-permute-start | bytes 196616 | tf_op jit(solution)/shard_map/ppermute | solution.py:30
  44.2 5.2 %collective-permute-start.7 = (bf16[4,64,128]{2,1,0:T(8,128)(2,1)S(1)}, bf16[4,64,128]{2,1,0:T(8,128)(2,1)S(1)}, u32[]{:S(2)}, u32[]{:S(2)}) collective-permute-start(bf16[4,64,128]{2,1,0:T(8,128)(2,1)S(1)} %all-to-all-done.1), channel_id=1, source_target_pairs={{128,0},{160,32},{192,64},{224,96},{256,128},{288,160},{320,192},{... | collective-permute-start | bytes 196616 | tf_op jit(solution)/shard_map/ppermute | solution.py:30
  49.7 4.8 %collective-permute-done.7 = bf16[4,64,128]{2,1,0:T(8,128)(2,1)S(1)} collective-permute-done((bf16[4,64,128]{2,1,0:T(8,128)(2,1)S(1)}, bf16[4,64,128]{2,1,0:T(8,128)(2,1)S(1)}, u32[]{:S(2)}, u32[]{:S(2)}) %collective-permute-start.7) | collective-permute-done | bytes 65568 | tf_op jit(solution)/shard_map/ppermute | solution.py:30
  58.4 4.5 %collective-permute-done.8 = bf16[4,64,128]{2,1,0:T(8,128)(2,1)S(1)} collective-permute-done((bf16[4,64,128]{2,1,0:T(8,128)(2,1)S(1)}, bf16[4,64,128]{2,1,0:T(8,128)(2,1)S(1)}, u32[]{:S(2)}, u32[]{:S(2)}) %collective-permute-start.8) | collective-permute-done | bytes 65568 | tf_op jit(solution)/shard_map/ppermute | solution.py:30
  62.9 5.0 %collective-permute-start.9 = (bf16[4,64,128]{2,1,0:T(8,128)(2,1)S(1)}, bf16[4,64,128]{2,1,0:T(8,128)(2,1)S(1)}, u32[]{:S(2)}, u32[]{:S(2)}) collective-permute-start(bf16[4,64,128]{2,1,0:T(8,128)(2,1)S(1)} %all-to-all-done.1), channel_id=1, source_target_pairs={{96,0},{128,32},{160,64},{192,96},{224,128},{256,160},{288,192},{3... | collective-permute-start | bytes 196616 | tf_op jit(solution)/shard_map/ppermute | solution.py:30
  70.1 8.2 %collective-permute-start.6 = (bf16[4,64,256]{2,1,0:T(8,128)(2,1)S(1)}, bf16[4,64,256]{2,1,0:T(8,128)(2,1)S(1)}, u32[]{:S(2)}, u32[]{:S(2)}) collective-permute-start(bf16[4,64,256]{2,1,0:T(8,128)(2,1)S(1)} %all-to-all-done), channel_id=1, source_target_pairs={{32,0},{64,32},{96,64},{128,96},{160,128},{192,160},{224,192},{256... | collective-permute-start | bytes 393224 | tf_op jit(solution)/shard_map/ppermute | solution.py:30
  86.6 4.2 %collective-permute-start = (bf16[4,64,256]{2,1,0:T(8,128)(2,1)S(1)}, bf16[4,64,256]{2,1,0:T(8,128)(2,1)S(1)}, u32[]{:S(2)}, u32[]{:S(2)}) collective-permute-start(bf16[4,64,256]{2,1,0:T(8,128)(2,1)S(1)} %all-to-all-done), channel_id=1, source_target_pairs={{128,0},{160,32},{192,64},{224,96},{256,128},{288,160},{320,192},{... | collective-permute-start | bytes 393224 | tf_op jit(solution)/shard_map/ppermute | solution.py:30
  90.8 8.6 %collective-permute-done = bf16[4,64,256]{2,1,0:T(8,128)(2,1)S(1)} collective-permute-done((bf16[4,64,256]{2,1,0:T(8,128)(2,1)S(1)}, bf16[4,64,256]{2,1,0:T(8,128)(2,1)S(1)}, u32[]{:S(2)}, u32[]{:S(2)}) %collective-permute-start) | collective-permute-done | bytes 131104 | tf_op jit(solution)/shard_map/ppermute | solution.py:30
  99.4 6.4 %collective-permute-start.1 = (bf16[4,64,256]{2,1,0:T(8,128)(2,1)S(1)}, bf16[4,64,256]{2,1,0:T(8,128)(2,1)S(1)}, u32[]{:S(2)}, u32[]{:S(2)}) collective-permute-start(bf16[4,64,256]{2,1,0:T(8,128)(2,1)S(1)} %all-to-all-done), channel_id=1, source_target_pairs={{416,0},{448,32},{480,64},{0,96},{32,128},{64,160},{96,192},{128,2... | collective-permute-start | bytes 393224 | tf_op jit(solution)/shard_map/ppermute | solution.py:30
  105.9 4.2 %collective-permute-done.1 = bf16[4,64,256]{2,1,0:T(8,128)(2,1)S(1)} collective-permute-done((bf16[4,64,256]{2,1,0:T(8,128)(2,1)S(1)}, bf16[4,64,256]{2,1,0:T(8,128)(2,1)S(1)}, u32[]{:S(2)}, u32[]{:S(2)}) %collective-permute-start.1) | collective-permute-done | bytes 131104 | tf_op jit(solution)/shard_map/ppermute | solution.py:30
  110.1 5.4 %collective-permute-start.2 = (bf16[4,64,256]{2,1,0:T(8,128)(2,1)S(1)}, bf16[4,64,256]{2,1,0:T(8,128)(2,1)S(1)}, u32[]{:S(2)}, u32[]{:S(2)}) collective-permute-start(bf16[4,64,256]{2,1,0:T(8,128)(2,1)S(1)} %all-to-all-done), channel_id=1, source_target_pairs={{96,0},{128,32},{160,64},{192,96},{224,128},{256,160},{288,192},{3... | collective-permute-start | bytes 393224 | tf_op jit(solution)/shard_map/ppermute | solution.py:30
  115.6 5.5 %collective-permute-done.2 = bf16[4,64,256]{2,1,0:T(8,128)(2,1)S(1)} collective-permute-done((bf16[4,64,256]{2,1,0:T(8,128)(2,1)S(1)}, bf16[4,64,256]{2,1,0:T(8,128)(2,1)S(1)}, u32[]{:S(2)}, u32[]{:S(2)}) %collective-permute-start.2) | collective-permute-done | bytes 131104 | tf_op jit(solution)/shard_map/ppermute | solution.py:30
  122.9 24.8 %all-gather.1 = f32[8,2,256]{2,1,0:T(2,128)S(1)} all-gather(f32[1,2,256]{2,1,0:T(2,128)S(1)} %maximum_bitcast_fusion), channel_id=2, replica_groups=mesh['rep'=2,'z'=8,'y'=4,'x'=4,'core'=2] {'x','core'}, dimensions={0}, use_global_device_ids=true | all-gather | bytes 18432 | tf_op jit(solution)/shard_map/all_gather | solution.py:92
  148.4 4.4 %all_to_all.50 = bf16[2,128,2048]{2,1,0:T(8,128)(2,1)S(1)} all-to-all(bf16[2,128,2048]{2,1,0:T(8,128)(2,1)S(1)} %bitcast.68), channel_id=1, replica_groups=mesh['rep'=2,'z'=8,'y'=4,'x'=4,'core'=2] {'core'}, dimensions={0} | all-to-all | bytes 2097152 | tf_op jit(solution)/shard_map/all_to_all | solution.py:21
  157.5 9.2 %all-to-all-done.3 = bf16[4,32,2048]{2,1,0:T(8,128)(2,1)S(1)} async-done(((bf16[4,32,2048]{2,1,0:T(8,128)(2,1)}), bf16[4,32,2048]{2,1,0:T(8,128)(2,1)S(1)}, u32[]{:S(2)}, u32[]{:S(2)}) %all-to-all-start.3) | async-done | bytes 524320 | tf_op jit(solution)/shard_map/all_to_all | solution.py:21
  171.4 8.0 %all-to-all-done.4 = bf16[4,32,2048]{2,1,0:T(8,128)(2,1)S(1)} async-done(((bf16[4,32,2048]{2,1,0:T(8,128)(2,1)}), bf16[4,32,2048]{2,1,0:T(8,128)(2,1)S(1)}, u32[]{:S(2)}, u32[]{:S(2)}) %all-to-all-start.4) | async-done | bytes 524320 | tf_op jit(solution)/shard_map/all_to_all | solution.py:21
  179.5 6.6 %all_to_all.51 = bf16[2,128,2048]{2,1,0:T(8,128)(2,1)S(1)} all-to-all(bf16[2,128,2048]{2,1,0:T(8,128)(2,1)S(1)} %broadcast_in_dim.114), channel_id=1, replica_groups=mesh['rep'=2,'z'=8,'y'=4,'x'=4,'core'=2] {'core'}, dimensions={0} | all-to-all | bytes 2097152 | tf_op jit(solution)/shard_map/all_to_all | solution.py:21
  186.1 4.9 %fusion.7 = f32[256,2048]{1,0:T(8,128)} fusion(bf16[4096,1024]{1,0:T(8,128)(2,1)} %all-gather.4.cloned.1.call-done, bf16[256,2048]{1,0:T(8,128)(2,1)S(1)} %bitcast.74, f32[512]{0:T(512)S(1)} %get-tuple-element.11), kind=kOutput, calls=%fused_computation.11 | convolution fusion | flops 1074266112 | bytes 7342080 | tf_op jit(solution)/shard_map/dot_general | solution.py:101
  191.0 4.2 %fusion = bf16[256,2048]{1,0:T(8,128)(2,1)S(1)} fusion(f32[256,2048]{1,0:T(8,128)} %fusion.7, bf16[4096,1024]{1,0:T(8,128)(2,1)} %all-gather.4.cloned.1.call-done, bf16[256,2048]{1,0:T(8,128)(2,1)S(1)} %bitcast.75, f32[512]{0:T(512)S(1)} %get-tuple-element.10), kind=kOutput, calls=%fused_computation.3 | convolution fusion | flops 1075314688 | bytes 8390656 | tf_op jit(solution)/shard_map/dot_general | solution.py:101
  195.2 4.6 %all_to_all.52 = bf16[2,128,2048]{2,1,0:T(8,128)(2,1)S(1)} all-to-all(bf16[2,128,2048]{2,1,0:T(8,128)(2,1)S(1)} %bitcast.76), channel_id=1, replica_groups=mesh['rep'=2,'z'=8,'y'=4,'x'=4,'core'=2] {'core'}, dimensions={0} | all-to-all | bytes 2097152 | tf_op jit(solution)/shard_map/all_to_all | solution.py:21
  200.1 11.6 %all_to_all.53 = bf16[4,32,2048]{2,1,0:T(8,128)(2,1)S(1)} all-to-all(bf16[4,32,2048]{2,1,0:T(8,128)(2,1)S(1)} %bitcast.73), channel_id=1, replica_groups=mesh['rep'=2,'z'=8,'y'=4,'x'=4,'core'=2] {'x'}, dimensions={0} | all-to-all | bytes 1048576 | tf_op jit(solution)/shard_map/all_to_all | solution.py:21
  211.8 10.7 %all_to_all.54 = bf16[4,32,2048]{2,1,0:T(8,128)(2,1)S(1)} all-to-all(bf16[4,32,2048]{2,1,0:T(8,128)(2,1)S(1)} %broadcast_in_dim.115), channel_id=1, replica_groups=mesh['rep'=2,'z'=8,'y'=4,'x'=4,'core'=2] {'x'}, dimensions={0} | all-to-all | bytes 1048576 | tf_op jit(solution)/shard_map/all_to_all | solution.py:21
  222.7 6.3 %all_to_all.55 = bf16[2,128,2048]{2,1,0:T(8,128)(2,1)S(1)} all-to-all(bf16[2,128,2048]{2,1,0:T(8,128)(2,1)S(1)} %broadcast_in_dim.116), channel_id=1, replica_groups=mesh['rep'=2,'z'=8,'y'=4,'x'=4,'core'=2] {'core'}, dimensions={0} | all-to-all | bytes 2097152 | tf_op jit(solution)/shard_map/all_to_all | solution.py:21
  (99 shorter events, 49.6 us)
Async XLA Ops:
  6.5 179.5 %all-gather.4.cloned.1.call-start = ((), (), s32[]{:S(2)}) async-start(), calls=%async_computation.10 | async-start | bytes 8519680 | tf_op jit(solution)/shard_map/all_gather | solution.py:129
  11.3 9.5 %all-to-all-start.1 = ((bf16[4,64,128]{2,1,0:T(8,128)(2,1)}), bf16[4,64,128]{2,1,0:T(8,128)(2,1)S(1)}, u32[]{:S(2)}, u32[]{:S(2)}) async-start(bf16[4,64,128]{2,1,0:T(8,128)(2,1)} %broadcast_in_dim.104), calls=%async_computation.1 | async-start | bytes 131072 | tf_op jit(solution)/shard_map/all_to_all | solution.py:21
  21.5 28.1 %all-to-all-start = ((bf16[4,64,256]{2,1,0:T(8,128)(2,1)}), bf16[4,64,256]{2,1,0:T(8,128)(2,1)S(1)}, u32[]{:S(2)}, u32[]{:S(2)}) async-start(bf16[4,64,256]{2,1,0:T(8,128)(2,1)} %broadcast_in_dim.93), calls=%async_computation | async-start | bytes 262144 | tf_op jit(solution)/shard_map/all_to_all | solution.py:21
  25.0 61.6 %collective-permute-start.13 = (bf16[4,64,128]{2,1,0:T(8,128)(2,1)S(1)}, bf16[4,64,128]{2,1,0:T(8,128)(2,1)S(1)}, u32[]{:S(2)}, u32[]{:S(2)}) collective-permute-start(bf16[4,64,128]{2,1,0:T(8,128)(2,1)S(1)} %all-to-all-done.1), channel_id=1, source_target_pairs={{32,0},{64,32},{96,64},{128,96},{160,128},{192,160},{224,192},{256... | collective-permute-start | bytes 196616 | tf_op jit(solution)/shard_map/ppermute | solution.py:30
  36.1 47.4 %collective-permute-start.12 = (bf16[4,64,128]{2,1,0:T(8,128)(2,1)S(1)}, bf16[4,64,128]{2,1,0:T(8,128)(2,1)S(1)}, u32[]{:S(2)}, u32[]{:S(2)}) collective-permute-start(bf16[4,64,128]{2,1,0:T(8,128)(2,1)S(1)} %all-to-all-done.1), channel_id=1, source_target_pairs={{480,0},{0,32},{32,64},{64,96},{96,128},{128,160},{160,192},{192,2... | collective-permute-start | bytes 196616 | tf_op jit(solution)/shard_map/ppermute | solution.py:30
  38.0 42.3 %collective-permute-start.11 = (bf16[4,64,128]{2,1,0:T(8,128)(2,1)S(1)}, bf16[4,64,128]{2,1,0:T(8,128)(2,1)S(1)}, u32[]{:S(2)}, u32[]{:S(2)}) collective-permute-start(bf16[4,64,128]{2,1,0:T(8,128)(2,1)S(1)} %all-to-all-done.1), channel_id=1, source_target_pairs={{64,0},{96,32},{128,64},{160,96},{192,128},{224,160},{256,192},{28... | collective-permute-start | bytes 196616 | tf_op jit(solution)/shard_map/ppermute | solution.py:30
  41.8 36.5 %collective-permute-start.10 = (bf16[4,64,128]{2,1,0:T(8,128)(2,1)S(1)}, bf16[4,64,128]{2,1,0:T(8,128)(2,1)S(1)}, u32[]{:S(2)}, u32[]{:S(2)}) collective-permute-start(bf16[4,64,128]{2,1,0:T(8,128)(2,1)S(1)} %all-to-all-done.1), channel_id=1, source_target_pairs={{448,0},{480,32},{0,64},{32,96},{64,128},{96,160},{128,192},{160,2... | collective-permute-start | bytes 196616 | tf_op jit(solution)/shard_map/ppermute | solution.py:30
  44.2 10.3 %collective-permute-start.7 = (bf16[4,64,128]{2,1,0:T(8,128)(2,1)S(1)}, bf16[4,64,128]{2,1,0:T(8,128)(2,1)S(1)}, u32[]{:S(2)}, u32[]{:S(2)}) collective-permute-start(bf16[4,64,128]{2,1,0:T(8,128)(2,1)S(1)} %all-to-all-done.1), channel_id=1, source_target_pairs={{128,0},{160,32},{192,64},{224,96},{256,128},{288,160},{320,192},{... | collective-permute-start | bytes 196616 | tf_op jit(solution)/shard_map/ppermute | solution.py:30
  49.5 71.7 %copy-start.1 = (bf16[256,2048]{1,0:T(8,128)(2,1)S(1)}, bf16[256,2048]{1,0:T(8,128)(2,1)}, u32[]{:S(2)}) copy-start(bf16[256,2048]{1,0:T(8,128)(2,1)} %param.15) | copy-start | bytes 3145732
  49.5 71.7 %copy-start.6 = (f32[2048]{0:T(1024)S(1)}, f32[2048]{0:T(1024)}, u32[]{:S(2)}) copy-start(f32[2048]{0:T(1024)} %param.16) | copy-start | bytes 24580
  54.5 8.4 %collective-permute-start.8 = (bf16[4,64,128]{2,1,0:T(8,128)(2,1)S(1)}, bf16[4,64,128]{2,1,0:T(8,128)(2,1)S(1)}, u32[]{:S(2)}, u32[]{:S(2)}) collective-permute-start(bf16[4,64,128]{2,1,0:T(8,128)(2,1)S(1)} %all-to-all-done.1), channel_id=1, source_target_pairs={{416,0},{448,32},{480,64},{0,96},{32,128},{64,160},{96,192},{128,2... | collective-permute-start | bytes 196616 | tf_op jit(solution)/shard_map/ppermute | solution.py:30
  62.9 7.2 %collective-permute-start.9 = (bf16[4,64,128]{2,1,0:T(8,128)(2,1)S(1)}, bf16[4,64,128]{2,1,0:T(8,128)(2,1)S(1)}, u32[]{:S(2)}, u32[]{:S(2)}) collective-permute-start(bf16[4,64,128]{2,1,0:T(8,128)(2,1)S(1)} %all-to-all-done.1), channel_id=1, source_target_pairs={{96,0},{128,32},{160,64},{192,96},{224,128},{256,160},{288,192},{3... | collective-permute-start | bytes 196616 | tf_op jit(solution)/shard_map/ppermute | solution.py:30
  70.1 51.1 %collective-permute-start.6 = (bf16[4,64,256]{2,1,0:T(8,128)(2,1)S(1)}, bf16[4,64,256]{2,1,0:T(8,128)(2,1)S(1)}, u32[]{:S(2)}, u32[]{:S(2)}) collective-permute-start(bf16[4,64,256]{2,1,0:T(8,128)(2,1)S(1)} %all-to-all-done), channel_id=1, source_target_pairs={{32,0},{64,32},{96,64},{128,96},{160,128},{192,160},{224,192},{256... | collective-permute-start | bytes 393224 | tf_op jit(solution)/shard_map/ppermute | solution.py:30
  78.3 42.8 %collective-permute-start.5 = (bf16[4,64,256]{2,1,0:T(8,128)(2,1)S(1)}, bf16[4,64,256]{2,1,0:T(8,128)(2,1)S(1)}, u32[]{:S(2)}, u32[]{:S(2)}) collective-permute-start(bf16[4,64,256]{2,1,0:T(8,128)(2,1)S(1)} %all-to-all-done), channel_id=1, source_target_pairs={{480,0},{0,32},{32,64},{64,96},{96,128},{128,160},{160,192},{192,2... | collective-permute-start | bytes 393224 | tf_op jit(solution)/shard_map/ppermute | solution.py:30
  80.3 40.8 %collective-permute-start.4 = (bf16[4,64,256]{2,1,0:T(8,128)(2,1)S(1)}, bf16[4,64,256]{2,1,0:T(8,128)(2,1)S(1)}, u32[]{:S(2)}, u32[]{:S(2)}) collective-permute-start(bf16[4,64,256]{2,1,0:T(8,128)(2,1)S(1)} %all-to-all-done), channel_id=1, source_target_pairs={{64,0},{96,32},{128,64},{160,96},{192,128},{224,160},{256,192},{28... | collective-permute-start | bytes 393224 | tf_op jit(solution)/shard_map/ppermute | solution.py:30
  83.4 37.6 %collective-permute-start.3 = (bf16[4,64,256]{2,1,0:T(8,128)(2,1)S(1)}, bf16[4,64,256]{2,1,0:T(8,128)(2,1)S(1)}, u32[]{:S(2)}, u32[]{:S(2)}) collective-permute-start(bf16[4,64,256]{2,1,0:T(8,128)(2,1)S(1)} %all-to-all-done), channel_id=1, source_target_pairs={{448,0},{480,32},{0,64},{32,96},{64,128},{96,160},{128,192},{160,2... | collective-permute-start | bytes 393224 | tf_op jit(solution)/shard_map/ppermute | solution.py:30
  86.6 12.8 %collective-permute-start = (bf16[4,64,256]{2,1,0:T(8,128)(2,1)S(1)}, bf16[4,64,256]{2,1,0:T(8,128)(2,1)S(1)}, u32[]{:S(2)}, u32[]{:S(2)}) collective-permute-start(bf16[4,64,256]{2,1,0:T(8,128)(2,1)S(1)} %all-to-all-done), channel_id=1, source_target_pairs={{128,0},{160,32},{192,64},{224,96},{256,128},{288,160},{320,192},{... | collective-permute-start | bytes 393224 | tf_op jit(solution)/shard_map/ppermute | solution.py:30
  99.4 10.7 %collective-permute-start.1 = (bf16[4,64,256]{2,1,0:T(8,128)(2,1)S(1)}, bf16[4,64,256]{2,1,0:T(8,128)(2,1)S(1)}, u32[]{:S(2)}, u32[]{:S(2)}) collective-permute-start(bf16[4,64,256]{2,1,0:T(8,128)(2,1)S(1)} %all-to-all-done), channel_id=1, source_target_pairs={{416,0},{448,32},{480,64},{0,96},{32,128},{64,160},{96,192},{128,2... | collective-permute-start | bytes 393224 | tf_op jit(solution)/shard_map/ppermute | solution.py:30
  110.1 10.9 %collective-permute-start.2 = (bf16[4,64,256]{2,1,0:T(8,128)(2,1)S(1)}, bf16[4,64,256]{2,1,0:T(8,128)(2,1)S(1)}, u32[]{:S(2)}, u32[]{:S(2)}) collective-permute-start(bf16[4,64,256]{2,1,0:T(8,128)(2,1)S(1)} %all-to-all-done), channel_id=1, source_target_pairs={{96,0},{128,32},{160,64},{192,96},{224,128},{256,160},{288,192},{3... | collective-permute-start | bytes 393224 | tf_op jit(solution)/shard_map/ppermute | solution.py:30
  121.7 26.1 %copy-start.4 = (f32[128]{0:T(128)S(1)}, f32[128]{0:T(128)}, u32[]{:S(2)}) copy-start(f32[128]{0:T(128)} %param.22) | copy-start | bytes 1540
  152.8 14.2 %copy-start.2 = (f32[2048]{0:T(1024)S(1)}, f32[2048]{0:T(1024)}, u32[]{:S(2)}) copy-start(f32[2048]{0:T(1024)} %param.25) | copy-start | bytes 24580
  153.9 17.5 %copy-start.3 = (f32[1024]{0:T(1024)S(1)}, f32[1024]{0:T(1024)}, u32[]{:S(2)}) copy-start(f32[1024]{0:T(1024)} %param.27) | copy-start | bytes 12292
  153.9 12.8 %all-to-all-start.3 = ((bf16[4,32,2048]{2,1,0:T(8,128)(2,1)}), bf16[4,32,2048]{2,1,0:T(8,128)(2,1)S(1)}, u32[]{:S(2)}, u32[]{:S(2)}) async-start(bf16[4,32,2048]{2,1,0:T(8,128)(2,1)} %bitcast.28), calls=%async_computation.3 | async-start | bytes 1048576 | tf_op jit(solution)/shard_map/all_to_all | solution.py:21
  167.9 11.5 %all-to-all-start.4 = ((bf16[4,32,2048]{2,1,0:T(8,128)(2,1)}), bf16[4,32,2048]{2,1,0:T(8,128)(2,1)S(1)}, u32[]{:S(2)}, u32[]{:S(2)}) async-start(bf16[4,32,2048]{2,1,0:T(8,128)(2,1)} %broadcast_in_dim.113), calls=%async_computation.4 | async-start | bytes 1048576 | tf_op jit(solution)/shard_map/all_to_all | solution.py:21
  (2 other events, 1.7 us)
Sparse Core Ops, SparseCore 0:
  10.3 158.3 all-gather.3

commit v2 on v1

--- a/solution.py
+++ b/solution.py
@@ -3,6 +3,7 @@
 from jax import lax
 from jax.sharding import Mesh
 from jax.sharding import PartitionSpec as P
+
 
 SEQ_LEN = 128
 FS = ("z", "y")
@@ -30,14 +31,39 @@
     return lax.ppermute(x, RING, [((i + distance) % n, i) for i in range(n)])
 
 
+def y_ring(block):
+    n = lax.axis_size("y")
+    at = lax.axis_index("y")
+    whole = jnp.zeros((n, *block.shape), block.dtype)
+    whole = lax.dynamic_update_index_in_dim(whole, block, at, 0)
+    for d in (2, 1, 3):
+        other = lax.ppermute(block, "y", [((i + d) % n, i) for i in range(n)])
+        whole = lax.dynamic_update_index_in_dim(whole, other, (at + d) % n, 0)
+    return whole
+
+
 def ring_window(block):
     n = lax.axis_size("z")
     at = lax.axis_index("z")
+    cut = block.shape[0] // 2
     whole = jnp.zeros((n, *block.shape), block.dtype)
     whole = lax.dynamic_update_index_in_dim(whole, block, at, 0)
-    for d in (4, -3, 3, -2, 2, -1, 1):
-        whole = lax.dynamic_update_index_in_dim(whole, shifted(block, d), (at + d) % n, 0)
-    return whole
+    ahead = behind = block
+    for d in range(1, n // 2):
+        ahead = shifted(ahead, 1)
+        behind = shifted(behind, -1)
+        whole = lax.dynamic_update_index_in_dim(whole, ahead, (at + d) % n, 0)
+        whole = lax.dynamic_update_index_in_dim(whole, behind, (at - d) % n, 0)
+    ahead = shifted(ahead[:cut], 1)
+    behind = shifted(behind[cut:], -1)
+    last = jnp.concatenate([ahead, behind])
+    return lax.dynamic_update_index_in_dim(whole, last, (at + n // 2) % n, 0)
+
+
+def fs_copies(x):
+    by_z = copies_from(x, "z")
+    by_y = copies_from(by_z, "y")
+    return by_y.swapaxes(0, 1).reshape(-1, x.shape[1])
 
 
 def summed(x, axis):
@@ -52,8 +78,7 @@
 
 
 def tp_gathered(rows):
-    part = copies_from(rows, "x")
-    part = part.reshape(-1, rows.shape[1])
+    part = copies_from(rows, "x").reshape(-1, rows.shape[1])
     return copies_from(part, "core").reshape(-1, rows.shape[1])
 
 
@@ -123,14 +148,20 @@
     width = value_weight.shape[1]
     mix_t = (mixout_weight.astype(BF16).astype(F32) * rounded(mixout_scale)).astype(BF16).T
     down_t = (down_weight.astype(BF16).astype(F32) * rounded(down_scale)).astype(BF16).T
-    half = up_weight.shape[1] // reps
-    up_half = lax.dynamic_slice_in_dim(up_weight, rep * half, half, 1).astype(BF16)
-    down_half = lax.dynamic_slice_in_dim(down_t, rep * half, half, 1)
-    ffn = lax.all_gather(jnp.concatenate([up_half, down_half], axis=1), REP_FS, axis=0, tiled=True)
-
     glu_local = jnp.concatenate([value_weight.astype(BF16), gate_weight.astype(BF16)], axis=1)
-    glu_whole = ring_window(copies_from(glu_local, "y")).reshape(-1, 2 * width)
-    mix_whole = ring_window(copies_from(mix_t, "y")).reshape(-1, width)
+    glu_whole = fs_copies(glu_local)
+    mix_whole = fs_copies(mix_t)
+
+    hid = up_weight.shape[1]
+    early = hid // 2
+    half = (hid - early) // reps
+    late = lax.dynamic_slice_in_dim(down_t, early + rep * half, half, 1)
+    late = lax.all_gather(jnp.pad(late, ((0, 0), (0, (-half) % 512))), RING, axis=0)[:, :, :half]
+    late = lax.all_gather(late, "y")
+    near = jnp.concatenate([up_weight.astype(BF16), down_t[:, :early]], axis=1)
+    near = ring_window(y_ring(near)).reshape(-1, hid + early)
+    zs = lax.axis_size("z")
+    late = [late[:, r * zs : (r + 1) * zs].swapaxes(0, 1).reshape(-1, half) for r in range(reps)]
 
     normed = rms_rows(tokens, first_gain)
     sums = jnp.dot(normed, glu_whole, preferred_element_type=F32)
@@ -142,14 +173,12 @@
     middle = (own_rows(tokens).astype(F32) + mix_sum).astype(BF16)
     normed2 = tp_gathered(rms_rows(middle, second_gain))
 
-    rows = ffn.shape[0] // reps
-    up_mult = rounded(up_scale)
-    down_sum = 0.0
+    up_sum = jnp.dot(normed2, near[:, :hid], preferred_element_type=F32)
+    hidden = jnp.square(jax.nn.relu(up_sum * rounded(up_scale))).astype(BF16)
+    down_sum = dot_t(hidden[:, :early], near[:, hid:])
     for r in range(reps):
-        part = ffn[r * rows : (r + 1) * rows]
-        up_sum = jnp.dot(normed2, part[:, :half], preferred_element_type=F32)
-        hidden = jnp.square(jax.nn.relu(up_sum * up_mult[r * half : (r + 1) * half])).astype(BF16)
-        down_sum = down_sum + dot_t(hidden, part[:, half:])
+        at = early + r * half
+        down_sum = down_sum + dot_t(hidden[:, at : at + half], late[r])
     layer_out = (middle.astype(F32) + tp_scattered(down_sum)).astype(BF16)
     return tp_gathered(layer_out)
 
@@ -176,6 +205,7 @@
         P(TP, FS),
         P(FS),
     )
+
     return jax.shard_map(
         on_device, mesh=torus, in_specs=placed, out_specs=P(REP_FS, None), check_vma=False
     )

time: 240 us -> 234 us (0.975)
  local copies, waits for them, and re-layouts: 4.38 us -> 25.8 us
  waiting for transfers between devices: 47.7 us -> 30.2 us
  blocking collectives: 69 us -> 60.7 us
    ppermute x14 -> x8, starting transfers between devices: 65.6 us -> 30.3 us  [shifted(): return lax.ppermute(x, RING, [((i + distance) % n, i) for i in range(n)])]
    all_to_all x4 -> x7, starting transfers between devices: 15.6 us -> 40 us  [exchange(): return lax.all_to_all(x, axis, split_axis=0, concat_axis=0, tiled=True)]
    ppermute x14 -> x8, waiting for transfers between devices: 29.8 us -> 6.3 us  [shifted(): return lax.ppermute(x, RING, [((i + distance) % n, i) for i in range(n)])]
    ppermute x0 -> x3, starting transfers between devices: none -> 10.9 us  [y_ring(): other = lax.ppermute(block, 'y', [((i + d) % n, i) for i in range(n)])]
    dynamic_update_slice x14 -> x9, local copies, waits for them, and re-layouts: 0.24 us -> 10.3 us  [the longest x3 5.11 us: ring_window(): whole = lax.dynamic_update_index_in_dim(whole, ahead, (at + d) % n, 0)]
    all_to_all x4 -> x7, waiting for transfers between devices: 17.9 us -> 23.8 us  [exchange(): return lax.all_to_all(x, axis, split_axis=0, concat_axis=0, tiled=True)]
    all_to_all x6 -> x5, blocking collectives: 44.2 us -> 38.3 us  [exchange(): return lax.all_to_all(x, axis, split_axis=0, concat_axis=0, tiled=True)]
    dot_general x3 -> x4, matrix products: 9.55 us -> 3.76 us  [dot_t(): lax.dot_general(a, b, (((1,), (1,)), ((), ())), preferred_element_type=F32)]
  transfers between devices with their start and end apart: 19 -> 20, of which waited for: 9 -> 6; matrix products, arithmetic and copies ran while one was open for 5% -> 16% of each run, Pallas kernels for 0% -> 0%
where the time goes in v2:
time: 234 us; the launch traced here: 232 us
  starting transfers between devices  81.2 us (35%)
  blocking collectives  60.7 us (26%)
  waiting for transfers between devices  30.2 us (13%)
  local copies, waits for them, and re-layouts  25.8 us (11%)
  between operations  14.1 us (6%)
  other arithmetic  11.8 us (5%)
  matrix products  8.24 us (4%)
    all_to_all x7, starting transfers between devices, exchange(): return lax.all_to_all(x, axis, split_axis=0, concat_axis=0, tiled=True)  40 us
    all_to_all x5, blocking collectives, exchange(): return lax.all_to_all(x, axis, split_axis=0, concat_axis=0, tiled=True)  38.3 us
    ppermute x8, starting transfers between devices, shifted(): return lax.ppermute(x, RING, [((i + distance) % n, i) for i in range(n)])  30.3 us
    all_to_all x7, waiting for transfers between devices, exchange(): return lax.all_to_all(x, axis, split_axis=0, concat_axis=0, tiled=True)  23.8 us
    all_gather x1, blocking collectives, channel_stats(): both = lax.all_gather(jnp.stack([total, spread]), TP)  22.3 us
    ppermute x3, starting transfers between devices, y_ring(): other = lax.ppermute(block, 'y', [((i + d) % n, i) for i in range(n)])  10.9 us
    ppermute x8, waiting for transfers between devices, shifted(): return lax.ppermute(x, RING, [((i + distance) % n, i) for i in range(n)])  6.3 us
    broadcast_in_dim x8, local copies, waits for them, and re-layouts, copies_from(): return exchange(jnp.broadcast_to(x, (lax.axis_size(axis), *x.shape)), axis)  5.5 us
  transfers between devices with their start and end apart: 20, of which 6 were waited for; matrix products, arithmetic and copies ran while one was open for 16% of the time, Pallas kernels for 0%

profile of v2, /device:TPU:1, one launch (start us, length us, event | category | flops | bytes accessed | tf_op | source)
XLA Modules:
  0.0 232.1 jit_solution(13671213174871841876)
XLA Ops:
  9.3 5.6 %collective-permute-start = (bf16[64,1536]{1,0:T(8,128)(2,1)S(1)}, bf16[64,1536]{1,0:T(8,128)(2,1)S(1)}, u32[]{:S(2)}, u32[]{:S(2)}) collective-permute-start(bf16[64,1536]{1,0:T(8,128)(2,1)S(1)} %pad_maximum_fusion), channel_id=1, source_target_pairs={{16,0},{24,8},{0,16},{8,24},{17,1},{25,9},{1,17},{9,25},{18,2},{26... | collective-permute-start | bytes 589832 | tf_op jit(solution)/shard_map/ppermute | solution.py:40
  22.4 12.2 %all-to-all-start.2 = ((bf16[8,64,128]{2,1,0:T(8,128)(2,1)}), bf16[8,64,128]{2,1,0:T(8,128)(2,1)S(1)}, u32[]{:S(2)}, u32[]{:S(2)}) async-start(bf16[8,64,128]{2,1,0:T(8,128)(2,1)} %broadcast_in_dim.88), calls=%async_computation.2 | async-start | bytes 262144 | tf_op jit(solution)/shard_map/all_to_all | solution.py:22
  39.7 5.3 %all-to-all-done.2 = bf16[8,64,128]{2,1,0:T(8,128)(2,1)S(1)} async-done(((bf16[8,64,128]{2,1,0:T(8,128)(2,1)}), bf16[8,64,128]{2,1,0:T(8,128)(2,1)S(1)}, u32[]{:S(2)}, u32[]{:S(2)}) %all-to-all-start.2) | async-done | bytes 131104 | tf_op jit(solution)/shard_map/all_to_all | solution.py:22
  45.9 3.5 %all-to-all-start.3 = ((bf16[4,8,64,128]{3,2,1,0:T(8,128)(2,1)}), bf16[4,8,64,128]{3,2,1,0:T(8,128)(2,1)S(1)}, u32[]{:S(2)}, u32[]{:S(2)}) async-start(bf16[4,8,64,128]{3,2,1,0:T(8,128)(2,1)} %broadcast_in_dim.89), calls=%async_computation.3 | async-start | bytes 1048576 | tf_op jit(solution)/shard_map/all_to_all | solution.py:22
  49.5 4.2 %collective-permute-start.3 = (bf16[4,64,1536]{2,1,0:T(8,128)(2,1)S(1)}, bf16[4,64,1536]{2,1,0:T(8,128)(2,1)}, u32[]{:S(2)}, u32[]{:S(2)}) collective-permute-start(bf16[4,64,1536]{2,1,0:T(8,128)(2,1)S(1)} %bitcast_dynamic-update-slice_fusion.7), channel_id=1, source_target_pairs={{32,0},{64,32},{96,64},{128,96},{160,128},{192,160},{224,192},{256... | collective-permute-start | bytes 2359304 | tf_op jit(solution)/shard_map/ppermute | solution.py:31
  57.0 6.4 %all-to-all-start = ((bf16[8,64,256]{2,1,0:T(8,128)(2,1)}), bf16[8,64,256]{2,1,0:T(8,128)(2,1)S(1)}, u32[]{:S(2)}, u32[]{:S(2)}) async-start(bf16[8,64,256]{2,1,0:T(8,128)(2,1)} %broadcast_in_dim.85), calls=%async_computation | async-start | bytes 524288 | tf_op jit(solution)/shard_map/all_to_all | solution.py:22
  63.6 3.4 %broadcast_in_dim.92 = bf16[8,4,64,1536]{3,2,1,0:T(8,128)(2,1)} broadcast(bf16[]{:T(256)} %constant.144.clone.1), dimensions={} | broadcast | bytes 6291458 | tf_op jit(solution)/shard_map/broadcast_in_dim | solution.py:49
  68.0 11.8 %all-to-all-done = bf16[8,64,256]{2,1,0:T(8,128)(2,1)S(1)} async-done(((bf16[8,64,256]{2,1,0:T(8,128)(2,1)}), bf16[8,64,256]{2,1,0:T(8,128)(2,1)S(1)}, u32[]{:S(2)}, u32[]{:S(2)}) %all-to-all-start) | async-done | bytes 262176 | tf_op jit(solution)/shard_map/all_to_all | solution.py:22
  80.9 4.3 %all-to-all-start.1 = ((bf16[4,8,64,256]{3,2,1,0:T(8,128)(2,1)}), bf16[4,8,64,256]{3,2,1,0:T(8,128)(2,1)S(1)}, u32[]{:S(2)}, u32[]{:S(2)}) async-start(bf16[4,8,64,256]{3,2,1,0:T(8,128)(2,1)} %broadcast_in_dim.86), calls=%async_computation.1 | async-start | bytes 2097152 | tf_op jit(solution)/shard_map/all_to_all | solution.py:22
  85.2 8.9 %collective-permute-start.5 = (bf16[4,64,1536]{2,1,0:T(8,128)(2,1)}, bf16[4,64,1536]{2,1,0:T(8,128)(2,1)}, u32[]{:S(2)}, u32[]{:S(2)}) collective-permute-start(bf16[4,64,1536]{2,1,0:T(8,128)(2,1)} %collective-permute-done.3), channel_id=1, source_target_pairs={{32,0},{64,32},{96,64},{128,96},{160,128},{192,160},{224,192},{256... | collective-permute-start | bytes 2359304 | tf_op jit(solution)/shard_map/ppermute | solution.py:31
  102.0 22.3 %all-gather.3 = f32[8,2,256]{2,1,0:T(2,128)S(1)} all-gather(f32[1,2,256]{2,1,0:T(2,128)S(1)} %maximum_bitcast_fusion.1), channel_id=2, replica_groups=mesh['rep'=2,'z'=8,'y'=4,'x'=4,'core'=2] {'x','core'}, dimensions={0}, use_global_device_ids=true | all-gather | bytes 18432 | tf_op jit(solution)/shard_map/all_gather | solution.py:117
  125.0 4.4 %all_to_all.60 = bf16[2,128,2048]{2,1,0:T(8,128)(2,1)S(1)} all-to-all(bf16[2,128,2048]{2,1,0:T(8,128)(2,1)S(1)} %bitcast.81), channel_id=1, replica_groups=mesh['rep'=2,'z'=8,'y'=4,'x'=4,'core'=2] {'core'}, dimensions={0} | all-to-all | bytes 2097152 | tf_op jit(solution)/shard_map/all_to_all | solution.py:22
  130.5 3.5 %all-to-all-start.5 = ((bf16[4,32,2048]{2,1,0:T(8,128)(2,1)}), bf16[4,32,2048]{2,1,0:T(8,128)(2,1)S(1)}, u32[]{:S(2)}, u32[]{:S(2)}) async-start(bf16[4,32,2048]{2,1,0:T(8,128)(2,1)} %bitcast.14), calls=%async_computation.5 | async-start | bytes 1048576 | tf_op jit(solution)/shard_map/all_to_all | solution.py:22
  134.1 4.9 %collective-permute-start.7 = (bf16[4,64,1536]{2,1,0:T(8,128)(2,1)}, bf16[4,64,1536]{2,1,0:T(8,128)(2,1)S(1)}, u32[]{:S(2)}, u32[]{:S(2)}) collective-permute-start(bf16[4,64,1536]{2,1,0:T(8,128)(2,1)} %collective-permute-done.5), channel_id=1, source_target_pairs={{32,0},{64,32},{96,64},{128,96},{160,128},{192,160},{224,192},{256... | collective-permute-start | bytes 2359304 | tf_op jit(solution)/shard_map/ppermute | solution.py:31
  146.1 4.1 %all-to-all-start.6 = ((bf16[4,32,2048]{2,1,0:T(8,128)(2,1)}), bf16[4,32,2048]{2,1,0:T(8,128)(2,1)S(1)}, u32[]{:S(2)}, u32[]{:S(2)}) async-start(bf16[4,32,2048]{2,1,0:T(8,128)(2,1)} %broadcast_in_dim.90), calls=%async_computation.6 | async-start | bytes 1048576 | tf_op jit(solution)/shard_map/all_to_all | solution.py:22
  152.3 6.0 %all-to-all-done.6 = bf16[4,32,2048]{2,1,0:T(8,128)(2,1)S(1)} async-done(((bf16[4,32,2048]{2,1,0:T(8,128)(2,1)}), bf16[4,32,2048]{2,1,0:T(8,128)(2,1)S(1)}, u32[]{:S(2)}, u32[]{:S(2)}) %all-to-all-start.6) | async-done | bytes 524320 | tf_op jit(solution)/shard_map/all_to_all | solution.py:22
  159.4 5.9 %all-to-all-start.7 = ((bf16[2,128,2048]{2,1,0:T(8,128)(2,1)}), bf16[2,128,2048]{2,1,0:T(8,128)(2,1)S(1)}, u32[]{:S(2)}, u32[]{:S(2)}) async-start(bf16[2,128,2048]{2,1,0:T(8,128)(2,1)} %broadcast_in_dim.91), calls=%async_computation.7 | async-start | bytes 2097152 | tf_op jit(solution)/shard_map/all_to_all | solution.py:22
  167.3 4.6 %collective-permute-start.9 = (bf16[2,64,1536]{2,1,0:T(8,128)(2,1)S(1)}, bf16[2,64,1536]{2,1,0:T(8,128)(2,1)S(1)}, u32[]{:S(2)}, u32[]{:S(2)}) collective-permute-start(bf16[2,64,1536]{2,1,0:T(8,128)(2,1)S(1)} %slice.66), channel_id=1, source_target_pairs={{32,0},{64,32},{96,64},{128,96},{160,128},{192,160},{224,192},{256... | collective-permute-start | bytes 1179656 | tf_op jit(solution)/shard_map/ppermute | solution.py:31
  173.8 5.4 %collective-permute-done.10 = bf16[2,64,1536]{2,1,0:T(8,128)(2,1)S(1)} collective-permute-done((bf16[2,64,1536]{2,1,0:T(8,128)(2,1)S(1)}, bf16[2,64,1536]{2,1,0:T(8,128)(2,1)S(1)}, u32[]{:S(2)}, u32[]{:S(2)}) %collective-permute-start.10) | collective-permute-done | bytes 393248 | tf_op jit(solution)/shard_map/ppermute | solution.py:31
  181.0 3.4 %fusion.17 = bf16[256,1024]{1,0:T(8,128)(2,1)S(1)} fusion(bf16[256,2048]{1,0:T(8,128)(2,1)S(1)} %bitcast.89, bf16[2048,1536]{1,0:T(8,128)(2,1)} %bitcast.30, f32[1024]{0:T(1024)S(1)} %convert_convert_fusion), kind=kOutput, calls=%fused_computation.15 | convolution fusion | flops 1074790400 | bytes 5771264 | tf_op jit(solution)/shard_map/dot_general | solution.py:176
  189.7 5.3 %all_to_all.61 = bf16[2,128,2048]{2,1,0:T(8,128)(2,1)S(1)} all-to-all(bf16[2,128,2048]{2,1,0:T(8,128)(2,1)S(1)} %bitcast.83), channel_id=1, replica_groups=mesh['rep'=2,'z'=8,'y'=4,'x'=4,'core'=2] {'core'}, dimensions={0} | all-to-all | bytes 2097152 | tf_op jit(solution)/shard_map/all_to_all | solution.py:22
  195.4 11.6 %all_to_all.62 = bf16[4,32,2048]{2,1,0:T(8,128)(2,1)S(1)} all-to-all(bf16[4,32,2048]{2,1,0:T(8,128)(2,1)S(1)} %bitcast.88), channel_id=1, replica_groups=mesh['rep'=2,'z'=8,'y'=4,'x'=4,'core'=2] {'x'}, dimensions={0} | all-to-all | bytes 1048576 | tf_op jit(solution)/shard_map/all_to_all | solution.py:22
  207.1 10.7 %all_to_all.63 = bf16[4,32,2048]{2,1,0:T(8,128)(2,1)S(1)} all-to-all(bf16[4,32,2048]{2,1,0:T(8,128)(2,1)S(1)} %broadcast_in_dim.106), channel_id=1, replica_groups=mesh['rep'=2,'z'=8,'y'=4,'x'=4,'core'=2] {'x'}, dimensions={0} | all-to-all | bytes 1048576 | tf_op jit(solution)/shard_map/all_to_all | solution.py:22
  218.0 6.3 %all_to_all.64 = bf16[2,128,2048]{2,1,0:T(8,128)(2,1)S(1)} all-to-all(bf16[2,128,2048]{2,1,0:T(8,128)(2,1)S(1)} %broadcast_in_dim.107), channel_id=1, replica_groups=mesh['rep'=2,'z'=8,'y'=4,'x'=4,'core'=2] {'core'}, dimensions={0} | all-to-all | bytes 2097152 | tf_op jit(solution)/shard_map/all_to_all | solution.py:22
  (114 shorter events, 53.7 us)
Async XLA Ops:
  6.5 94.4 %copy-start = (f32[31,128]{1,0:T(8,128)S(1)}, f32[31,128]{1,0:T(8,128)}, u32[]{:S(2)}) copy-start(f32[31,128]{1,0:T(8,128)} %param.21) | copy-start | bytes 47620
  6.5 56.9 %copy-start.6 = (f32[128]{0:T(128)S(1)}, f32[128]{0:T(128)}, u32[]{:S(2)}) copy-start(f32[128]{0:T(128)} %param.19) | copy-start | bytes 1540
  6.5 56.9 %copy-start.5 = (f32[128]{0:T(128)S(1)}, f32[128]{0:T(128)}, u32[]{:S(2)}) copy-start(f32[128]{0:T(128)} %param.20) | copy-start | bytes 1540
  6.5 57.1 %copy-start.3 = (f32[1024]{0:T(1024)S(1)}, f32[1024]{0:T(1024)}, u32[]{:S(2)}) copy-start(f32[1024]{0:T(1024)} %param.27) | copy-start | bytes 12292
  9.3 30.4 %collective-permute-start = (bf16[64,1536]{1,0:T(8,128)(2,1)S(1)}, bf16[64,1536]{1,0:T(8,128)(2,1)S(1)}, u32[]{:S(2)}, u32[]{:S(2)}) collective-permute-start(bf16[64,1536]{1,0:T(8,128)(2,1)S(1)} %pad_maximum_fusion), channel_id=1, source_target_pairs={{16,0},{24,8},{0,16},{8,24},{17,1},{25,9},{1,17},{9,25},{18,2},{26... | collective-permute-start | bytes 589832 | tf_op jit(solution)/shard_map/ppermute | solution.py:40
  14.9 24.7 %collective-permute-start.1 = (bf16[64,1536]{1,0:T(8,128)(2,1)S(1)}, bf16[64,1536]{1,0:T(8,128)(2,1)S(1)}, u32[]{:S(2)}, u32[]{:S(2)}) collective-permute-start(bf16[64,1536]{1,0:T(8,128)(2,1)S(1)} %pad_maximum_fusion), channel_id=1, source_target_pairs={{8,0},{16,8},{24,16},{0,24},{9,1},{17,9},{25,17},{1,25},{10,2},{18... | collective-permute-start | bytes 589832 | tf_op jit(solution)/shard_map/ppermute | solution.py:40
  17.6 31.8 %collective-permute-start.2 = (bf16[64,1536]{1,0:T(8,128)(2,1)S(1)}, bf16[64,1536]{1,0:T(8,128)(2,1)S(1)}, u32[]{:S(2)}, u32[]{:S(2)}) collective-permute-start(bf16[64,1536]{1,0:T(8,128)(2,1)S(1)} %pad_maximum_fusion), channel_id=1, source_target_pairs={{24,0},{0,8},{8,16},{16,24},{25,1},{1,9},{9,17},{17,25},{26,2},{2,... | collective-permute-start | bytes 589832 | tf_op jit(solution)/shard_map/ppermute | solution.py:40
  22.4 22.6 %all-to-all-start.2 = ((bf16[8,64,128]{2,1,0:T(8,128)(2,1)}), bf16[8,64,128]{2,1,0:T(8,128)(2,1)S(1)}, u32[]{:S(2)}, u32[]{:S(2)}) async-start(bf16[8,64,128]{2,1,0:T(8,128)(2,1)} %broadcast_in_dim.88), calls=%async_computation.2 | async-start | bytes 262144 | tf_op jit(solution)/shard_map/all_to_all | solution.py:22
  34.7 108.3 %all-gather.7.cloned.1.call-start = ((), (), s32[]{:S(2)}) async-start(), calls=%async_computation.12 | async-start | bytes 1114112 | tf_op jit(solution)/shard_map/all_gather | solution.py:159
  45.9 10.4 %all-to-all-start.3 = ((bf16[4,8,64,128]{3,2,1,0:T(8,128)(2,1)}), bf16[4,8,64,128]{3,2,1,0:T(8,128)(2,1)S(1)}, u32[]{:S(2)}, u32[]{:S(2)}) async-start(bf16[4,8,64,128]{3,2,1,0:T(8,128)(2,1)} %broadcast_in_dim.89), calls=%async_computation.3 | async-start | bytes 1048576 | tf_op jit(solution)/shard_map/all_to_all | solution.py:22
  49.5 35.7 %collective-permute-start.3 = (bf16[4,64,1536]{2,1,0:T(8,128)(2,1)S(1)}, bf16[4,64,1536]{2,1,0:T(8,128)(2,1)}, u32[]{:S(2)}, u32[]{:S(2)}) collective-permute-start(bf16[4,64,1536]{2,1,0:T(8,128)(2,1)S(1)} %bitcast_dynamic-update-slice_fusion.7), channel_id=1, source_target_pairs={{32,0},{64,32},{96,64},{128,96},{160,128},{192,160},{224,192},{256... | collective-permute-start | bytes 2359304 | tf_op jit(solution)/shard_map/ppermute | solution.py:31
  53.7 40.5 %collective-permute-start.4 = (bf16[4,64,1536]{2,1,0:T(8,128)(2,1)S(1)}, bf16[4,64,1536]{2,1,0:T(8,128)(2,1)}, u32[]{:S(2)}, u32[]{:S(2)}) collective-permute-start(bf16[4,64,1536]{2,1,0:T(8,128)(2,1)S(1)} %bitcast_dynamic-update-slice_fusion.7), channel_id=1, source_target_pairs={{480,0},{0,32},{32,64},{64,96},{96,128},{128,160},{160,192},{192,2... | collective-permute-start | bytes 2359304 | tf_op jit(solution)/shard_map/ppermute | solution.py:31
  57.0 22.8 %all-to-all-start = ((bf16[8,64,256]{2,1,0:T(8,128)(2,1)}), bf16[8,64,256]{2,1,0:T(8,128)(2,1)S(1)}, u32[]{:S(2)}, u32[]{:S(2)}) async-start(bf16[8,64,256]{2,1,0:T(8,128)(2,1)} %broadcast_in_dim.85), calls=%async_computation | async-start | bytes 524288 | tf_op jit(solution)/shard_map/all_to_all | solution.py:22
  80.9 19.4 %all-to-all-start.1 = ((bf16[4,8,64,256]{3,2,1,0:T(8,128)(2,1)}), bf16[4,8,64,256]{3,2,1,0:T(8,128)(2,1)S(1)}, u32[]{:S(2)}, u32[]{:S(2)}) async-start(bf16[4,8,64,256]{3,2,1,0:T(8,128)(2,1)} %broadcast_in_dim.86), calls=%async_computation.1 | async-start | bytes 2097152 | tf_op jit(solution)/shard_map/all_to_all | solution.py:22
  85.2 48.8 %collective-permute-start.5 = (bf16[4,64,1536]{2,1,0:T(8,128)(2,1)}, bf16[4,64,1536]{2,1,0:T(8,128)(2,1)}, u32[]{:S(2)}, u32[]{:S(2)}) collective-permute-start(bf16[4,64,1536]{2,1,0:T(8,128)(2,1)} %collective-permute-done.3), channel_id=1, source_target_pairs={{32,0},{64,32},{96,64},{128,96},{160,128},{192,160},{224,192},{256... | collective-permute-start | bytes 2359304 | tf_op jit(solution)/shard_map/ppermute | solution.py:31
  94.2 44.8 %collective-permute-start.6 = (bf16[4,64,1536]{2,1,0:T(8,128)(2,1)}, bf16[4,64,1536]{2,1,0:T(8,128)(2,1)}, u32[]{:S(2)}, u32[]{:S(2)}) collective-permute-start(bf16[4,64,1536]{2,1,0:T(8,128)(2,1)} %collective-permute-done.4), channel_id=1, source_target_pairs={{480,0},{0,32},{32,64},{64,96},{96,128},{128,160},{160,192},{192,2... | collective-permute-start | bytes 2359304 | tf_op jit(solution)/shard_map/ppermute | solution.py:31
  130.5 14.3 %all-to-all-start.5 = ((bf16[4,32,2048]{2,1,0:T(8,128)(2,1)}), bf16[4,32,2048]{2,1,0:T(8,128)(2,1)S(1)}, u32[]{:S(2)}, u32[]{:S(2)}) async-start(bf16[4,32,2048]{2,1,0:T(8,128)(2,1)} %bitcast.14), calls=%async_computation.5 | async-start | bytes 1048576 | tf_op jit(solution)/shard_map/all_to_all | solution.py:22
  134.0 50.5 %all-gather.9.cloned.1.call-start = ((), (), s32[]{:S(2)}) async-start(), calls=%async_computation.13 | async-start | bytes 2621440 | tf_op jit(solution)/shard_map/all_gather | solution.py:160
  134.1 33.2 %collective-permute-start.7 = (bf16[4,64,1536]{2,1,0:T(8,128)(2,1)}, bf16[4,64,1536]{2,1,0:T(8,128)(2,1)S(1)}, u32[]{:S(2)}, u32[]{:S(2)}) collective-permute-start(bf16[4,64,1536]{2,1,0:T(8,128)(2,1)} %collective-permute-done.5), channel_id=1, source_target_pairs={{32,0},{64,32},{96,64},{128,96},{160,128},{192,160},{224,192},{256... | collective-permute-start | bytes 2359304 | tf_op jit(solution)/shard_map/ppermute | solution.py:31
  138.9 26.4 %collective-permute-start.8 = (bf16[4,64,1536]{2,1,0:T(8,128)(2,1)}, bf16[4,64,1536]{2,1,0:T(8,128)(2,1)S(1)}, u32[]{:S(2)}, u32[]{:S(2)}) collective-permute-start(bf16[4,64,1536]{2,1,0:T(8,128)(2,1)} %collective-permute-done.6), channel_id=1, source_target_pairs={{480,0},{0,32},{32,64},{64,96},{96,128},{128,160},{160,192},{192,2... | collective-permute-start | bytes 2359304 | tf_op jit(solution)/shard_map/ppermute | solution.py:31
  146.1 12.2 %all-to-all-start.6 = ((bf16[4,32,2048]{2,1,0:T(8,128)(2,1)}), bf16[4,32,2048]{2,1,0:T(8,128)(2,1)S(1)}, u32[]{:S(2)}, u32[]{:S(2)}) async-start(bf16[4,32,2048]{2,1,0:T(8,128)(2,1)} %broadcast_in_dim.90), calls=%async_computation.6 | async-start | bytes 1048576 | tf_op jit(solution)/shard_map/all_to_all | solution.py:22
  159.4 21.7 %all-to-all-start.7 = ((bf16[2,128,2048]{2,1,0:T(8,128)(2,1)}), bf16[2,128,2048]{2,1,0:T(8,128)(2,1)S(1)}, u32[]{:S(2)}, u32[]{:S(2)}) async-start(bf16[2,128,2048]{2,1,0:T(8,128)(2,1)} %broadcast_in_dim.91), calls=%async_computation.7 | async-start | bytes 2097152 | tf_op jit(solution)/shard_map/all_to_all | solution.py:22
  165.3 13.9 %collective-permute-start.10 = (bf16[2,64,1536]{2,1,0:T(8,128)(2,1)S(1)}, bf16[2,64,1536]{2,1,0:T(8,128)(2,1)S(1)}, u32[]{:S(2)}, u32[]{:S(2)}) collective-permute-start(bf16[2,64,1536]{2,1,0:T(8,128)(2,1)S(1)} %slice.67), channel_id=1, source_target_pairs={{480,0},{0,32},{32,64},{64,96},{96,128},{128,160},{160,192},{192,2... | collective-permute-start | bytes 1179656 | tf_op jit(solution)/shard_map/ppermute | solution.py:31
  167.3 12.8 %collective-permute-start.9 = (bf16[2,64,1536]{2,1,0:T(8,128)(2,1)S(1)}, bf16[2,64,1536]{2,1,0:T(8,128)(2,1)S(1)}, u32[]{:S(2)}, u32[]{:S(2)}) collective-permute-start(bf16[2,64,1536]{2,1,0:T(8,128)(2,1)S(1)} %slice.66), channel_id=1, source_target_pairs={{32,0},{64,32},{96,64},{128,96},{160,128},{192,160},{224,192},{256... | collective-permute-start | bytes 1179656 | tf_op jit(solution)/shard_map/ppermute | solution.py:31
  (4 other events, 154.5 us)
Sparse Core Ops, SparseCore 0:
  37.5 66.4 all-gather.6
  145.0 34.2 all-gather.8

commit v3 on v2

--- a/solution.py
+++ b/solution.py
@@ -33,31 +33,42 @@
 
 def y_ring(block):
     n = lax.axis_size("y")
-    at = lax.axis_index("y")
-    whole = jnp.zeros((n, *block.shape), block.dtype)
-    whole = lax.dynamic_update_index_in_dim(whole, block, at, 0)
+    others = {}
     for d in (2, 1, 3):
-        other = lax.ppermute(block, "y", [((i + d) % n, i) for i in range(n)])
-        whole = lax.dynamic_update_index_in_dim(whole, other, (at + d) % n, 0)
-    return whole
+        others[d] = lax.ppermute(block, "y", [((i + d) % n, i) for i in range(n)])
+    return jnp.stack([block, others[1], others[2], others[3]])
 
 
 def ring_window(block):
     n = lax.axis_size("z")
-    at = lax.axis_index("z")
     cut = block.shape[0] // 2
-    whole = jnp.zeros((n, *block.shape), block.dtype)
-    whole = lax.dynamic_update_index_in_dim(whole, block, at, 0)
+    pieces = {0: block}
     ahead = behind = block
     for d in range(1, n // 2):
         ahead = shifted(ahead, 1)
         behind = shifted(behind, -1)
-        whole = lax.dynamic_update_index_in_dim(whole, ahead, (at + d) % n, 0)
-        whole = lax.dynamic_update_index_in_dim(whole, behind, (at - d) % n, 0)
+        pieces[d], pieces[n - d] = ahead, behind
     ahead = shifted(ahead[:cut], 1)
     behind = shifted(behind[cut:], -1)
-    last = jnp.concatenate([ahead, behind])
-    return lax.dynamic_update_index_in_dim(whole, last, (at + n // 2) % n, 0)
+    pieces[n // 2] = jnp.concatenate([ahead, behind])
+    return [pieces[d] for d in range(n)]
+
+
+def rolled(x, shift, axis):
+    return lax.dynamic_slice_in_dim(jnp.concatenate([x, x], axis=axis), shift, x.shape[axis], axis)
+
+
+def to_relative(x):
+    zs, ys = lax.axis_size("z"), lax.axis_size("y")
+    x = rolled(x, lax.axis_index("z") * (x.shape[1] // zs), 1).reshape(x.shape[0], zs, -1)
+    return rolled(x, lax.axis_index("y") * (x.shape[2] // ys), 2).reshape(x.shape[0], -1)
+
+
+def from_relative(x):
+    zs, ys = lax.axis_size("z"), lax.axis_size("y")
+    x = x.reshape(x.shape[0], zs, -1)
+    x = rolled(x, (ys - lax.axis_index("y")) % ys * (x.shape[2] // ys), 2).reshape(x.shape[0], -1)
+    return rolled(x, (zs - lax.axis_index("z")) % zs * (x.shape[1] // zs), 1)
 
 
 def fs_copies(x):
@@ -143,43 +154,33 @@
     down_weight,
     down_scale,
 ):
-    rep = lax.axis_index("rep")
-    reps = lax.axis_size("rep")
     width = value_weight.shape[1]
+    hid = up_weight.shape[1]
     mix_t = (mixout_weight.astype(BF16).astype(F32) * rounded(mixout_scale)).astype(BF16).T
     down_t = (down_weight.astype(BF16).astype(F32) * rounded(down_scale)).astype(BF16).T
-    glu_local = jnp.concatenate([value_weight.astype(BF16), gate_weight.astype(BF16)], axis=1)
-    glu_whole = fs_copies(glu_local)
-    mix_whole = fs_copies(mix_t)
-
-    hid = up_weight.shape[1]
-    early = hid // 2
-    half = (hid - early) // reps
-    late = lax.dynamic_slice_in_dim(down_t, early + rep * half, half, 1)
-    late = lax.all_gather(jnp.pad(late, ((0, 0), (0, (-half) % 512))), RING, axis=0)[:, :, :half]
-    late = lax.all_gather(late, "y")
-    near = jnp.concatenate([up_weight.astype(BF16), down_t[:, :early]], axis=1)
-    near = ring_window(y_ring(near)).reshape(-1, hid + early)
-    zs = lax.axis_size("z")
-    late = [late[:, r * zs : (r + 1) * zs].swapaxes(0, 1).reshape(-1, half) for r in range(reps)]
+    conv_local = jnp.concatenate([value_weight.astype(BF16), gate_weight.astype(BF16), mix_t], axis=1)
+    conv_whole = fs_copies(conv_local)
+    pieces = ring_window(y_ring(jnp.concatenate([up_weight.astype(BF16), down_t], axis=1)))
+    pieces = [p.reshape(-1, 2 * hid) for p in pieces]
 
     normed = rms_rows(tokens, first_gain)
-    sums = jnp.dot(normed, glu_whole, preferred_element_type=F32)
+    sums = jnp.dot(normed, conv_whole[:, : 2 * width], preferred_element_type=F32)
     glu = sums[:, :width] * rounded(value_scale) * jax.nn.sigmoid(sums[:, width:] * rounded(gate_scale))
     conv = causal_conv(glu, conv_taps)
     mean, var = channel_stats(conv)
     mixed_in = jax.nn.silu((conv - mean[:, None]) * lax.rsqrt(var[:, None] + 1e-05) * chan_gain).astype(BF16)
-    mix_sum = tp_scattered(dot_t(mixed_in, mix_whole))
+    mix_sum = tp_scattered(dot_t(mixed_in, conv_whole[:, 2 * width :]))
     middle = (own_rows(tokens).astype(F32) + mix_sum).astype(BF16)
-    normed2 = tp_gathered(rms_rows(middle, second_gain))
-
-    up_sum = jnp.dot(normed2, near[:, :hid], preferred_element_type=F32)
+    normed2 = tp_gathered(to_relative(rms_rows(middle, second_gain)))
+
+    rows = pieces[0].shape[0]
+    up_sum = 0.0
+    for d in (0, 1, 7, 2, 6, 3, 5, 4):
+        part = normed2[:, d * rows : (d + 1) * rows]
+        up_sum = up_sum + jnp.dot(part, pieces[d][:, :hid], preferred_element_type=F32)
     hidden = jnp.square(jax.nn.relu(up_sum * rounded(up_scale))).astype(BF16)
-    down_sum = dot_t(hidden[:, :early], near[:, hid:])
-    for r in range(reps):
-        at = early + r * half
-        down_sum = down_sum + dot_t(hidden[:, at : at + half], late[r])
-    layer_out = (middle.astype(F32) + tp_scattered(down_sum)).astype(BF16)
+    down_sum = jnp.concatenate([dot_t(hidden, p[:, hid:]).astype(BF16) for p in pieces], axis=1)
+    layer_out = (middle.astype(F32) + from_relative(tp_scattered(down_sum))).astype(BF16)
     return tp_gathered(layer_out)
 
 

time: 234 us -> 230 us (0.983)
  waiting for transfers between devices: 30.2 us -> 68.8 us
  local copies, waits for them, and re-layouts: 25.8 us -> 6.04 us
  between operations: 14.1 us -> 0.63 us
  blocking collectives: 60.7 us -> 48.7 us
  matrix products: 8.24 us -> 18.4 us
  starting transfers between devices: 81.2 us -> 76.6 us
    ppermute x8, waiting for transfers between devices: 6.3 us -> 27.2 us  [shifted(): return lax.ppermute(x, RING, [((i + distance) % n, i) for i in range(n)])]
    ppermute x3, waiting for transfers between devices: 0.01 us -> 13.5 us  [y_ring(): others[d] = lax.ppermute(block, 'y', [((i + d) % n, i) for i in range(n)])]
    dynamic_update_slice x10 -> x0, local copies, waits for them, and re-layouts: 11.2 us -> none  [the longest x3 5.11 us: ring_window(): whole = lax.dynamic_update_index_in_dim(whole, ahead, (at + d) % n, 0)]
    all_to_all x7 -> x5, starting transfers between devices: 40 us -> 28.9 us  [exchange(): return lax.all_to_all(x, axis, split_axis=0, concat_axis=0, tiled=True)]
    all_gather x1, blocking collectives: 22.3 us -> 13 us  [channel_stats(): both = lax.all_gather(jnp.stack([total, spread]), TP)]
    ppermute x8, starting transfers between devices: 30.3 us -> 38 us  [shifted(): return lax.ppermute(x, RING, [((i + distance) % n, i) for i in range(n)])]
    dot_general x2 -> x9, matrix products: 3.92 us -> 9.52 us  [the longest x8 7.78 us: on_device(): jnp.dot(part, pieces[d][:, :hid], preferred_element_type=F32)]
    dot_general x4 -> x9, matrix products: 3.76 us -> 8.36 us  [dot_t(): lax.dot_general(a, b, (((1,), (1,)), ((), ())), preferred_element_type=F32)]
  transfers between devices with their start and end apart: 20 -> 16, of which waited for: 6 -> 10; matrix products, arithmetic and copies ran while one was open for 16% -> 7% of each run, Pallas kernels for 0% -> 0%
where the time goes in v3:
time: 230 us; the launch traced here: 229 us
  starting transfers between devices  76.6 us (33%)
  waiting for transfers between devices  68.8 us (30%)
  blocking collectives  48.7 us (21%)
  matrix products  18.4 us (8%)
  other arithmetic  9.52 us (4%)
  local copies, waits for them, and re-layouts  6.04 us (3%)
    ppermute x8, starting transfers between devices, shifted(): return lax.ppermute(x, RING, [((i + distance) % n, i) for i in range(n)])  38 us
    all_to_all x5, blocking collectives, exchange(): return lax.all_to_all(x, axis, split_axis=0, concat_axis=0, tiled=True)  35.7 us
    all_to_all x5, starting transfers between devices, exchange(): return lax.all_to_all(x, axis, split_axis=0, concat_axis=0, tiled=True)  28.9 us
    all_to_all x5, waiting for transfers between devices, exchange(): return lax.all_to_all(x, axis, split_axis=0, concat_axis=0, tiled=True)  28.1 us
    ppermute x8, waiting for transfers between devices, shifted(): return lax.ppermute(x, RING, [((i + distance) % n, i) for i in range(n)])  27.2 us
    ppermute x3, waiting for transfers between devices, y_ring(): others[d] = lax.ppermute(block, 'y', [((i + d) % n, i) for i in range(n)])  13.5 us
    all_gather x1, blocking collectives, channel_stats(): both = lax.all_gather(jnp.stack([total, spread]), TP)  13 us
    ppermute x3, starting transfers between devices, y_ring(): others[d] = lax.ppermute(block, 'y', [((i + d) % n, i) for i in range(n)])  9.68 us
  transfers between devices with their start and end apart: 16, of which 10 were waited for; matrix products, arithmetic and copies ran while one was open for 7% of the time, Pallas kernels for 0%

profile of v3, /device:TPU:1, one launch (start us, length us, event | category | flops | bytes accessed | tf_op | source)
XLA Modules:
  0.0 228.7 jit_solution(8743361787814942318)
XLA Ops:
  3.8 13.1 %all-to-all-start = ((bf16[8,64,384]{2,1,0:T(8,128)(2,1)}), bf16[8,64,384]{2,1,0:T(8,128)(2,1)S(1)}, u32[]{:S(2)}, u32[]{:S(2)}) async-start(bf16[8,64,384]{2,1,0:T(8,128)(2,1)} %broadcast_in_dim.14), calls=%async_computation | async-start | bytes 786432 | tf_op jit(solution)/shard_map/all_to_all | solution.py:22
  17.5 16.8 %all-to-all-done = bf16[8,64,384]{2,1,0:T(8,128)(2,1)S(1)} async-done(((bf16[8,64,384]{2,1,0:T(8,128)(2,1)}), bf16[8,64,384]{2,1,0:T(8,128)(2,1)S(1)}, u32[]{:S(2)}, u32[]{:S(2)}) %all-to-all-start) | async-done | bytes 393248 | tf_op jit(solution)/shard_map/all_to_all | solution.py:22
  35.7 4.3 %all-to-all-start.1 = ((bf16[4,8,64,384]{3,2,1,0:T(8,128)(2,1)}), bf16[4,8,64,384]{3,2,1,0:T(8,128)(2,1)S(1)}, u32[]{:S(2)}, u32[]{:S(2)}) async-start(bf16[4,8,64,384]{3,2,1,0:T(8,128)(2,1)} %broadcast_in_dim.15), calls=%async_computation.1 | async-start | bytes 3145728 | tf_op jit(solution)/shard_map/all_to_all | solution.py:22
  40.3 4.7 %collective-permute-start = (bf16[64,2048]{1,0:T(8,128)(2,1)S(1)}, bf16[64,2048]{1,0:T(8,128)(2,1)S(1)}, u32[]{:S(2)}, u32[]{:S(2)}) collective-permute-start(bf16[64,2048]{1,0:T(8,128)(2,1)S(1)} %get-tuple-element.10), channel_id=1, source_target_pairs={{8,0},{16,8},{24,16},{0,24},{9,1},{17,9},{25,17},{1,25},{10,2},{18... | collective-permute-start | bytes 786440 | tf_op jit(solution)/shard_map/ppermute | solution.py:38
  47.5 2.5 %collective-permute-start.2 = (bf16[64,2048]{1,0:T(8,128)(2,1)S(1)}, bf16[64,2048]{1,0:T(8,128)(2,1)S(1)}, u32[]{:S(2)}, u32[]{:S(2)}) collective-permute-start(bf16[64,2048]{1,0:T(8,128)(2,1)S(1)} %get-tuple-element.10), channel_id=1, source_target_pairs={{24,0},{0,8},{8,16},{16,24},{25,1},{1,9},{9,17},{17,25},{26,2},{2,... | collective-permute-start | bytes 786440 | tf_op jit(solution)/shard_map/ppermute | solution.py:38
  50.3 7.9 %collective-permute-done = bf16[64,2048]{1,0:T(8,128)(2,1)S(1)} collective-permute-done((bf16[64,2048]{1,0:T(8,128)(2,1)S(1)}, bf16[64,2048]{1,0:T(8,128)(2,1)S(1)}, u32[]{:S(2)}, u32[]{:S(2)}) %collective-permute-start) | collective-permute-done | bytes 262176 | tf_op jit(solution)/shard_map/ppermute | solution.py:38
  59.3 4.5 %collective-permute-done.2 = bf16[64,2048]{1,0:T(8,128)(2,1)S(1)} collective-permute-done((bf16[64,2048]{1,0:T(8,128)(2,1)S(1)}, bf16[64,2048]{1,0:T(8,128)(2,1)S(1)}, u32[]{:S(2)}, u32[]{:S(2)}) %collective-permute-start.2) | collective-permute-done | bytes 262176 | tf_op jit(solution)/shard_map/ppermute | solution.py:38
  64.9 16.3 %collective-permute-start.3 = (bf16[4,64,2048]{2,1,0:T(8,128)(2,1)}, bf16[4,64,2048]{2,1,0:T(8,128)(2,1)}, u32[]{:S(2)}, u32[]{:S(2)}) collective-permute-start(bf16[4,64,2048]{2,1,0:T(8,128)(2,1)} %pad_maximum_fusion), channel_id=1, source_target_pairs={{32,0},{64,32},{96,64},{128,96},{160,128},{192,160},{224,192},{256... | collective-permute-start | bytes 3145736 | tf_op jit(solution)/shard_map/ppermute | solution.py:31
  86.4 13.0 %all-gather.1 = f32[8,2,256]{2,1,0:T(2,128)S(1)} all-gather(f32[1,2,256]{2,1,0:T(2,128)S(1)} %maximum_bitcast_fusion), channel_id=2, replica_groups=mesh['rep'=2,'z'=8,'y'=4,'x'=4,'core'=2] {'x','core'}, dimensions={0}, use_global_device_ids=true | all-gather | bytes 18432 | tf_op jit(solution)/shard_map/all_gather | solution.py:128
  100.1 4.4 %all_to_all.50 = bf16[2,128,2048]{2,1,0:T(8,128)(2,1)S(1)} all-to-all(bf16[2,128,2048]{2,1,0:T(8,128)(2,1)S(1)} %bitcast.70), channel_id=1, replica_groups=mesh['rep'=2,'z'=8,'y'=4,'x'=4,'core'=2] {'core'}, dimensions={0} | all-to-all | bytes 2097152 | tf_op jit(solution)/shard_map/all_to_all | solution.py:22
  105.6 3.6 %all-to-all-start.3 = ((bf16[4,32,2048]{2,1,0:T(8,128)(2,1)}), bf16[4,32,2048]{2,1,0:T(8,128)(2,1)S(1)}, u32[]{:S(2)}, u32[]{:S(2)}) async-start(bf16[4,32,2048]{2,1,0:T(8,128)(2,1)} %bitcast.11), calls=%async_computation.3 | async-start | bytes 1048576 | tf_op jit(solution)/shard_map/all_to_all | solution.py:22
  111.1 4.8 %collective-permute-start.5 = (bf16[4,64,2048]{2,1,0:T(8,128)(2,1)}, bf16[4,64,2048]{2,1,0:T(8,128)(2,1)}, u32[]{:S(2)}, u32[]{:S(2)}) collective-permute-start(bf16[4,64,2048]{2,1,0:T(8,128)(2,1)} %collective-permute-done.3), channel_id=1, source_target_pairs={{32,0},{64,32},{96,64},{128,96},{160,128},{192,160},{224,192},{256... | collective-permute-start | bytes 3145736 | tf_op jit(solution)/shard_map/ppermute | solution.py:31
  120.9 3.5 %all-to-all-start.4 = ((bf16[4,32,2048]{2,1,0:T(8,128)(2,1)}), bf16[4,32,2048]{2,1,0:T(8,128)(2,1)S(1)}, u32[]{:S(2)}, u32[]{:S(2)}) async-start(bf16[4,32,2048]{2,1,0:T(8,128)(2,1)} %broadcast_in_dim.17), calls=%async_computation.4 | async-start | bytes 1048576 | tf_op jit(solution)/shard_map/all_to_all | solution.py:22
  124.4 12.5 %collective-permute-done.6 = bf16[4,64,2048]{2,1,0:T(8,128)(2,1)} collective-permute-done((bf16[4,64,2048]{2,1,0:T(8,128)(2,1)}, bf16[4,64,2048]{2,1,0:T(8,128)(2,1)}, u32[]{:S(2)}, u32[]{:S(2)}) %collective-permute-start.6) | collective-permute-done | bytes 1048608 | tf_op jit(solution)/shard_map/ppermute | solution.py:31
  138.7 4.6 %collective-permute-start.7 = (bf16[4,64,2048]{2,1,0:T(8,128)(2,1)}, bf16[4,64,2048]{2,1,0:T(8,128)(2,1)S(1)}, u32[]{:S(2)}, u32[]{:S(2)}) collective-permute-start(bf16[4,64,2048]{2,1,0:T(8,128)(2,1)} %collective-permute-done.5), channel_id=1, source_target_pairs={{32,0},{64,32},{96,64},{128,96},{160,128},{192,160},{224,192},{256... | collective-permute-start | bytes 3145736 | tf_op jit(solution)/shard_map/ppermute | solution.py:31
  143.5 6.4 %all_to_all.51 = bf16[2,128,2048]{2,1,0:T(8,128)(2,1)S(1)} all-to-all(bf16[2,128,2048]{2,1,0:T(8,128)(2,1)S(1)} %broadcast_in_dim.18), channel_id=1, replica_groups=mesh['rep'=2,'z'=8,'y'=4,'x'=4,'core'=2] {'core'}, dimensions={0} | all-to-all | bytes 2097152 | tf_op jit(solution)/shard_map/all_to_all | solution.py:22
  155.3 7.9 %collective-permute-done.8 = bf16[4,64,2048]{2,1,0:T(8,128)(2,1)S(1)} collective-permute-done((bf16[4,64,2048]{2,1,0:T(8,128)(2,1)}, bf16[4,64,2048]{2,1,0:T(8,128)(2,1)S(1)}, u32[]{:S(2)}, u32[]{:S(2)}) %collective-permute-start.8) | collective-permute-done | bytes 1048608 | tf_op jit(solution)/shard_map/ppermute | solution.py:31
  165.2 4.6 %collective-permute-start.9 = (bf16[2,64,2048]{2,1,0:T(8,128)(2,1)S(1)}, bf16[2,64,2048]{2,1,0:T(8,128)(2,1)S(1)}, u32[]{:S(2)}, u32[]{:S(2)}) collective-permute-start(bf16[2,64,2048]{2,1,0:T(8,128)(2,1)S(1)} %slice.150), channel_id=1, source_target_pairs={{32,0},{64,32},{96,64},{128,96},{160,128},{192,160},{224,192},{256... | collective-permute-start | bytes 1572872 | tf_op jit(solution)/shard_map/ppermute | solution.py:31
  171.5 5.9 %collective-permute-done.10 = bf16[2,64,2048]{2,1,0:T(8,128)(2,1)S(1)} collective-permute-done((bf16[2,64,2048]{2,1,0:T(8,128)(2,1)S(1)}, bf16[2,64,2048]{2,1,0:T(8,128)(2,1)S(1)}, u32[]{:S(2)}, u32[]{:S(2)}) %collective-permute-start.10) | collective-permute-done | bytes 524320 | tf_op jit(solution)/shard_map/ppermute | solution.py:31
  187.2 7.8 %all_to_all.52 = bf16[2,128,2048]{1,2,0:T(8,128)(2,1)S(1)} all-to-all(bf16[2,128,2048]{1,2,0:T(8,128)(2,1)S(1)} %copy_bitcast_fusion), channel_id=1, replica_groups=mesh['rep'=2,'z'=8,'y'=4,'x'=4,'core'=2] {'core'}, dimensions={0} | all-to-all | bytes 2097152 | tf_op jit(solution)/shard_map/all_to_all | solution.py:22
  196.6 4.5 %all-to-all-start.7 = ((bf16[4,32,2048]{2,1,0:T(8,128)(2,1)}), bf16[4,32,2048]{2,1,0:T(8,128)(2,1)S(1)}, u32[]{:S(2)}, u32[]{:S(2)}) async-start(bf16[4,32,2048]{2,1,0:T(8,128)(2,1)} %bitcast.27), calls=%async_computation.7 | async-start | bytes 1048576 | tf_op jit(solution)/shard_map/all_to_all | solution.py:22
  201.0 8.9 %all-to-all-done.7 = bf16[4,32,2048]{2,1,0:T(8,128)(2,1)S(1)} async-done(((bf16[4,32,2048]{2,1,0:T(8,128)(2,1)}), bf16[4,32,2048]{2,1,0:T(8,128)(2,1)S(1)}, u32[]{:S(2)}, u32[]{:S(2)}) %all-to-all-start.7) | async-done | bytes 524320 | tf_op jit(solution)/shard_map/all_to_all | solution.py:22
  210.6 10.2 %all_to_all.53 = bf16[4,32,2048]{2,1,0:T(8,128)(2,1)S(1)} all-to-all(bf16[4,32,2048]{2,1,0:T(8,128)(2,1)S(1)} %broadcast_in_dim.19), channel_id=1, replica_groups=mesh['rep'=2,'z'=8,'y'=4,'x'=4,'core'=2] {'x'}, dimensions={0} | all-to-all | bytes 1048576 | tf_op jit(solution)/shard_map/all_to_all | solution.py:22
  220.9 6.8 %all_to_all.54 = bf16[2,128,2048]{2,1,0:T(8,128)(2,1)S(1)} all-to-all(bf16[2,128,2048]{2,1,0:T(8,128)(2,1)S(1)} %broadcast_in_dim.20), channel_id=1, replica_groups=mesh['rep'=2,'z'=8,'y'=4,'x'=4,'core'=2] {'core'}, dimensions={0} | all-to-all | bytes 2097152 | tf_op jit(solution)/shard_map/all_to_all | solution.py:22
  (107 shorter events, 48.6 us)
Async XLA Ops:
  0.0 85.2 %copy-start = (f32[31,128]{1,0:T(8,128)S(1)}, f32[31,128]{1,0:T(8,128)}, u32[]{:S(2)}) copy-start(f32[31,128]{1,0:T(8,128)} %param.21) | copy-start | bytes 47620
  3.8 30.5 %all-to-all-start = ((bf16[8,64,384]{2,1,0:T(8,128)(2,1)}), bf16[8,64,384]{2,1,0:T(8,128)(2,1)S(1)}, u32[]{:S(2)}, u32[]{:S(2)}) async-start(bf16[8,64,384]{2,1,0:T(8,128)(2,1)} %broadcast_in_dim.14), calls=%async_computation | async-start | bytes 786432 | tf_op jit(solution)/shard_map/all_to_all | solution.py:22
  35.7 47.5 %all-to-all-start.1 = ((bf16[4,8,64,384]{3,2,1,0:T(8,128)(2,1)}), bf16[4,8,64,384]{3,2,1,0:T(8,128)(2,1)S(1)}, u32[]{:S(2)}, u32[]{:S(2)}) async-start(bf16[4,8,64,384]{3,2,1,0:T(8,128)(2,1)} %broadcast_in_dim.15), calls=%async_computation.1 | async-start | bytes 3145728 | tf_op jit(solution)/shard_map/all_to_all | solution.py:22
  40.1 9.9 %copy-start.1 = (bf16[256,2048]{1,0:T(8,128)(2,1)S(1)}, bf16[256,2048]{1,0:T(8,128)(2,1)}, u32[]{:S(2)}) copy-start(bf16[256,2048]{1,0:T(8,128)(2,1)} %param.15) | copy-start | bytes 3145732
  40.1 10.2 %copy-start.7 = (f32[128]{0:T(128)S(1)}, f32[128]{0:T(128)}, u32[]{:S(2)}) copy-start(f32[128]{0:T(128)} %param.20) | copy-start | bytes 1540
  40.1 10.2 %copy-start.8 = (f32[128]{0:T(128)S(1)}, f32[128]{0:T(128)}, u32[]{:S(2)}) copy-start(f32[128]{0:T(128)} %param.19) | copy-start | bytes 1540
  40.3 17.9 %collective-permute-start = (bf16[64,2048]{1,0:T(8,128)(2,1)S(1)}, bf16[64,2048]{1,0:T(8,128)(2,1)S(1)}, u32[]{:S(2)}, u32[]{:S(2)}) collective-permute-start(bf16[64,2048]{1,0:T(8,128)(2,1)S(1)} %get-tuple-element.10), channel_id=1, source_target_pairs={{8,0},{16,8},{24,16},{0,24},{9,1},{17,9},{25,17},{1,25},{10,2},{18... | collective-permute-start | bytes 786440 | tf_op jit(solution)/shard_map/ppermute | solution.py:38
  45.0 14.3 %collective-permute-start.1 = (bf16[64,2048]{1,0:T(8,128)(2,1)S(1)}, bf16[64,2048]{1,0:T(8,128)(2,1)S(1)}, u32[]{:S(2)}, u32[]{:S(2)}) collective-permute-start(bf16[64,2048]{1,0:T(8,128)(2,1)S(1)} %get-tuple-element.10), channel_id=1, source_target_pairs={{16,0},{24,8},{0,16},{8,24},{17,1},{25,9},{1,17},{9,25},{18,2},{26... | collective-permute-start | bytes 786440 | tf_op jit(solution)/shard_map/ppermute | solution.py:38
  47.5 16.4 %collective-permute-start.2 = (bf16[64,2048]{1,0:T(8,128)(2,1)S(1)}, bf16[64,2048]{1,0:T(8,128)(2,1)S(1)}, u32[]{:S(2)}, u32[]{:S(2)}) collective-permute-start(bf16[64,2048]{1,0:T(8,128)(2,1)S(1)} %get-tuple-element.10), channel_id=1, source_target_pairs={{24,0},{0,8},{8,16},{16,24},{25,1},{1,9},{9,17},{17,25},{26,2},{2,... | collective-permute-start | bytes 786440 | tf_op jit(solution)/shard_map/ppermute | solution.py:38
  64.9 18.5 %copy-start.9 = (f32[2048]{0:T(1024)S(1)}, f32[2048]{0:T(1024)}, u32[]{:S(2)}) copy-start(f32[2048]{0:T(1024)} %param.16) | copy-start | bytes 24580
  64.9 46.2 %collective-permute-start.3 = (bf16[4,64,2048]{2,1,0:T(8,128)(2,1)}, bf16[4,64,2048]{2,1,0:T(8,128)(2,1)}, u32[]{:S(2)}, u32[]{:S(2)}) collective-permute-start(bf16[4,64,2048]{2,1,0:T(8,128)(2,1)} %pad_maximum_fusion), channel_id=1, source_target_pairs={{32,0},{64,32},{96,64},{128,96},{160,128},{192,160},{224,192},{256... | collective-permute-start | bytes 3145736 | tf_op jit(solution)/shard_map/ppermute | solution.py:31
  81.3 27.9 %collective-permute-start.4 = (bf16[4,64,2048]{2,1,0:T(8,128)(2,1)}, bf16[4,64,2048]{2,1,0:T(8,128)(2,1)}, u32[]{:S(2)}, u32[]{:S(2)}) collective-permute-start(bf16[4,64,2048]{2,1,0:T(8,128)(2,1)} %pad_maximum_fusion), channel_id=1, source_target_pairs={{480,0},{0,32},{32,64},{64,96},{96,128},{128,160},{160,192},{192,2... | collective-permute-start | bytes 3145736 | tf_op jit(solution)/shard_map/ppermute | solution.py:31
  85.2 14.3 %copy-start.6 = (f32[128]{0:T(128)S(1)}, f32[128]{0:T(128)}, u32[]{:S(2)}) copy-start(f32[128]{0:T(128)} %param.22) | copy-start | bytes 1540
  105.6 13.9 %copy-start.4 = (f32[2048]{0:T(1024)S(1)}, f32[2048]{0:T(1024)}, u32[]{:S(2)}) copy-start(f32[2048]{0:T(1024)} %param.25) | copy-start | bytes 24580
  105.6 12.8 %all-to-all-start.3 = ((bf16[4,32,2048]{2,1,0:T(8,128)(2,1)}), bf16[4,32,2048]{2,1,0:T(8,128)(2,1)S(1)}, u32[]{:S(2)}, u32[]{:S(2)}) async-start(bf16[4,32,2048]{2,1,0:T(8,128)(2,1)} %bitcast.11), calls=%async_computation.3 | async-start | bytes 1048576 | tf_op jit(solution)/shard_map/all_to_all | solution.py:22
  109.2 27.6 %collective-permute-start.6 = (bf16[4,64,2048]{2,1,0:T(8,128)(2,1)}, bf16[4,64,2048]{2,1,0:T(8,128)(2,1)}, u32[]{:S(2)}, u32[]{:S(2)}) collective-permute-start(bf16[4,64,2048]{2,1,0:T(8,128)(2,1)} %collective-permute-done.4), channel_id=1, source_target_pairs={{480,0},{0,32},{32,64},{64,96},{96,128},{128,160},{160,192},{192,2... | collective-permute-start | bytes 3145736 | tf_op jit(solution)/shard_map/ppermute | solution.py:31
  111.1 27.6 %collective-permute-start.5 = (bf16[4,64,2048]{2,1,0:T(8,128)(2,1)}, bf16[4,64,2048]{2,1,0:T(8,128)(2,1)}, u32[]{:S(2)}, u32[]{:S(2)}) collective-permute-start(bf16[4,64,2048]{2,1,0:T(8,128)(2,1)} %collective-permute-done.3), channel_id=1, source_target_pairs={{32,0},{64,32},{96,64},{128,96},{160,128},{192,160},{224,192},{256... | collective-permute-start | bytes 3145736 | tf_op jit(solution)/shard_map/ppermute | solution.py:31
  119.5 4.9 %copy-start.5 = (f32[1024]{0:T(1024)S(1)}, f32[1024]{0:T(1024)}, u32[]{:S(2)}) copy-start(f32[1024]{0:T(1024)} %param.27) | copy-start | bytes 12292
  120.9 22.5 %all-to-all-start.4 = ((bf16[4,32,2048]{2,1,0:T(8,128)(2,1)}), bf16[4,32,2048]{2,1,0:T(8,128)(2,1)S(1)}, u32[]{:S(2)}, u32[]{:S(2)}) async-start(bf16[4,32,2048]{2,1,0:T(8,128)(2,1)} %broadcast_in_dim.17), calls=%async_computation.4 | async-start | bytes 1048576 | tf_op jit(solution)/shard_map/all_to_all | solution.py:22
  136.8 26.4 %collective-permute-start.8 = (bf16[4,64,2048]{2,1,0:T(8,128)(2,1)}, bf16[4,64,2048]{2,1,0:T(8,128)(2,1)S(1)}, u32[]{:S(2)}, u32[]{:S(2)}) collective-permute-start(bf16[4,64,2048]{2,1,0:T(8,128)(2,1)} %collective-permute-done.6), channel_id=1, source_target_pairs={{480,0},{0,32},{32,64},{64,96},{96,128},{128,160},{160,192},{192,2... | collective-permute-start | bytes 3145736 | tf_op jit(solution)/shard_map/ppermute | solution.py:31
  138.7 26.4 %collective-permute-start.7 = (bf16[4,64,2048]{2,1,0:T(8,128)(2,1)}, bf16[4,64,2048]{2,1,0:T(8,128)(2,1)S(1)}, u32[]{:S(2)}, u32[]{:S(2)}) collective-permute-start(bf16[4,64,2048]{2,1,0:T(8,128)(2,1)} %collective-permute-done.5), channel_id=1, source_target_pairs={{32,0},{64,32},{96,64},{128,96},{160,128},{192,160},{224,192},{256... | collective-permute-start | bytes 3145736 | tf_op jit(solution)/shard_map/ppermute | solution.py:31
  163.2 14.1 %collective-permute-start.10 = (bf16[2,64,2048]{2,1,0:T(8,128)(2,1)S(1)}, bf16[2,64,2048]{2,1,0:T(8,128)(2,1)S(1)}, u32[]{:S(2)}, u32[]{:S(2)}) collective-permute-start(bf16[2,64,2048]{2,1,0:T(8,128)(2,1)S(1)} %slice.151), channel_id=1, source_target_pairs={{480,0},{0,32},{32,64},{64,96},{96,128},{128,160},{160,192},{192,2... | collective-permute-start | bytes 1572872 | tf_op jit(solution)/shard_map/ppermute | solution.py:31
  165.2 13.1 %collective-permute-start.9 = (bf16[2,64,2048]{2,1,0:T(8,128)(2,1)S(1)}, bf16[2,64,2048]{2,1,0:T(8,128)(2,1)S(1)}, u32[]{:S(2)}, u32[]{:S(2)}) collective-permute-start(bf16[2,64,2048]{2,1,0:T(8,128)(2,1)S(1)} %slice.150), channel_id=1, source_target_pairs={{32,0},{64,32},{96,64},{128,96},{160,128},{192,160},{224,192},{256... | collective-permute-start | bytes 1572872 | tf_op jit(solution)/shard_map/ppermute | solution.py:31
  196.6 13.4 %all-to-all-start.7 = ((bf16[4,32,2048]{2,1,0:T(8,128)(2,1)}), bf16[4,32,2048]{2,1,0:T(8,128)(2,1)S(1)}, u32[]{:S(2)}, u32[]{:S(2)}) async-start(bf16[4,32,2048]{2,1,0:T(8,128)(2,1)} %bitcast.27), calls=%async_computation.7 | async-start | bytes 1048576 | tf_op jit(solution)/shard_map/all_to_all | solution.py:22
  (2 other events, 8.8 us)

commit v4 on v3

--- a/solution.py
+++ b/solution.py
@@ -1,6 +1,8 @@
 import jax
 import jax.numpy as jnp
 from jax import lax
+from jax.experimental import pallas as pl
+from jax.experimental.pallas import tpu as pltpu
 from jax.sharding import Mesh
 from jax.sharding import PartitionSpec as P
 
@@ -26,32 +28,48 @@
     return exchange(jnp.broadcast_to(x, (lax.axis_size(axis), *x.shape)), axis)
 
 
-def shifted(x, distance):
-    n = lax.axis_size(RING)
-    return lax.ppermute(x, RING, [((i + distance) % n, i) for i in range(n)])
-
-
 def y_ring(block):
     n = lax.axis_size("y")
     others = {}
     for d in (2, 1, 3):
         others[d] = lax.ppermute(block, "y", [((i + d) % n, i) for i in range(n)])
-    return jnp.stack([block, others[1], others[2], others[3]])
-
-
-def ring_window(block):
-    n = lax.axis_size("z")
-    cut = block.shape[0] // 2
-    pieces = {0: block}
-    ahead = behind = block
-    for d in range(1, n // 2):
-        ahead = shifted(ahead, 1)
-        behind = shifted(behind, -1)
-        pieces[d], pieces[n - d] = ahead, behind
-    ahead = shifted(ahead[:cut], 1)
-    behind = shifted(behind[cut:], -1)
-    pieces[n // 2] = jnp.concatenate([ahead, behind])
-    return [pieces[d] for d in range(n)]
+    return [block, others[1], others[2], others[3]]
+
+
+def hop(x):
+    n = lax.axis_size(RING)
+    pairs = [((2 * ((i + 1) % n)), 2 * i) for i in range(n)] + [(2 * ((i - 1) % n) + 1, 2 * i + 1) for i in range(n)]
+    return lax.ppermute(x, (*RING, "core"), pairs)
+
+
+def side_ring(chunks):
+    core = lax.axis_index("core")
+    pieces = {}
+    for name, block in chunks.items():
+        pieces[name] = [jnp.stack([block, swapped(block)])]
+    for d in range(1, 5):
+        for got in pieces.values():
+            last = got[-1]
+            if d == 4:
+                last = lax.dynamic_slice_in_dim(last, core * (last.shape[1] // 2), last.shape[1] // 2, 1)
+            got.append(hop(last))
+    return [[p.reshape(2, -1, p.shape[-1]) for p in got] for got in pieces.values()]
+
+
+def to_sides(x):
+    w = x.shape[1] // 16
+    at = lambda a, b: x[:, a * w : b * w]
+    ahead = jnp.concatenate([at(0, 1), at(2, 9)], axis=1)
+    behind = jnp.concatenate([at(1, 2), at(14, 16), at(12, 14), at(10, 12), at(9, 10)], axis=1)
+    return ahead, behind
+
+
+def from_sides(ahead, behind):
+    w = ahead.shape[1] // 8
+    at = lambda a, b: behind[:, a * w : b * w]
+    return jnp.concatenate(
+        [ahead[:, :w], at(0, 1), ahead[:, w:], at(7, 8), at(5, 7), at(3, 5), at(1, 3)], axis=1
+    )
 
 
 def rolled(x, shift, axis):
@@ -77,20 +95,19 @@
     return by_y.swapaxes(0, 1).reshape(-1, x.shape[1])
 
 
-def summed(x, axis):
-    n = lax.axis_size(axis)
-    blocks = exchange(x.reshape(n, x.shape[0] // n, x.shape[1]), axis)
+def swapped(x):
+    return lax.ppermute(x, "core", [(0, 1), (1, 0)])
+
+
+def x_scattered(mine, theirs):
+    half = (mine + theirs.astype(F32)).astype(BF16)
+    n = lax.axis_size("x")
+    blocks = exchange(half.reshape(n, half.shape[0] // n, half.shape[1]), "x")
     return blocks.astype(F32).sum(axis=0)
 
 
-def tp_scattered(x):
-    part = summed(x.astype(BF16), "core").astype(BF16)
-    return summed(part, "x")
-
-
-def tp_gathered(rows):
-    part = copies_from(rows, "x").reshape(-1, rows.shape[1])
-    return copies_from(part, "core").reshape(-1, rows.shape[1])
+def x_gathered(rows):
+    return copies_from(rows, "x").reshape(-1, rows.shape[1])
 
 
 def own_rows(x):
@@ -125,7 +142,7 @@
     total = jnp.sum(conv, axis=1)
     centred = conv - (total / width)[:, None]
     spread = jnp.sum(centred * centred, axis=1)
-    both = lax.all_gather(jnp.stack([total, spread]), TP)
+    both = copies_from(jnp.stack([total, spread]), TP)
     n = both.shape[0]
     mean = both[:, 0].sum(axis=0) / (n * width)
     off = both[:, 0] / width - mean
@@ -135,6 +152,86 @@
 
 def dot_t(a, b):
     return lax.dot_general(a, b, (((1,), (1,)), ((), ())), preferred_element_type=F32)
+
+
+def fetch_side(slot, core, pieces, whole, sems):
+    half = pieces[0].shape[1] // 2
+    sources = [pieces[0].at[slot, pl.ds(core * half, half)]] + [p.at[slot] for p in pieces[1:]]
+    at, copies = 0, []
+    for i, source in enumerate(sources):
+        n = source.shape[0]
+        copies.append(pltpu.make_async_copy(source, whole.at[pl.ds(at, n)], sems.at[i]))
+        copies[-1].start()
+        at += n
+    return copies
+
+
+def up_body(slot, core_ref, own, theirs, *refs):
+    pieces, (out, x, w, x_sems, w_sems) = refs[:-5], refs[-5:]
+    core = core_ref[0]
+    n = own.shape[0]
+    copies = [
+        pltpu.make_async_copy(own, x.at[pl.ds(core * n, n)], x_sems.at[0]),
+        pltpu.make_async_copy(theirs, x.at[pl.ds((1 - core) * n, n)], x_sems.at[1]),
+    ]
+    for copy in copies:
+        copy.start()
+    for copy in copies + fetch_side(slot, core, pieces, w, w_sems):
+        copy.wait()
+    out[...] = jnp.dot(x[...], w[...], preferred_element_type=F32).astype(out.dtype)
+
+
+def down_body(slot, core_ref, hidden, acc, *refs):
+    pieces, (out, w, w_sems) = refs[:-3], refs[-3:]
+    for copy in fetch_side(slot, core_ref[0], pieces, w, w_sems):
+        copy.wait()
+    part = dot_t(hidden[...], w[...])
+    if slot == 0:
+        out[...] = part
+        return
+    part = (part + acc[...]).astype(out.dtype)
+    blocks, halves, n, _ = out.shape
+    for i in range(blocks):
+        for j in range(halves):
+            at = (j * blocks + i) * n
+            out[i, j] = part[at : at + n]
+
+
+def side_call(body, name, slot, core, operands, pieces, out_shape, scratch):
+    anywhere = pl.BlockSpec(memory_space=pl.ANY)
+    inside = pl.BlockSpec(memory_space=pltpu.VMEM)
+    here = anywhere if name == "up" else inside
+    cols = pieces[0].shape[2]
+    rows = 4 * pieces[0].shape[1]
+    return pl.pallas_call(
+        lambda *refs: body(slot, *refs),
+        in_specs=[pl.BlockSpec(memory_space=pltpu.SMEM)] + [here] * len(operands) + [anywhere] * len(pieces),
+        out_specs=inside,
+        out_shape=out_shape,
+        scratch_shapes=scratch + [pltpu.VMEM((rows, cols), BF16)]
+        + ([pltpu.SemaphoreType.DMA((2,))] if name == "up" else [])
+        + [pltpu.SemaphoreType.DMA((len(pieces),))],
+        cost_estimate=pl.CostEstimate(flops=512 * rows * cols, bytes_accessed=2 * rows * cols, transcendentals=0),
+    )(core.reshape(1), *operands, *pieces)
+
+
+def ffn(own, theirs, core, scale, ups, downs):
+    tokens, cols = 2 * own.shape[0], own.shape[1]
+    hid = scale.shape[0]
+    up = lambda slot, kind: side_call(
+        up_body, "up", slot, core, (own, theirs), ups,
+        jax.ShapeDtypeStruct((tokens, hid), kind), [pltpu.VMEM((tokens, cols), BF16)],
+    )
+    sent = swapped(up(1, BF16))
+    up_sum = up(0, F32) + sent.astype(F32)
+    hidden = jnp.square(jax.nn.relu(up_sum * scale)).astype(BF16)
+    other = swapped(hidden)
+    kept = side_call(
+        down_body, "down", 0, core, (hidden, hidden), downs, jax.ShapeDtypeStruct((tokens, cols), F32), []
+    )
+    n = lax.axis_size("x")
+    blocks = jax.ShapeDtypeStruct((n, 2, tokens // (2 * n), cols), BF16)
+    return side_call(down_body, "down", 1, core, (other, kept), downs, blocks, [])
 
 
 def on_device(
@@ -160,8 +257,9 @@
     down_t = (down_weight.astype(BF16).astype(F32) * rounded(down_scale)).astype(BF16).T
     conv_local = jnp.concatenate([value_weight.astype(BF16), gate_weight.astype(BF16), mix_t], axis=1)
     conv_whole = fs_copies(conv_local)
-    pieces = ring_window(y_ring(jnp.concatenate([up_weight.astype(BF16), down_t], axis=1)))
-    pieces = [p.reshape(-1, 2 * hid) for p in pieces]
+    near = y_ring(jnp.concatenate([up_weight.astype(BF16), down_t], axis=1))
+    chunks = {"up": jnp.stack([b[:, :hid] for b in near]), "down": jnp.stack([b[:, hid:] for b in near])}
+    ups, downs = side_ring(chunks)
 
     normed = rms_rows(tokens, first_gain)
     sums = jnp.dot(normed, conv_whole[:, : 2 * width], preferred_element_type=F32)
@@ -169,19 +267,28 @@
     conv = causal_conv(glu, conv_taps)
     mean, var = channel_stats(conv)
     mixed_in = jax.nn.silu((conv - mean[:, None]) * lax.rsqrt(var[:, None] + 1e-05) * chan_gain).astype(BF16)
-    mix_sum = tp_scattered(dot_t(mixed_in, conv_whole[:, 2 * width :]))
+    core = lax.axis_index("core")
+    half = mixed_in.shape[0] // 2
+    mix_whole = conv_whole[:, 2 * width :]
+    sent = dot_t(lax.dynamic_slice_in_dim(mixed_in, (1 - core) * half, half, 0), mix_whole).astype(BF16)
+    kept = dot_t(lax.dynamic_slice_in_dim(mixed_in, core * half, half, 0), mix_whole)
+    mix_sum = x_scattered(kept, swapped(sent))
     middle = (own_rows(tokens).astype(F32) + mix_sum).astype(BF16)
-    normed2 = tp_gathered(to_relative(rms_rows(middle, second_gain)))
-
-    rows = pieces[0].shape[0]
-    up_sum = 0.0
-    for d in (0, 1, 7, 2, 6, 3, 5, 4):
-        part = normed2[:, d * rows : (d + 1) * rows]
-        up_sum = up_sum + jnp.dot(part, pieces[d][:, :hid], preferred_element_type=F32)
-    hidden = jnp.square(jax.nn.relu(up_sum * rounded(up_scale))).astype(BF16)
-    down_sum = jnp.concatenate([dot_t(hidden, p[:, hid:]).astype(BF16) for p in pieces], axis=1)
-    layer_out = (middle.astype(F32) + from_relative(tp_scattered(down_sum))).astype(BF16)
-    return tp_gathered(layer_out)
+    sides = jnp.stack(to_sides(to_relative(rms_rows(middle, second_gain))))
+    sides = copies_from(sides, "x")
+    cols = sides.shape[-1]
+    side_of = lambda c: lax.dynamic_index_in_dim(sides, c, 1, keepdims=False).reshape(-1, cols)
+    theirs = swapped(side_of(1 - core))
+    blocks = ffn(side_of(core), theirs, core, rounded(up_scale), ups, downs)
+    blocks = exchange(blocks, "x").astype(F32).sum(axis=0)
+    kept = lax.dynamic_index_in_dim(blocks, core, 0, keepdims=False)
+    sent = lax.dynamic_index_in_dim(blocks, 1 - core, 0, keepdims=False).astype(BF16)
+    got = swapped(sent).astype(F32)
+    first = core == 0
+    down_sum = from_relative(from_sides(jnp.where(first, kept, got), jnp.where(first, got, kept)))
+    mine = x_gathered((middle.astype(F32) + down_sum).astype(BF16))
+    theirs = swapped(mine)
+    return jnp.concatenate([jnp.where(first, mine, theirs), jnp.where(first, theirs, mine)])
 
 
 def solution(mesh):
@@ -207,6 +314,4 @@
         P(FS),
     )
 
-    return jax.shard_map(
-        on_device, mesh=torus, in_specs=placed, out_specs=P(REP_FS, None), check_vma=False
-    )
+    return jax.shard_map(on_device, mesh=torus, in_specs=placed, out_specs=P(REP_FS, None), check_vma=False)

time: 230 us -> 223 us (0.970)
  starting transfers between devices: 76.6 us -> 103 us
  waiting for transfers between devices: 68.8 us -> 42.9 us
  blocking collectives: 48.7 us -> 25.4 us
  Pallas kernels: 0 us -> 15.5 us
  matrix products: 18.4 us -> 5.48 us
  other arithmetic: 9.52 us -> 19.9 us
  local copies, waits for them, and re-layouts: 6.04 us -> 8.83 us
    all_to_all x5, waiting for transfers between devices: 28.1 us -> 7.87 us  [exchange(): return lax.all_to_all(x, axis, split_axis=0, concat_axis=0, tiled=True)]
    ppermute x8 -> x16, starting transfers between devices: 38 us -> 54.9 us  [the longest x8 34.2 us: swapped(): return lax.ppermute(x, 'core', [(0, 1), (1, 0)])]
    pallas_call x0 -> x4, Pallas kernels: none -> 15.5 us  [side_call(): pl.pallas_call(lambda *refs: body(slot, *refs), in_specs=[pl.BlockSpec(me...]
    ppermute x3, waiting for transfers between devices: 13.5 us -> 0.01 us  [y_ring(): others[d] = lax.ppermute(block, 'y', [((i + d) % n, i) for i in range(n)])]
    all_gather x1 -> x0, blocking collectives: 13 us -> none  [channel_stats(): both = lax.all_gather(jnp.stack([total, spread]), TP)]
    all_to_all x5 -> x2, blocking collectives: 35.7 us -> 25.4 us  [exchange(): return lax.all_to_all(x, axis, split_axis=0, concat_axis=0, tiled=True)]
    another operation x2 -> x11, other arithmetic: 1.15 us -> 11.1 us  [the longest x6 11 us: side_ring(): pieces[name] = [jnp.stack([block, swapped(block)])]]
    all_to_all x5, starting transfers between devices: 28.9 us -> 38.1 us  [exchange(): return lax.all_to_all(x, axis, split_axis=0, concat_axis=0, tiled=True)]
  transfers between devices with their start and end apart: 16 -> 24, of which waited for: 10 -> 10; matrix products, arithmetic and copies ran while one was open for 7% -> 12% of each run, Pallas kernels for 0% -> 5%
where the time goes in v4:
time: 223 us; the launch traced here: 222 us
  starting transfers between devices  103 us (46%)
  waiting for transfers between devices  42.9 us (19%)
  blocking collectives  25.4 us (11%)
  other arithmetic  19.9 us (9%)
  Pallas kernels  15.5 us (7%)
  local copies, waits for them, and re-layouts  8.83 us (4%)
  matrix products  5.48 us (2%)
    all_to_all x5, starting transfers between devices, exchange(): return lax.all_to_all(x, axis, split_axis=0, concat_axis=0, tiled=True)  38.1 us
    ppermute x8, starting transfers between devices, swapped(): return lax.ppermute(x, 'core', [(0, 1), (1, 0)])  34.2 us
    ppermute x8, waiting for transfers between devices, hop(): return lax.ppermute(x, (*RING, 'core'), pairs)  32.7 us
    all_to_all x2, blocking collectives, exchange(): return lax.all_to_all(x, axis, split_axis=0, concat_axis=0, tiled=True)  25.4 us
    ppermute x8, starting transfers between devices, hop(): return lax.ppermute(x, (*RING, 'core'), pairs)  20.7 us
    pallas_call x4, Pallas kernels, side_call(): pl.pallas_call(lambda *refs: body(slot, *refs), in_specs=[pl.BlockSpec(me...  15.5 us
    another operation x6, other arithmetic, side_ring(): pieces[name] = [jnp.stack([block, swapped(block)])]  11 us
    ppermute x3, starting transfers between devices, y_ring(): others[d] = lax.ppermute(block, 'y', [((i + d) % n, i) for i in range(n)])  9.5 us
  transfers between devices with their start and end apart: 24, of which 10 were waited for; matrix products, arithmetic and copies ran while one was open for 12% of the time, Pallas kernels for 5%

profile of v4, /device:TPU:1, one launch (start us, length us, event | category | flops | bytes accessed | tf_op | source)
XLA Modules:
  0.0 221.6 jit_solution(5743348804734141124)
XLA Ops:
  4.0 13.1 %all-to-all-start = ((bf16[8,64,384]{2,1,0:T(8,128)(2,1)}), bf16[8,64,384]{2,1,0:T(8,128)(2,1)S(1)}, u32[]{:S(2)}, u32[]{:S(2)}) async-start(bf16[8,64,384]{2,1,0:T(8,128)(2,1)} %broadcast_in_dim.12), calls=%async_computation | async-start | bytes 786432 | tf_op jit(solution)/shard_map/all_to_all | solution.py:24
  17.2 4.6 %collective-permute-start.2 = (bf16[64,2048]{1,0:T(8,128)(2,1)S(1)}, bf16[64,2048]{1,0:T(8,128)(2,1)S(1)}, u32[]{:S(2)}, u32[]{:S(2)}) collective-permute-start(bf16[64,2048]{1,0:T(8,128)(2,1)S(1)} %pad_maximum_fusion.7), channel_id=1, source_target_pairs={{8,0},{16,8},{24,16},{0,24},{9,1},{17,9},{25,17},{1,25},{10,2},{18... | collective-permute-start | bytes 786440 | tf_op jit(solution)/shard_map/ppermute | solution.py:35
  27.0 7.4 %all-to-all-done = bf16[8,64,384]{2,1,0:T(8,128)(2,1)S(1)} async-done(((bf16[8,64,384]{2,1,0:T(8,128)(2,1)}), bf16[8,64,384]{2,1,0:T(8,128)(2,1)S(1)}, u32[]{:S(2)}, u32[]{:S(2)}) %all-to-all-start) | async-done | bytes 393248 | tf_op jit(solution)/shard_map/all_to_all | solution.py:24
  35.9 4.3 %all-to-all-start.1 = ((bf16[4,8,64,384]{3,2,1,0:T(8,128)(2,1)}), bf16[4,8,64,384]{3,2,1,0:T(8,128)(2,1)S(1)}, u32[]{:S(2)}, u32[]{:S(2)}) async-start(bf16[4,8,64,384]{3,2,1,0:T(8,128)(2,1)} %broadcast_in_dim.13), calls=%async_computation.1 | async-start | bytes 3145728 | tf_op jit(solution)/shard_map/all_to_all | solution.py:24
  41.4 8.8 %collective-permute-start.5 = (bf16[4,64,1024]{2,1,0:T(8,128)(2,1)}, bf16[4,64,1024]{2,1,0:T(8,128)(2,1)}, u32[]{:S(2)}, u32[]{:S(2)}) collective-permute-start(bf16[4,64,1024]{2,1,0:T(8,128)(2,1)} %get-tuple-element.14), channel_id=1, source_target_pairs={{0,1},{1,0},{2,3},{3,2},{4,5},{5,4},{6,7},{7,6},{8,9},{9,8},{10,11... | collective-permute-start | bytes 1572872 | tf_op jit(solution)/shard_map/ppermute | solution.py:99
  57.5 12.4 %all-to-all-start.2 = ((f32[8,2,256]{2,1,0:T(2,128)}), f32[8,2,256]{2,1,0:T(2,128)S(1)}, u32[]{:S(2)}, u32[]{:S(2)}) async-start(f32[8,2,256]{2,1,0:T(2,128)} %broadcast_in_dim.15), calls=%async_computation.2 | async-start | bytes 32768 | tf_op jit(solution)/shard_map/all_to_all | solution.py:24
  72.1 6.6 %collective-permute-start.6 = (bf16[2,4,64,1024]{3,2,1,0:T(8,128)(2,1)}, bf16[2,4,64,1024]{3,2,1,0:T(8,128)(2,1)S(1)}, u32[]{:S(2)}, u32[]{:S(2)}) collective-permute-start(bf16[2,4,64,1024]{3,2,1,0:T(8,128)(2,1)} %pad_maximum_fusion.1), channel_id=1, source_target_pairs={{32,0},{64,32},{96,64},{128,96},{160,128},{192,160},{224,192},{256... | collective-permute-start | bytes 3145736 | tf_op jit(solution)/shard_map/ppermute | solution.py:42
  80.0 3.9 %collective-permute-start = (bf16[128,2048]{1,0:T(8,128)(2,1)}, bf16[128,2048]{1,0:T(8,128)(2,1)}, u32[]{:S(2)}, u32[]{:S(2)}) collective-permute-start(bf16[128,2048]{1,0:T(8,128)(2,1)} %convolution_convert_fusion), channel_id=1, source_target_pairs={{0,1},{1,0},{2,3},{3,2},{4,5},{5,4},{6,7},{7,6},{8,9},{9,8},{10,11... | collective-permute-start | bytes 1572872 | tf_op jit(solution)/shard_map/ppermute | solution.py:99
  87.9 4.8 %collective-permute-done.6 = bf16[2,4,64,1024]{3,2,1,0:T(8,128)(2,1)S(1)} collective-permute-done((bf16[2,4,64,1024]{3,2,1,0:T(8,128)(2,1)}, bf16[2,4,64,1024]{3,2,1,0:T(8,128)(2,1)S(1)}, u32[]{:S(2)}, u32[]{:S(2)}) %collective-permute-start.6) | collective-permute-done | bytes 1048608 | tf_op jit(solution)/shard_map/ppermute | solution.py:42
  96.8 4.3 %all-to-all-start.3 = ((bf16[4,32,2048]{2,1,0:T(8,128)(2,1)}), bf16[4,32,2048]{2,1,0:T(8,128)(2,1)S(1)}, u32[]{:S(2)}, u32[]{:S(2)}) async-start(bf16[4,32,2048]{2,1,0:T(8,128)(2,1)} %bitcast.98), calls=%async_computation.3 | async-start | bytes 1048576 | tf_op jit(solution)/shard_map/all_to_all | solution.py:24
  106.0 9.3 %collective-permute-done.7 = bf16[2,4,64,1024]{3,2,1,0:T(8,128)(2,1)} collective-permute-done((bf16[2,4,64,1024]{3,2,1,0:T(8,128)(2,1)S(1)}, bf16[2,4,64,1024]{3,2,1,0:T(8,128)(2,1)}, u32[]{:S(2)}, u32[]{:S(2)}) %collective-permute-start.7) | collective-permute-done | bytes 1048608 | tf_op jit(solution)/shard_map/ppermute | solution.py:42
  119.9 4.1 %all-to-all-start.4 = ((bf16[4,2,32,1024]{3,2,1,0:T(8,128)(2,1)}), bf16[4,2,32,1024]{3,2,1,0:T(8,128)(2,1)}, u32[]{:S(2)}, u32[]{:S(2)}) async-start(bf16[4,2,32,1024]{3,2,1,0:T(8,128)(2,1)} %broadcast_in_dim.16), calls=%async_computation.4 | async-start | bytes 1048576 | tf_op jit(solution)/shard_map/all_to_all | solution.py:24
  128.4 9.3 %collective-permute-done.8 = bf16[2,4,64,1024]{3,2,1,0:T(8,128)(2,1)S(1)} collective-permute-done((bf16[2,4,64,1024]{3,2,1,0:T(8,128)(2,1)}, bf16[2,4,64,1024]{3,2,1,0:T(8,128)(2,1)S(1)}, u32[]{:S(2)}, u32[]{:S(2)}) %collective-permute-start.8) | collective-permute-done | bytes 1048608 | tf_op jit(solution)/shard_map/ppermute | solution.py:42
  142.3 5.9 %collective-permute-start.1 = (bf16[128,1024]{1,0:T(8,128)(2,1)S(1)}, bf16[128,1024]{1,0:T(8,128)(2,1)S(1)}, u32[]{:S(2)}, u32[]{:S(2)}) collective-permute-start(bf16[128,1024]{1,0:T(8,128)(2,1)S(1)} %bitcast.114), channel_id=1, source_target_pairs={{0,1},{1,0},{2,3},{3,2},{4,5},{5,4},{6,7},{7,6},{8,9},{9,8},{10,11... | collective-permute-start | bytes 786440 | tf_op jit(solution)/shard_map/ppermute | solution.py:99
  150.5 4.0 %collective-permute-done.9 = bf16[2,2,64,1024]{3,2,1,0:T(8,128)(2,1)} collective-permute-done((bf16[2,2,64,1024]{3,2,1,0:T(8,128)(2,1)}, bf16[2,2,64,1024]{3,2,1,0:T(8,128)(2,1)}, u32[]{:S(2)}, u32[]{:S(2)}) %collective-permute-start.9) | collective-permute-done | bytes 524320 | tf_op jit(solution)/shard_map/ppermute | solution.py:42
  154.6 3.2 %shard_map.146 = bf16[256,1024]{1,0:T(8,128)(2,1)} custom-call(s32[1]{0:T(128)} %bitcast.10.refs_0_, bf16[128,1024]{1,0:T(8,128)(2,1)} %bitcast.95, bf16[128,1024]{1,0:T(8,128)(2,1)} %copy-done.10, bf16[2,256,1024]{2,1,0:T(8,128)(2,1)} %pad_maximum_fusion.refs_3_, bf16[2,256,1024]{2,1,0:T(8,128)(2,1)} %bitcast.91, bf16[2,256,1024]{2,1,0:T(8,128)(2,1)} %bitcast.25.refs_5_, ...), custom_call_target="tpu_custom_call" | custom-call | flops 536870912 | bytes 2097152 | tf_op jit(solution)/shard_map/pallas_call | solution.py:206
  162.7 3.4 %shard_map.145 = f32[256,1024]{1,0:T(8,128)} custom-call(s32[1]{0:T(128)} %bitcast.10.refs_0_, bf16[128,1024]{1,0:T(8,128)(2,1)} %bitcast.96, bf16[128,1024]{1,0:T(8,128)(2,1)} %copy-done.10, bf16[2,256,1024]{2,1,0:T(8,128)(2,1)} %pad_maximum_fusion.refs_3_, bf16[2,256,1024]{2,1,0:T(8,128)(2,1)} %bitcast.92, bf16[2,256,1024]{2,1,0:T(8,128)(2,1)} %bitcast.25.refs_5_, ...), custom_call_target="tpu_custom_call" | custom-call | flops 536870912 | bytes 2097152 | tf_op jit(solution)/shard_map/pallas_call | solution.py:206
  167.7 5.1 %collective-permute-start.11 = (bf16[256,1024]{1,0:T(8,128)(2,1)S(1)}, bf16[256,1024]{1,0:T(8,128)(2,1)S(1)}, u32[]{:S(2)}, u32[]{:S(2)}) collective-permute-start(bf16[256,1024]{1,0:T(8,128)(2,1)S(1)} %multiply_convert_fusion.refs_1_.refs_2_), channel_id=1, source_target_pairs={{0,1},{1,0},{2,3},{3,2},{4,5},{5,4},{6,7},{7,6},{8,9},{9,8},{10,11... | collective-permute-start | bytes 1572872 | tf_op jit(solution)/shard_map/ppermute | solution.py:99
  175.9 4.5 %shard_map.147.refs_2_ = f32[256,1024]{1,0:T(8,128)} custom-call(s32[1]{0:T(128)} %bitcast.10.refs_0_, bf16[256,1024]{1,0:T(8,128)(2,1)} %copy-done.3, bf16[256,1024]{1,0:T(8,128)(2,1)} %copy-done.3, bf16[2,256,1024]{2,1,0:T(8,128)(2,1)} %pad_maximum_fusion.2.refs_3_, bf16[2,256,1024]{2,1,0:T(8,128)(2,1)} %bitcast.36.refs_4_, ...), custom_call_target="tpu_custom_call" | custom-call | flops 536870912 | bytes 2097152 | tf_op jit(solution)/shard_map/pallas_call | solution.py:206
  181.2 4.5 %shard_map.148 = bf16[4,2,32,1024]{3,2,1,0:T(8,128)(2,1)} custom-call(s32[1]{0:T(128)} %bitcast.10.refs_0_, bf16[256,1024]{1,0:T(8,128)(2,1)} %copy-done.12, f32[256,1024]{1,0:T(8,128)} %shard_map.147.refs_2_, bf16[2,256,1024]{2,1,0:T(8,128)(2,1)} %pad_maximum_fusion.2.refs_3_, bf16[2,256,1024]{2,1,0:T(8,128)(2,1)} %bitcast.36.refs_4_, ...), custom_call_target="tpu_custom_call" | custom-call | flops 536870912 | bytes 2097152 | tf_op jit(solution)/shard_map/pallas_call | solution.py:206
  185.6 13.8 %all_to_all.35 = bf16[4,2,32,1024]{3,2,1,0:T(8,128)(2,1)S(1)} all-to-all(bf16[4,2,32,1024]{3,2,1,0:T(8,128)(2,1)} %shard_map.148), channel_id=1, replica_groups=mesh['rep'=2,'z'=8,'y'=4,'x'=4,'core'=2] {'x'}, dimensions={0} | all-to-all | bytes 1048576 | tf_op jit(solution)/shard_map/all_to_all | solution.py:24
  199.5 3.1 %collective-permute-start.17 = (bf16[32,1024]{1,0:T(8,128)(2,1)S(1)}, bf16[32,1024]{1,0:T(8,128)(2,1)S(1)}, u32[]{:S(2)}, u32[]{:S(2)}) collective-permute-start(bf16[32,1024]{1,0:T(8,128)(2,1)S(1)} %fusion.30), channel_id=1, source_target_pairs={{0,1},{1,0},{2,3},{3,2},{4,5},{5,4},{6,7},{7,6},{8,9},{9,8},{10,11... | collective-permute-start | bytes 196616 | tf_op jit(solution)/shard_map/ppermute | solution.py:99
  204.1 11.6 %all_to_all.36 = bf16[4,32,2048]{2,1,0:T(8,128)(2,1)S(1)} all-to-all(bf16[4,32,2048]{2,1,0:T(8,128)(2,1)S(1)} %broadcast_in_dim.17), channel_id=1, replica_groups=mesh['rep'=2,'z'=8,'y'=4,'x'=4,'core'=2] {'x'}, dimensions={0} | all-to-all | bytes 1048576 | tf_op jit(solution)/shard_map/all_to_all | solution.py:24
  215.8 3.1 %collective-permute-start.18 = (bf16[128,2048]{1,0:T(8,128)(2,1)S(1)}, bf16[128,2048]{1,0:T(8,128)(2,1)S(1)}, u32[]{:S(2)}, u32[]{:S(2)}) collective-permute-start(bf16[128,2048]{1,0:T(8,128)(2,1)S(1)} %bitcast.97), channel_id=1, source_target_pairs={{0,1},{1,0},{2,3},{3,2},{4,5},{5,4},{6,7},{7,6},{8,9},{9,8},{10,11... | collective-permute-start | bytes 1572872 | tf_op jit(solution)/shard_map/ppermute | solution.py:99
  (153 shorter events, 65.7 us)
Async XLA Ops:
  4.0 30.5 %all-to-all-start = ((bf16[8,64,384]{2,1,0:T(8,128)(2,1)}), bf16[8,64,384]{2,1,0:T(8,128)(2,1)S(1)}, u32[]{:S(2)}, u32[]{:S(2)}) async-start(bf16[8,64,384]{2,1,0:T(8,128)(2,1)} %broadcast_in_dim.12), calls=%async_computation | async-start | bytes 786432 | tf_op jit(solution)/shard_map/all_to_all | solution.py:24
  17.2 23.0 %collective-permute-start.2 = (bf16[64,2048]{1,0:T(8,128)(2,1)S(1)}, bf16[64,2048]{1,0:T(8,128)(2,1)S(1)}, u32[]{:S(2)}, u32[]{:S(2)}) collective-permute-start(bf16[64,2048]{1,0:T(8,128)(2,1)S(1)} %pad_maximum_fusion.7), channel_id=1, source_target_pairs={{8,0},{16,8},{24,16},{0,24},{9,1},{17,9},{25,17},{1,25},{10,2},{18... | collective-permute-start | bytes 786440 | tf_op jit(solution)/shard_map/ppermute | solution.py:35
  21.9 18.4 %collective-permute-start.3 = (bf16[64,2048]{1,0:T(8,128)(2,1)S(1)}, bf16[64,2048]{1,0:T(8,128)(2,1)S(1)}, u32[]{:S(2)}, u32[]{:S(2)}) collective-permute-start(bf16[64,2048]{1,0:T(8,128)(2,1)S(1)} %pad_maximum_fusion.7), channel_id=1, source_target_pairs={{16,0},{24,8},{0,16},{8,24},{17,1},{25,9},{1,17},{9,25},{18,2},{26... | collective-permute-start | bytes 786440 | tf_op jit(solution)/shard_map/ppermute | solution.py:35
  24.1 16.2 %collective-permute-start.4 = (bf16[64,2048]{1,0:T(8,128)(2,1)S(1)}, bf16[64,2048]{1,0:T(8,128)(2,1)S(1)}, u32[]{:S(2)}, u32[]{:S(2)}) collective-permute-start(bf16[64,2048]{1,0:T(8,128)(2,1)S(1)} %pad_maximum_fusion.7), channel_id=1, source_target_pairs={{24,0},{0,8},{8,16},{16,24},{25,1},{1,9},{9,17},{17,25},{26,2},{2,... | collective-permute-start | bytes 786440 | tf_op jit(solution)/shard_map/ppermute | solution.py:35
  35.9 17.9 %all-to-all-start.1 = ((bf16[4,8,64,384]{3,2,1,0:T(8,128)(2,1)}), bf16[4,8,64,384]{3,2,1,0:T(8,128)(2,1)S(1)}, u32[]{:S(2)}, u32[]{:S(2)}) async-start(bf16[4,8,64,384]{3,2,1,0:T(8,128)(2,1)} %broadcast_in_dim.13), calls=%async_computation.1 | async-start | bytes 3145728 | tf_op jit(solution)/shard_map/all_to_all | solution.py:24
  41.4 28.5 %collective-permute-start.5 = (bf16[4,64,1024]{2,1,0:T(8,128)(2,1)}, bf16[4,64,1024]{2,1,0:T(8,128)(2,1)}, u32[]{:S(2)}, u32[]{:S(2)}) collective-permute-start(bf16[4,64,1024]{2,1,0:T(8,128)(2,1)} %get-tuple-element.14), channel_id=1, source_target_pairs={{0,1},{1,0},{2,3},{3,2},{4,5},{5,4},{6,7},{7,6},{8,9},{9,8},{10,11... | collective-permute-start | bytes 1572872 | tf_op jit(solution)/shard_map/ppermute | solution.py:99
  51.3 32.6 %collective-permute-start.12 = (bf16[4,64,1024]{2,1,0:T(8,128)(2,1)}, bf16[4,64,1024]{2,1,0:T(8,128)(2,1)}, u32[]{:S(2)}, u32[]{:S(2)}) collective-permute-start(bf16[4,64,1024]{2,1,0:T(8,128)(2,1)} %get-tuple-element.12), channel_id=1, source_target_pairs={{0,1},{1,0},{2,3},{3,2},{4,5},{5,4},{6,7},{7,6},{8,9},{9,8},{10,11... | collective-permute-start | bytes 1572872 | tf_op jit(solution)/shard_map/ppermute | solution.py:99
  57.5 21.1 %all-to-all-start.2 = ((f32[8,2,256]{2,1,0:T(2,128)}), f32[8,2,256]{2,1,0:T(2,128)S(1)}, u32[]{:S(2)}, u32[]{:S(2)}) async-start(f32[8,2,256]{2,1,0:T(2,128)} %broadcast_in_dim.15), calls=%async_computation.2 | async-start | bytes 32768 | tf_op jit(solution)/shard_map/all_to_all | solution.py:24
  72.1 20.6 %collective-permute-start.6 = (bf16[2,4,64,1024]{3,2,1,0:T(8,128)(2,1)}, bf16[2,4,64,1024]{3,2,1,0:T(8,128)(2,1)S(1)}, u32[]{:S(2)}, u32[]{:S(2)}) collective-permute-start(bf16[2,4,64,1024]{3,2,1,0:T(8,128)(2,1)} %pad_maximum_fusion.1), channel_id=1, source_target_pairs={{32,0},{64,32},{96,64},{128,96},{160,128},{192,160},{224,192},{256... | collective-permute-start | bytes 3145736 | tf_op jit(solution)/shard_map/ppermute | solution.py:42
  80.0 14.7 %collective-permute-start = (bf16[128,2048]{1,0:T(8,128)(2,1)}, bf16[128,2048]{1,0:T(8,128)(2,1)}, u32[]{:S(2)}, u32[]{:S(2)}) collective-permute-start(bf16[128,2048]{1,0:T(8,128)(2,1)} %convolution_convert_fusion), channel_id=1, source_target_pairs={{0,1},{1,0},{2,3},{3,2},{4,5},{5,4},{6,7},{7,6},{8,9},{9,8},{10,11... | collective-permute-start | bytes 1572872 | tf_op jit(solution)/shard_map/ppermute | solution.py:99
  86.0 18.0 %collective-permute-start.13 = (bf16[2,4,64,1024]{3,2,1,0:T(8,128)(2,1)}, bf16[2,4,64,1024]{3,2,1,0:T(8,128)(2,1)}, u32[]{:S(2)}, u32[]{:S(2)}) collective-permute-start(bf16[2,4,64,1024]{3,2,1,0:T(8,128)(2,1)} %pad_maximum_fusion.3), channel_id=1, source_target_pairs={{32,0},{64,32},{96,64},{128,96},{160,128},{192,160},{224,192},{256... | collective-permute-start | bytes 3145736 | tf_op jit(solution)/shard_map/ppermute | solution.py:42
  92.7 22.6 %collective-permute-start.7 = (bf16[2,4,64,1024]{3,2,1,0:T(8,128)(2,1)S(1)}, bf16[2,4,64,1024]{3,2,1,0:T(8,128)(2,1)}, u32[]{:S(2)}, u32[]{:S(2)}) collective-permute-start(bf16[2,4,64,1024]{3,2,1,0:T(8,128)(2,1)S(1)} %collective-permute-done.6), channel_id=1, source_target_pairs={{32,0},{64,32},{96,64},{128,96},{160,128},{192,160},{224,192},{256... | collective-permute-start | bytes 3145736 | tf_op jit(solution)/shard_map/ppermute | solution.py:42
  96.8 20.4 %all-to-all-start.3 = ((bf16[4,32,2048]{2,1,0:T(8,128)(2,1)}), bf16[4,32,2048]{2,1,0:T(8,128)(2,1)S(1)}, u32[]{:S(2)}, u32[]{:S(2)}) async-start(bf16[4,32,2048]{2,1,0:T(8,128)(2,1)} %bitcast.98), calls=%async_computation.3 | async-start | bytes 1048576 | tf_op jit(solution)/shard_map/all_to_all | solution.py:24
  104.0 22.4 %collective-permute-start.14 = (bf16[2,4,64,1024]{3,2,1,0:T(8,128)(2,1)}, bf16[2,4,64,1024]{3,2,1,0:T(8,128)(2,1)S(1)}, u32[]{:S(2)}, u32[]{:S(2)}) collective-permute-start(bf16[2,4,64,1024]{3,2,1,0:T(8,128)(2,1)} %collective-permute-done.13), channel_id=1, source_target_pairs={{32,0},{64,32},{96,64},{128,96},{160,128},{192,160},{224,192},{256... | collective-permute-start | bytes 3145736 | tf_op jit(solution)/shard_map/ppermute | solution.py:42
  115.3 22.4 %collective-permute-start.8 = (bf16[2,4,64,1024]{3,2,1,0:T(8,128)(2,1)}, bf16[2,4,64,1024]{3,2,1,0:T(8,128)(2,1)S(1)}, u32[]{:S(2)}, u32[]{:S(2)}) collective-permute-start(bf16[2,4,64,1024]{3,2,1,0:T(8,128)(2,1)} %collective-permute-done.7), channel_id=1, source_target_pairs={{32,0},{64,32},{96,64},{128,96},{160,128},{192,160},{224,192},{256... | collective-permute-start | bytes 3145736 | tf_op jit(solution)/shard_map/ppermute | solution.py:42
  119.9 20.6 %all-to-all-start.4 = ((bf16[4,2,32,1024]{3,2,1,0:T(8,128)(2,1)}), bf16[4,2,32,1024]{3,2,1,0:T(8,128)(2,1)}, u32[]{:S(2)}, u32[]{:S(2)}) async-start(bf16[4,2,32,1024]{3,2,1,0:T(8,128)(2,1)} %broadcast_in_dim.16), calls=%async_computation.4 | async-start | bytes 1048576 | tf_op jit(solution)/shard_map/all_to_all | solution.py:24
  126.4 33.8 %collective-permute-start.15 = (bf16[2,4,64,1024]{3,2,1,0:T(8,128)(2,1)S(1)}, bf16[2,4,64,1024]{3,2,1,0:T(8,128)(2,1)S(1)}, u32[]{:S(2)}, u32[]{:S(2)}) collective-permute-start(bf16[2,4,64,1024]{3,2,1,0:T(8,128)(2,1)S(1)} %collective-permute-done.14), channel_id=1, source_target_pairs={{32,0},{64,32},{96,64},{128,96},{160,128},{192,160},{224,192},{256... | collective-permute-start | bytes 3145736 | tf_op jit(solution)/shard_map/ppermute | solution.py:42
  138.5 16.0 %collective-permute-start.9 = (bf16[2,2,64,1024]{3,2,1,0:T(8,128)(2,1)}, bf16[2,2,64,1024]{3,2,1,0:T(8,128)(2,1)}, u32[]{:S(2)}, u32[]{:S(2)}) collective-permute-start(bf16[2,2,64,1024]{3,2,1,0:T(8,128)(2,1)} %constant_dynamic-slice_fusion.1), channel_id=1, source_target_pairs={{32,0},{64,32},{96,64},{128,96},{160,128},{192,160},{224,192},{256... | collective-permute-start | bytes 1572872 | tf_op jit(solution)/shard_map/ppermute | solution.py:42
  142.3 8.2 %collective-permute-start.1 = (bf16[128,1024]{1,0:T(8,128)(2,1)S(1)}, bf16[128,1024]{1,0:T(8,128)(2,1)S(1)}, u32[]{:S(2)}, u32[]{:S(2)}) collective-permute-start(bf16[128,1024]{1,0:T(8,128)(2,1)S(1)} %bitcast.114), channel_id=1, source_target_pairs={{0,1},{1,0},{2,3},{3,2},{4,5},{5,4},{6,7},{7,6},{8,9},{9,8},{10,11... | collective-permute-start | bytes 786440 | tf_op jit(solution)/shard_map/ppermute | solution.py:99
  157.8 8.3 %collective-permute-start.10 = (bf16[256,1024]{1,0:T(8,128)(2,1)}, bf16[256,1024]{1,0:T(8,128)(2,1)}, u32[]{:S(2)}, u32[]{:S(2)}) collective-permute-start(bf16[256,1024]{1,0:T(8,128)(2,1)} %shard_map.146), channel_id=1, source_target_pairs={{0,1},{1,0},{2,3},{3,2},{4,5},{5,4},{6,7},{7,6},{8,9},{9,8},{10,11... | collective-permute-start | bytes 1572872 | tf_op jit(solution)/shard_map/ppermute | solution.py:99
  160.3 14.8 %collective-permute-start.16 = (bf16[2,2,64,1024]{3,2,1,0:T(8,128)(2,1)S(1)}, bf16[2,2,64,1024]{3,2,1,0:T(8,128)(2,1)S(1)}, u32[]{:S(2)}, u32[]{:S(2)}) collective-permute-start(bf16[2,2,64,1024]{3,2,1,0:T(8,128)(2,1)S(1)} %constant_dynamic-slice_fusion), channel_id=1, source_target_pairs={{32,0},{64,32},{96,64},{128,96},{160,128},{192,160},{224,192},{256... | collective-permute-start | bytes 1572872 | tf_op jit(solution)/shard_map/ppermute | solution.py:42
  167.7 12.7 %collective-permute-start.11 = (bf16[256,1024]{1,0:T(8,128)(2,1)S(1)}, bf16[256,1024]{1,0:T(8,128)(2,1)S(1)}, u32[]{:S(2)}, u32[]{:S(2)}) collective-permute-start(bf16[256,1024]{1,0:T(8,128)(2,1)S(1)} %multiply_convert_fusion.refs_1_.refs_2_), channel_id=1, source_target_pairs={{0,1},{1,0},{2,3},{3,2},{4,5},{5,4},{6,7},{7,6},{8,9},{9,8},{10,11... | collective-permute-start | bytes 1572872 | tf_op jit(solution)/shard_map/ppermute | solution.py:99
  199.5 3.9 %collective-permute-start.17 = (bf16[32,1024]{1,0:T(8,128)(2,1)S(1)}, bf16[32,1024]{1,0:T(8,128)(2,1)S(1)}, u32[]{:S(2)}, u32[]{:S(2)}) collective-permute-start(bf16[32,1024]{1,0:T(8,128)(2,1)S(1)} %fusion.30), channel_id=1, source_target_pairs={{0,1},{1,0},{2,3},{3,2},{4,5},{5,4},{6,7},{7,6},{8,9},{9,8},{10,11... | collective-permute-start | bytes 196616 | tf_op jit(solution)/shard_map/ppermute | solution.py:99
  215.8 4.6 %collective-permute-start.18 = (bf16[128,2048]{1,0:T(8,128)(2,1)S(1)}, bf16[128,2048]{1,0:T(8,128)(2,1)S(1)}, u32[]{:S(2)}, u32[]{:S(2)}) collective-permute-start(bf16[128,2048]{1,0:T(8,128)(2,1)S(1)} %bitcast.97), channel_id=1, source_target_pairs={{0,1},{1,0},{2,3},{3,2},{4,5},{5,4},{6,7},{7,6},{8,9},{9,8},{10,11... | collective-permute-start | bytes 1572872 | tf_op jit(solution)/shard_map/ppermute | solution.py:99
  (21 other events, 291.9 us)

commit v5 on v4

--- a/solution.py
+++ b/solution.py
@@ -46,14 +46,17 @@
     core = lax.axis_index("core")
     pieces = {}
     for name, block in chunks.items():
-        pieces[name] = [jnp.stack([block, swapped(block)])]
+        pieces[name] = [block, swapped(block)]
     for d in range(1, 5):
         for got in pieces.values():
-            last = got[-1]
+            last = jnp.stack(got) if d == 1 else got[-1]
             if d == 4:
                 last = lax.dynamic_slice_in_dim(last, core * (last.shape[1] // 2), last.shape[1] // 2, 1)
             got.append(hop(last))
-    return [[p.reshape(2, -1, p.shape[-1]) for p in got] for got in pieces.values()]
+    return [
+        [p.reshape(-1, p.shape[-1]) for p in got[:2]] + [p.reshape(2, -1, p.shape[-1]) for p in got[2:]]
+        for got in pieces.values()
+    ]
 
 
 def to_sides(x):
@@ -155,8 +158,8 @@
 
 
 def fetch_side(slot, core, pieces, whole, sems):
-    half = pieces[0].shape[1] // 2
-    sources = [pieces[0].at[slot, pl.ds(core * half, half)]] + [p.at[slot] for p in pieces[1:]]
+    half = pieces[0].shape[0] // 2
+    sources = [pieces[0].at[pl.ds(core * half, half)]] + [p.at[slot] for p in pieces[1:]]
     at, copies = 0, []
     for i, source in enumerate(sources):
         n = source.shape[0]
@@ -200,9 +203,10 @@
 def side_call(body, name, slot, core, operands, pieces, out_shape, scratch):
     anywhere = pl.BlockSpec(memory_space=pl.ANY)
     inside = pl.BlockSpec(memory_space=pltpu.VMEM)
+    pieces = [pieces[slot]] + pieces[2:]
     here = anywhere if name == "up" else inside
-    cols = pieces[0].shape[2]
-    rows = 4 * pieces[0].shape[1]
+    cols = pieces[0].shape[1]
+    rows = 4 * pieces[0].shape[0]
     return pl.pallas_call(
         lambda *refs: body(slot, *refs),
         in_specs=[pl.BlockSpec(memory_space=pltpu.SMEM)] + [here] * len(operands) + [anywhere] * len(pieces),

time: 223 us -> 222 us (level)
  other arithmetic: 19.9 us -> 17.1 us
  waiting for transfers between devices: 42.9 us -> 45.3 us
    another operation x6 -> x4, other arithmetic: 11 us -> 6.41 us  [side_ring(): last = jnp.stack(got) if d == 1 else got[-1]]
  transfers between devices with their start and end apart: 24 -> 24, of which waited for: 10 -> 11; matrix products, arithmetic and copies ran while one was open for 12% -> 10% of each run, Pallas kernels for 5% -> 5%
where the time goes in v5:
time: 222 us; the launch traced here: 220 us
  starting transfers between devices  102 us (46%)
  waiting for transfers between devices  45.3 us (20%)
  blocking collectives  25.4 us (11%)
  other arithmetic  17.1 us (8%)
  Pallas kernels  15.6 us (7%)
  local copies, waits for them, and re-layouts  8.81 us (4%)
  matrix products  4.45 us (2%)
    all_to_all x5, starting transfers between devices, exchange(): return lax.all_to_all(x, axis, split_axis=0, concat_axis=0, tiled=True)  38.1 us
    ppermute x8, starting transfers between devices, swapped(): return lax.ppermute(x, 'core', [(0, 1), (1, 0)])  34.3 us
    ppermute x8, waiting for transfers between devices, hop(): return lax.ppermute(x, (*RING, 'core'), pairs)  33.9 us
    all_to_all x2, blocking collectives, exchange(): return lax.all_to_all(x, axis, split_axis=0, concat_axis=0, tiled=True)  25.4 us
    ppermute x8, starting transfers between devices, hop(): return lax.ppermute(x, (*RING, 'core'), pairs)  20.5 us
    pallas_call x4, Pallas kernels, side_call(): pl.pallas_call(lambda *refs: body(slot, *refs), in_specs=[pl.BlockSpec(me...  15.6 us
    ppermute x3, starting transfers between devices, y_ring(): others[d] = lax.ppermute(block, 'y', [((i + d) % n, i) for i in range(n)])  9.5 us
    all_to_all x5, waiting for transfers between devices, exchange(): return lax.all_to_all(x, axis, split_axis=0, concat_axis=0, tiled=True)  7.9 us
  transfers between devices with their start and end apart: 24, of which 11 were waited for; matrix products, arithmetic and copies ran while one was open for 10% of the time, Pallas kernels for 5%

profile of v5, /device:TPU:1, one launch (start us, length us, event | category | flops | bytes accessed | tf_op | source)
XLA Modules:
  0.0 220.1 jit_solution(16023152156466471878)
XLA Ops:
  4.0 13.1 %all-to-all-start = ((bf16[8,64,384]{2,1,0:T(8,128)(2,1)}), bf16[8,64,384]{2,1,0:T(8,128)(2,1)S(1)}, u32[]{:S(2)}, u32[]{:S(2)}) async-start(bf16[8,64,384]{2,1,0:T(8,128)(2,1)} %broadcast_in_dim.12), calls=%async_computation | async-start | bytes 786432 | tf_op jit(solution)/shard_map/all_to_all | solution.py:24
  17.2 4.6 %collective-permute-start.2 = (bf16[64,2048]{1,0:T(8,128)(2,1)S(1)}, bf16[64,2048]{1,0:T(8,128)(2,1)S(1)}, u32[]{:S(2)}, u32[]{:S(2)}) collective-permute-start(bf16[64,2048]{1,0:T(8,128)(2,1)S(1)} %pad_maximum_fusion.5), channel_id=1, source_target_pairs={{8,0},{16,8},{24,16},{0,24},{9,1},{17,9},{25,17},{1,25},{10,2},{18... | collective-permute-start | bytes 786440 | tf_op jit(solution)/shard_map/ppermute | solution.py:35
  27.0 7.4 %all-to-all-done = bf16[8,64,384]{2,1,0:T(8,128)(2,1)S(1)} async-done(((bf16[8,64,384]{2,1,0:T(8,128)(2,1)}), bf16[8,64,384]{2,1,0:T(8,128)(2,1)S(1)}, u32[]{:S(2)}, u32[]{:S(2)}) %all-to-all-start) | async-done | bytes 393248 | tf_op jit(solution)/shard_map/all_to_all | solution.py:24
  35.9 4.3 %all-to-all-start.1 = ((bf16[4,8,64,384]{3,2,1,0:T(8,128)(2,1)}), bf16[4,8,64,384]{3,2,1,0:T(8,128)(2,1)S(1)}, u32[]{:S(2)}, u32[]{:S(2)}) async-start(bf16[4,8,64,384]{3,2,1,0:T(8,128)(2,1)} %broadcast_in_dim.13), calls=%async_computation.1 | async-start | bytes 3145728 | tf_op jit(solution)/shard_map/all_to_all | solution.py:24
  41.4 8.8 %collective-permute-start.5 = (bf16[4,64,1024]{2,1,0:T(8,128)(2,1)}, bf16[4,64,1024]{2,1,0:T(8,128)(2,1)}, u32[]{:S(2)}, u32[]{:S(2)}) collective-permute-start(bf16[4,64,1024]{2,1,0:T(8,128)(2,1)} %get-tuple-element.14), channel_id=1, source_target_pairs={{0,1},{1,0},{2,3},{3,2},{4,5},{5,4},{6,7},{7,6},{8,9},{9,8},{10,11... | collective-permute-start | bytes 1572872 | tf_op jit(solution)/shard_map/ppermute | solution.py:102
  57.5 12.3 %all-to-all-start.2 = ((f32[8,2,256]{2,1,0:T(2,128)}), f32[8,2,256]{2,1,0:T(2,128)S(1)}, u32[]{:S(2)}, u32[]{:S(2)}) async-start(f32[8,2,256]{2,1,0:T(2,128)} %broadcast_in_dim.15), calls=%async_computation.2 | async-start | bytes 32768 | tf_op jit(solution)/shard_map/all_to_all | solution.py:24
  72.0 6.5 %collective-permute-start.6 = (bf16[2,4,64,1024]{3,2,1,0:T(8,128)(2,1)}, bf16[2,4,64,1024]{3,2,1,0:T(8,128)(2,1)}, u32[]{:S(2)}, u32[]{:S(2)}) collective-permute-start(bf16[2,4,64,1024]{3,2,1,0:T(8,128)(2,1)} %pad_maximum_fusion), channel_id=1, source_target_pairs={{32,0},{64,32},{96,64},{128,96},{160,128},{192,160},{224,192},{256... | collective-permute-start | bytes 3145736 | tf_op jit(solution)/shard_map/ppermute | solution.py:42
  80.0 3.9 %collective-permute-start = (bf16[128,2048]{1,0:T(8,128)(2,1)}, bf16[128,2048]{1,0:T(8,128)(2,1)S(1)}, u32[]{:S(2)}, u32[]{:S(2)}) collective-permute-start(bf16[128,2048]{1,0:T(8,128)(2,1)} %convolution_convert_fusion), channel_id=1, source_target_pairs={{0,1},{1,0},{2,3},{3,2},{4,5},{5,4},{6,7},{7,6},{8,9},{9,8},{10,11... | collective-permute-start | bytes 1572872 | tf_op jit(solution)/shard_map/ppermute | solution.py:102
  87.9 4.9 %collective-permute-done.6 = bf16[2,4,64,1024]{3,2,1,0:T(8,128)(2,1)} collective-permute-done((bf16[2,4,64,1024]{3,2,1,0:T(8,128)(2,1)}, bf16[2,4,64,1024]{3,2,1,0:T(8,128)(2,1)}, u32[]{:S(2)}, u32[]{:S(2)}) %collective-permute-start.6) | collective-permute-done | bytes 1048608 | tf_op jit(solution)/shard_map/ppermute | solution.py:42
  95.9 4.3 %all-to-all-start.3 = ((bf16[4,32,2048]{2,1,0:T(8,128)(2,1)}), bf16[4,32,2048]{2,1,0:T(8,128)(2,1)}, u32[]{:S(2)}, u32[]{:S(2)}) async-start(bf16[4,32,2048]{2,1,0:T(8,128)(2,1)} %bitcast.9), calls=%async_computation.3 | async-start | bytes 1048576 | tf_op jit(solution)/shard_map/all_to_all | solution.py:24
  100.1 3.8 %collective-permute-done.13 = bf16[2,4,64,1024]{3,2,1,0:T(8,128)(2,1)S(1)} collective-permute-done((bf16[2,4,64,1024]{3,2,1,0:T(8,128)(2,1)}, bf16[2,4,64,1024]{3,2,1,0:T(8,128)(2,1)S(1)}, u32[]{:S(2)}, u32[]{:S(2)}) %collective-permute-start.13) | collective-permute-done | bytes 1048608 | tf_op jit(solution)/shard_map/ppermute | solution.py:42
  105.9 9.4 %collective-permute-done.7 = bf16[2,4,64,1024]{3,2,1,0:T(8,128)(2,1)} collective-permute-done((bf16[2,4,64,1024]{3,2,1,0:T(8,128)(2,1)}, bf16[2,4,64,1024]{3,2,1,0:T(8,128)(2,1)}, u32[]{:S(2)}, u32[]{:S(2)}) %collective-permute-start.7) | collective-permute-done | bytes 1048608 | tf_op jit(solution)/shard_map/ppermute | solution.py:42
  120.9 4.1 %all-to-all-start.4 = ((bf16[4,2,32,1024]{3,2,1,0:T(8,128)(2,1)}), bf16[4,2,32,1024]{3,2,1,0:T(8,128)(2,1)}, u32[]{:S(2)}, u32[]{:S(2)}) async-start(bf16[4,2,32,1024]{3,2,1,0:T(8,128)(2,1)} %broadcast_in_dim.16), calls=%async_computation.4 | async-start | bytes 1048576 | tf_op jit(solution)/shard_map/all_to_all | solution.py:24
  128.3 9.3 %collective-permute-done.8 = bf16[2,4,64,1024]{3,2,1,0:T(8,128)(2,1)S(1)} collective-permute-done((bf16[2,4,64,1024]{3,2,1,0:T(8,128)(2,1)}, bf16[2,4,64,1024]{3,2,1,0:T(8,128)(2,1)S(1)}, u32[]{:S(2)}, u32[]{:S(2)}) %collective-permute-start.8) | collective-permute-done | bytes 1048608 | tf_op jit(solution)/shard_map/ppermute | solution.py:42
  142.3 6.0 %collective-permute-start.1 = (bf16[128,1024]{1,0:T(8,128)(2,1)S(1)}, bf16[128,1024]{1,0:T(8,128)(2,1)S(1)}, u32[]{:S(2)}, u32[]{:S(2)}) collective-permute-start(bf16[128,1024]{1,0:T(8,128)(2,1)S(1)} %bitcast.113), channel_id=1, source_target_pairs={{0,1},{1,0},{2,3},{3,2},{4,5},{5,4},{6,7},{7,6},{8,9},{9,8},{10,11... | collective-permute-start | bytes 786440 | tf_op jit(solution)/shard_map/ppermute | solution.py:102
  149.4 5.2 %collective-permute-done.9 = bf16[2,2,64,1024]{3,2,1,0:T(8,128)(2,1)} collective-permute-done((bf16[2,2,64,1024]{3,2,1,0:T(8,128)(2,1)}, bf16[2,2,64,1024]{3,2,1,0:T(8,128)(2,1)}, u32[]{:S(2)}, u32[]{:S(2)}) %collective-permute-start.9) | collective-permute-done | bytes 524320 | tf_op jit(solution)/shard_map/ppermute | solution.py:42
  154.6 3.3 %shard_map.146 = bf16[256,1024]{1,0:T(8,128)(2,1)} custom-call(s32[1]{0:T(128)} %bitcast.10.refs_0_, bf16[128,1024]{1,0:T(8,128)(2,1)} %bitcast.95, bf16[128,1024]{1,0:T(8,128)(2,1)} %copy-done.11, bf16[256,1024]{1,0:T(8,128)(2,1)} %bitcast.27.refs_3_, bf16[2,256,1024]{2,1,0:T(8,128)(2,1)} %bitcast.23.refs_4_, bf16[2,256,1024]{2,1,0:T(8,128)(2,1)} %bitcast.24.refs_5_, ...), custom_call_target="tpu_custom_call" | custom-call | flops 536870912 | bytes 2097152 | tf_op jit(solution)/shard_map/pallas_call | solution.py:210
  163.3 3.4 %shard_map.145 = f32[256,1024]{1,0:T(8,128)} custom-call(s32[1]{0:T(128)} %bitcast.10.refs_0_, bf16[128,1024]{1,0:T(8,128)(2,1)} %bitcast.96, bf16[128,1024]{1,0:T(8,128)(2,1)} %copy-done.11, bf16[256,1024]{1,0:T(8,128)(2,1)} %bitcast.20.refs_3_, bf16[2,256,1024]{2,1,0:T(8,128)(2,1)} %bitcast.23.refs_4_, bf16[2,256,1024]{2,1,0:T(8,128)(2,1)} %bitcast.24.refs_5_, ...), custom_call_target="tpu_custom_call" | custom-call | flops 536870912 | bytes 2097152 | tf_op jit(solution)/shard_map/pallas_call | solution.py:210
  168.4 5.1 %collective-permute-start.11 = (bf16[256,1024]{1,0:T(8,128)(2,1)S(1)}, bf16[256,1024]{1,0:T(8,128)(2,1)S(1)}, u32[]{:S(2)}, u32[]{:S(2)}) collective-permute-start(bf16[256,1024]{1,0:T(8,128)(2,1)S(1)} %multiply_convert_fusion.refs_1_.refs_2_), channel_id=1, source_target_pairs={{0,1},{1,0},{2,3},{3,2},{4,5},{5,4},{6,7},{7,6},{8,9},{9,8},{10,11... | collective-permute-start | bytes 1572872 | tf_op jit(solution)/shard_map/ppermute | solution.py:102
  174.3 4.5 %shard_map.147.refs_2_ = f32[256,1024]{1,0:T(8,128)} custom-call(s32[1]{0:T(128)} %bitcast.10.refs_0_, bf16[256,1024]{1,0:T(8,128)(2,1)} %copy-done.3, bf16[256,1024]{1,0:T(8,128)(2,1)} %copy-done.3, bf16[256,1024]{1,0:T(8,128)(2,1)} %bitcast.32.refs_3_, bf16[2,256,1024]{2,1,0:T(8,128)(2,1)} %bitcast.91, bf16[2,256,1024]{2,1,0:T(8,128)(2,1)} %bitcast.93, ...), custom_call_target="tpu_custom_call" | custom-call | flops 536870912 | bytes 2097152 | tf_op jit(solution)/shard_map/pallas_call | solution.py:210
  179.6 4.5 %shard_map.148 = bf16[4,2,32,1024]{3,2,1,0:T(8,128)(2,1)} custom-call(s32[1]{0:T(128)} %bitcast.10.refs_0_, bf16[256,1024]{1,0:T(8,128)(2,1)} %copy-done.12, f32[256,1024]{1,0:T(8,128)} %shard_map.147.refs_2_, bf16[256,1024]{1,0:T(8,128)(2,1)} %bitcast.39.refs_3_, bf16[2,256,1024]{2,1,0:T(8,128)(2,1)} %bitcast.92, bf16[2,256,1024]{2,1,0:T(8,128)(2,1)} %bitcast.94, ...), custom_call_target="tpu_custom_call" | custom-call | flops 536870912 | bytes 2097152 | tf_op jit(solution)/shard_map/pallas_call | solution.py:210
  184.1 13.8 %all_to_all.35 = bf16[4,2,32,1024]{3,2,1,0:T(8,128)(2,1)S(1)} all-to-all(bf16[4,2,32,1024]{3,2,1,0:T(8,128)(2,1)} %shard_map.148), channel_id=1, replica_groups=mesh['rep'=2,'z'=8,'y'=4,'x'=4,'core'=2] {'x'}, dimensions={0} | all-to-all | bytes 1048576 | tf_op jit(solution)/shard_map/all_to_all | solution.py:24
  202.6 11.6 %all_to_all.36 = bf16[4,32,2048]{2,1,0:T(8,128)(2,1)S(1)} all-to-all(bf16[4,32,2048]{2,1,0:T(8,128)(2,1)S(1)} %broadcast_in_dim.17), channel_id=1, replica_groups=mesh['rep'=2,'z'=8,'y'=4,'x'=4,'core'=2] {'x'}, dimensions={0} | all-to-all | bytes 1048576 | tf_op jit(solution)/shard_map/all_to_all | solution.py:24
  214.2 3.1 %collective-permute-start.18 = (bf16[128,2048]{1,0:T(8,128)(2,1)S(1)}, bf16[128,2048]{1,0:T(8,128)(2,1)S(1)}, u32[]{:S(2)}, u32[]{:S(2)}) collective-permute-start(bf16[128,2048]{1,0:T(8,128)(2,1)S(1)} %bitcast.99), channel_id=1, source_target_pairs={{0,1},{1,0},{2,3},{3,2},{4,5},{5,4},{6,7},{7,6},{8,9},{9,8},{10,11... | collective-permute-start | bytes 1572872 | tf_op jit(solution)/shard_map/ppermute | solution.py:102
  (149 shorter events, 61.9 us)
Async XLA Ops:
  4.0 30.5 %all-to-all-start = ((bf16[8,64,384]{2,1,0:T(8,128)(2,1)}), bf16[8,64,384]{2,1,0:T(8,128)(2,1)S(1)}, u32[]{:S(2)}, u32[]{:S(2)}) async-start(bf16[8,64,384]{2,1,0:T(8,128)(2,1)} %broadcast_in_dim.12), calls=%async_computation | async-start | bytes 786432 | tf_op jit(solution)/shard_map/all_to_all | solution.py:24
  17.2 23.0 %collective-permute-start.2 = (bf16[64,2048]{1,0:T(8,128)(2,1)S(1)}, bf16[64,2048]{1,0:T(8,128)(2,1)S(1)}, u32[]{:S(2)}, u32[]{:S(2)}) collective-permute-start(bf16[64,2048]{1,0:T(8,128)(2,1)S(1)} %pad_maximum_fusion.5), channel_id=1, source_target_pairs={{8,0},{16,8},{24,16},{0,24},{9,1},{17,9},{25,17},{1,25},{10,2},{18... | collective-permute-start | bytes 786440 | tf_op jit(solution)/shard_map/ppermute | solution.py:35
  21.9 18.4 %collective-permute-start.3 = (bf16[64,2048]{1,0:T(8,128)(2,1)S(1)}, bf16[64,2048]{1,0:T(8,128)(2,1)S(1)}, u32[]{:S(2)}, u32[]{:S(2)}) collective-permute-start(bf16[64,2048]{1,0:T(8,128)(2,1)S(1)} %pad_maximum_fusion.5), channel_id=1, source_target_pairs={{16,0},{24,8},{0,16},{8,24},{17,1},{25,9},{1,17},{9,25},{18,2},{26... | collective-permute-start | bytes 786440 | tf_op jit(solution)/shard_map/ppermute | solution.py:35
  24.1 16.2 %collective-permute-start.4 = (bf16[64,2048]{1,0:T(8,128)(2,1)S(1)}, bf16[64,2048]{1,0:T(8,128)(2,1)S(1)}, u32[]{:S(2)}, u32[]{:S(2)}) collective-permute-start(bf16[64,2048]{1,0:T(8,128)(2,1)S(1)} %pad_maximum_fusion.5), channel_id=1, source_target_pairs={{24,0},{0,8},{8,16},{16,24},{25,1},{1,9},{9,17},{17,25},{26,2},{2,... | collective-permute-start | bytes 786440 | tf_op jit(solution)/shard_map/ppermute | solution.py:35
  35.9 17.9 %all-to-all-start.1 = ((bf16[4,8,64,384]{3,2,1,0:T(8,128)(2,1)}), bf16[4,8,64,384]{3,2,1,0:T(8,128)(2,1)S(1)}, u32[]{:S(2)}, u32[]{:S(2)}) async-start(bf16[4,8,64,384]{3,2,1,0:T(8,128)(2,1)} %broadcast_in_dim.13), calls=%async_computation.1 | async-start | bytes 3145728 | tf_op jit(solution)/shard_map/all_to_all | solution.py:24
  41.4 28.5 %collective-permute-start.5 = (bf16[4,64,1024]{2,1,0:T(8,128)(2,1)}, bf16[4,64,1024]{2,1,0:T(8,128)(2,1)}, u32[]{:S(2)}, u32[]{:S(2)}) collective-permute-start(bf16[4,64,1024]{2,1,0:T(8,128)(2,1)} %get-tuple-element.14), channel_id=1, source_target_pairs={{0,1},{1,0},{2,3},{3,2},{4,5},{5,4},{6,7},{7,6},{8,9},{9,8},{10,11... | collective-permute-start | bytes 1572872 | tf_op jit(solution)/shard_map/ppermute | solution.py:102
  51.3 32.6 %collective-permute-start.12 = (bf16[4,64,1024]{2,1,0:T(8,128)(2,1)}, bf16[4,64,1024]{2,1,0:T(8,128)(2,1)}, u32[]{:S(2)}, u32[]{:S(2)}) collective-permute-start(bf16[4,64,1024]{2,1,0:T(8,128)(2,1)} %get-tuple-element.12), channel_id=1, source_target_pairs={{0,1},{1,0},{2,3},{3,2},{4,5},{5,4},{6,7},{7,6},{8,9},{9,8},{10,11... | collective-permute-start | bytes 1572872 | tf_op jit(solution)/shard_map/ppermute | solution.py:102
  57.5 21.1 %all-to-all-start.2 = ((f32[8,2,256]{2,1,0:T(2,128)}), f32[8,2,256]{2,1,0:T(2,128)S(1)}, u32[]{:S(2)}, u32[]{:S(2)}) async-start(f32[8,2,256]{2,1,0:T(2,128)} %broadcast_in_dim.15), calls=%async_computation.2 | async-start | bytes 32768 | tf_op jit(solution)/shard_map/all_to_all | solution.py:24
  72.0 20.8 %collective-permute-start.6 = (bf16[2,4,64,1024]{3,2,1,0:T(8,128)(2,1)}, bf16[2,4,64,1024]{3,2,1,0:T(8,128)(2,1)}, u32[]{:S(2)}, u32[]{:S(2)}) collective-permute-start(bf16[2,4,64,1024]{3,2,1,0:T(8,128)(2,1)} %pad_maximum_fusion), channel_id=1, source_target_pairs={{32,0},{64,32},{96,64},{128,96},{160,128},{192,160},{224,192},{256... | collective-permute-start | bytes 3145736 | tf_op jit(solution)/shard_map/ppermute | solution.py:42
  80.0 14.8 %collective-permute-start = (bf16[128,2048]{1,0:T(8,128)(2,1)}, bf16[128,2048]{1,0:T(8,128)(2,1)S(1)}, u32[]{:S(2)}, u32[]{:S(2)}) collective-permute-start(bf16[128,2048]{1,0:T(8,128)(2,1)} %convolution_convert_fusion), channel_id=1, source_target_pairs={{0,1},{1,0},{2,3},{3,2},{4,5},{5,4},{6,7},{7,6},{8,9},{9,8},{10,11... | collective-permute-start | bytes 1572872 | tf_op jit(solution)/shard_map/ppermute | solution.py:102
  86.0 17.9 %collective-permute-start.13 = (bf16[2,4,64,1024]{3,2,1,0:T(8,128)(2,1)}, bf16[2,4,64,1024]{3,2,1,0:T(8,128)(2,1)S(1)}, u32[]{:S(2)}, u32[]{:S(2)}) collective-permute-start(bf16[2,4,64,1024]{3,2,1,0:T(8,128)(2,1)} %pad_maximum_fusion.1), channel_id=1, source_target_pairs={{32,0},{64,32},{96,64},{128,96},{160,128},{192,160},{224,192},{256... | collective-permute-start | bytes 3145736 | tf_op jit(solution)/shard_map/ppermute | solution.py:42
  92.8 22.5 %collective-permute-start.7 = (bf16[2,4,64,1024]{3,2,1,0:T(8,128)(2,1)}, bf16[2,4,64,1024]{3,2,1,0:T(8,128)(2,1)}, u32[]{:S(2)}, u32[]{:S(2)}) collective-permute-start(bf16[2,4,64,1024]{3,2,1,0:T(8,128)(2,1)} %collective-permute-done.6), channel_id=1, source_target_pairs={{32,0},{64,32},{96,64},{128,96},{160,128},{192,160},{224,192},{256... | collective-permute-start | bytes 3145736 | tf_op jit(solution)/shard_map/ppermute | solution.py:42
  95.9 21.4 %all-to-all-start.3 = ((bf16[4,32,2048]{2,1,0:T(8,128)(2,1)}), bf16[4,32,2048]{2,1,0:T(8,128)(2,1)}, u32[]{:S(2)}, u32[]{:S(2)}) async-start(bf16[4,32,2048]{2,1,0:T(8,128)(2,1)} %bitcast.9), calls=%async_computation.3 | async-start | bytes 1048576 | tf_op jit(solution)/shard_map/all_to_all | solution.py:24
  103.9 22.5 %collective-permute-start.14 = (bf16[2,4,64,1024]{3,2,1,0:T(8,128)(2,1)S(1)}, bf16[2,4,64,1024]{3,2,1,0:T(8,128)(2,1)S(1)}, u32[]{:S(2)}, u32[]{:S(2)}) collective-permute-start(bf16[2,4,64,1024]{3,2,1,0:T(8,128)(2,1)S(1)} %collective-permute-done.13), channel_id=1, source_target_pairs={{32,0},{64,32},{96,64},{128,96},{160,128},{192,160},{224,192},{256... | collective-permute-start | bytes 3145736 | tf_op jit(solution)/shard_map/ppermute | solution.py:42
  115.3 22.4 %collective-permute-start.8 = (bf16[2,4,64,1024]{3,2,1,0:T(8,128)(2,1)}, bf16[2,4,64,1024]{3,2,1,0:T(8,128)(2,1)S(1)}, u32[]{:S(2)}, u32[]{:S(2)}) collective-permute-start(bf16[2,4,64,1024]{3,2,1,0:T(8,128)(2,1)} %collective-permute-done.7), channel_id=1, source_target_pairs={{32,0},{64,32},{96,64},{128,96},{160,128},{192,160},{224,192},{256... | collective-permute-start | bytes 3145736 | tf_op jit(solution)/shard_map/ppermute | solution.py:42
  120.9 19.5 %all-to-all-start.4 = ((bf16[4,2,32,1024]{3,2,1,0:T(8,128)(2,1)}), bf16[4,2,32,1024]{3,2,1,0:T(8,128)(2,1)}, u32[]{:S(2)}, u32[]{:S(2)}) async-start(bf16[4,2,32,1024]{3,2,1,0:T(8,128)(2,1)} %broadcast_in_dim.16), calls=%async_computation.4 | async-start | bytes 1048576 | tf_op jit(solution)/shard_map/all_to_all | solution.py:24
  126.4 34.5 %collective-permute-start.15 = (bf16[2,4,64,1024]{3,2,1,0:T(8,128)(2,1)S(1)}, bf16[2,4,64,1024]{3,2,1,0:T(8,128)(2,1)S(1)}, u32[]{:S(2)}, u32[]{:S(2)}) collective-permute-start(bf16[2,4,64,1024]{3,2,1,0:T(8,128)(2,1)S(1)} %collective-permute-done.14), channel_id=1, source_target_pairs={{32,0},{64,32},{96,64},{128,96},{160,128},{192,160},{224,192},{256... | collective-permute-start | bytes 3145736 | tf_op jit(solution)/shard_map/ppermute | solution.py:42
  138.5 16.1 %collective-permute-start.9 = (bf16[2,2,64,1024]{3,2,1,0:T(8,128)(2,1)}, bf16[2,2,64,1024]{3,2,1,0:T(8,128)(2,1)}, u32[]{:S(2)}, u32[]{:S(2)}) collective-permute-start(bf16[2,2,64,1024]{3,2,1,0:T(8,128)(2,1)} %constant_dynamic-slice_fusion.1), channel_id=1, source_target_pairs={{32,0},{64,32},{96,64},{128,96},{160,128},{192,160},{224,192},{256... | collective-permute-start | bytes 1572872 | tf_op jit(solution)/shard_map/ppermute | solution.py:42
  142.3 7.1 %collective-permute-start.1 = (bf16[128,1024]{1,0:T(8,128)(2,1)S(1)}, bf16[128,1024]{1,0:T(8,128)(2,1)S(1)}, u32[]{:S(2)}, u32[]{:S(2)}) collective-permute-start(bf16[128,1024]{1,0:T(8,128)(2,1)S(1)} %bitcast.113), channel_id=1, source_target_pairs={{0,1},{1,0},{2,3},{3,2},{4,5},{5,4},{6,7},{7,6},{8,9},{9,8},{10,11... | collective-permute-start | bytes 786440 | tf_op jit(solution)/shard_map/ppermute | solution.py:102
  157.9 8.9 %collective-permute-start.10 = (bf16[256,1024]{1,0:T(8,128)(2,1)}, bf16[256,1024]{1,0:T(8,128)(2,1)}, u32[]{:S(2)}, u32[]{:S(2)}) collective-permute-start(bf16[256,1024]{1,0:T(8,128)(2,1)} %shard_map.146), channel_id=1, source_target_pairs={{0,1},{1,0},{2,3},{3,2},{4,5},{5,4},{6,7},{7,6},{8,9},{9,8},{10,11... | collective-permute-start | bytes 1572872 | tf_op jit(solution)/shard_map/ppermute | solution.py:102
  160.9 12.6 %collective-permute-start.16 = (bf16[2,2,64,1024]{3,2,1,0:T(8,128)(2,1)S(1)}, bf16[2,2,64,1024]{3,2,1,0:T(8,128)(2,1)S(1)}, u32[]{:S(2)}, u32[]{:S(2)}) collective-permute-start(bf16[2,2,64,1024]{3,2,1,0:T(8,128)(2,1)S(1)} %constant_dynamic-slice_fusion), channel_id=1, source_target_pairs={{32,0},{64,32},{96,64},{128,96},{160,128},{192,160},{224,192},{256... | collective-permute-start | bytes 1572872 | tf_op jit(solution)/shard_map/ppermute | solution.py:42
  168.4 10.4 %collective-permute-start.11 = (bf16[256,1024]{1,0:T(8,128)(2,1)S(1)}, bf16[256,1024]{1,0:T(8,128)(2,1)S(1)}, u32[]{:S(2)}, u32[]{:S(2)}) collective-permute-start(bf16[256,1024]{1,0:T(8,128)(2,1)S(1)} %multiply_convert_fusion.refs_1_.refs_2_), channel_id=1, source_target_pairs={{0,1},{1,0},{2,3},{3,2},{4,5},{5,4},{6,7},{7,6},{8,9},{9,8},{10,11... | collective-permute-start | bytes 1572872 | tf_op jit(solution)/shard_map/ppermute | solution.py:102
  198.0 3.9 %collective-permute-start.17 = (bf16[32,1024]{1,0:T(8,128)(2,1)S(1)}, bf16[32,1024]{1,0:T(8,128)(2,1)S(1)}, u32[]{:S(2)}, u32[]{:S(2)}) collective-permute-start(bf16[32,1024]{1,0:T(8,128)(2,1)S(1)} %fusion.30), channel_id=1, source_target_pairs={{0,1},{1,0},{2,3},{3,2},{4,5},{5,4},{6,7},{7,6},{8,9},{9,8},{10,11... | collective-permute-start | bytes 196616 | tf_op jit(solution)/shard_map/ppermute | solution.py:102
  214.2 4.6 %collective-permute-start.18 = (bf16[128,2048]{1,0:T(8,128)(2,1)S(1)}, bf16[128,2048]{1,0:T(8,128)(2,1)S(1)}, u32[]{:S(2)}, u32[]{:S(2)}) collective-permute-start(bf16[128,2048]{1,0:T(8,128)(2,1)S(1)} %bitcast.99), channel_id=1, source_target_pairs={{0,1},{1,0},{2,3},{3,2},{4,5},{5,4},{6,7},{7,6},{8,9},{9,8},{10,11... | collective-permute-start | bytes 1572872 | tf_op jit(solution)/shard_map/ppermute | solution.py:102
  (20 other events, 301.5 us)

commit v6 on v5

--- a/solution.py
+++ b/solution.py
@@ -159,40 +159,47 @@
 
 def fetch_side(slot, core, pieces, whole, sems):
     half = pieces[0].shape[0] // 2
-    sources = [pieces[0].at[pl.ds(core * half, half)]] + [p.at[slot] for p in pieces[1:]]
+    sources = [pieces[slot].at[pl.ds(core * half, half)]] + [p.at[slot] for p in pieces[2:]]
     at, copies = 0, []
     for i, source in enumerate(sources):
         n = source.shape[0]
-        copies.append(pltpu.make_async_copy(source, whole.at[pl.ds(at, n)], sems.at[i]))
+        copies.append(pltpu.make_async_copy(source, whole.at[slot, pl.ds(at, n)], sems.at[slot, i]))
         copies[-1].start()
         at += n
     return copies
 
 
-def up_body(slot, core_ref, own, theirs, *refs):
-    pieces, (out, x, w, x_sems, w_sems) = refs[:-5], refs[-5:]
+def up_body(core_ref, own, theirs, *refs):
+    pieces, (kept, sent, x, w, x_sems, w_sems) = refs[:-6], refs[-6:]
     core = core_ref[0]
     n = own.shape[0]
-    copies = [
+    first = [
         pltpu.make_async_copy(own, x.at[pl.ds(core * n, n)], x_sems.at[0]),
         pltpu.make_async_copy(theirs, x.at[pl.ds((1 - core) * n, n)], x_sems.at[1]),
     ]
-    for copy in copies:
+    for copy in first:
         copy.start()
-    for copy in copies + fetch_side(slot, core, pieces, w, w_sems):
+    first += fetch_side(1, core, pieces, w, w_sems)
+    second = fetch_side(0, core, pieces, w, w_sems)
+    for copy in first:
         copy.wait()
-    out[...] = jnp.dot(x[...], w[...], preferred_element_type=F32).astype(out.dtype)
-
-
-def down_body(slot, core_ref, hidden, acc, *refs):
+    sent[...] = jnp.dot(x[...], w[1], preferred_element_type=F32).astype(sent.dtype)
+    for copy in second:
+        copy.wait()
+    kept[...] = jnp.dot(x[...], w[0], preferred_element_type=F32)
+
+
+def down_body(core_ref, hidden, other, *refs):
     pieces, (out, w, w_sems) = refs[:-3], refs[-3:]
-    for copy in fetch_side(slot, core_ref[0], pieces, w, w_sems):
+    core = core_ref[0]
+    first = fetch_side(0, core, pieces, w, w_sems)
+    second = fetch_side(1, core, pieces, w, w_sems)
+    for copy in first:
         copy.wait()
-    part = dot_t(hidden[...], w[...])
-    if slot == 0:
-        out[...] = part
-        return
-    part = (part + acc[...]).astype(out.dtype)
+    part = dot_t(hidden[...], w[0])
+    for copy in second:
+        copy.wait()
+    part = (part + dot_t(other[...], w[1])).astype(out.dtype)
     blocks, halves, n, _ = out.shape
     for i in range(blocks):
         for j in range(halves):
@@ -200,42 +207,39 @@
             out[i, j] = part[at : at + n]
 
 
-def side_call(body, name, slot, core, operands, pieces, out_shape, scratch):
+def side_call(body, core, operands, where, pieces, out_shape, scratch, more):
     anywhere = pl.BlockSpec(memory_space=pl.ANY)
     inside = pl.BlockSpec(memory_space=pltpu.VMEM)
-    pieces = [pieces[slot]] + pieces[2:]
-    here = anywhere if name == "up" else inside
-    cols = pieces[0].shape[1]
-    rows = 4 * pieces[0].shape[0]
+    rows, cols = 4 * pieces[0].shape[0], pieces[0].shape[1]
     return pl.pallas_call(
-        lambda *refs: body(slot, *refs),
-        in_specs=[pl.BlockSpec(memory_space=pltpu.SMEM)] + [here] * len(operands) + [anywhere] * len(pieces),
-        out_specs=inside,
+        body,
+        in_specs=[pl.BlockSpec(memory_space=pltpu.SMEM)] + [where] * len(operands) + [anywhere] * len(pieces),
+        out_specs=jax.tree.map(lambda _: inside, out_shape),
         out_shape=out_shape,
-        scratch_shapes=scratch + [pltpu.VMEM((rows, cols), BF16)]
-        + ([pltpu.SemaphoreType.DMA((2,))] if name == "up" else [])
-        + [pltpu.SemaphoreType.DMA((len(pieces),))],
-        cost_estimate=pl.CostEstimate(flops=512 * rows * cols, bytes_accessed=2 * rows * cols, transcendentals=0),
+        scratch_shapes=scratch
+        + [pltpu.VMEM((2, rows, cols), BF16)]
+        + more
+        + [pltpu.SemaphoreType.DMA((2, len(pieces) - 1))],
+        cost_estimate=pl.CostEstimate(flops=1024 * rows * cols, bytes_accessed=4 * rows * cols, transcendentals=0),
+        compiler_params=pltpu.CompilerParams(vmem_limit_bytes=52 * 2**20),
     )(core.reshape(1), *operands, *pieces)
 
 
 def ffn(own, theirs, core, scale, ups, downs):
     tokens, cols = 2 * own.shape[0], own.shape[1]
     hid = scale.shape[0]
-    up = lambda slot, kind: side_call(
-        up_body, "up", slot, core, (own, theirs), ups,
-        jax.ShapeDtypeStruct((tokens, hid), kind), [pltpu.VMEM((tokens, cols), BF16)],
-    )
-    sent = swapped(up(1, BF16))
-    up_sum = up(0, F32) + sent.astype(F32)
+    anywhere = pl.BlockSpec(memory_space=pl.ANY)
+    inside = pl.BlockSpec(memory_space=pltpu.VMEM)
+    shapes = [jax.ShapeDtypeStruct((tokens, hid), F32), jax.ShapeDtypeStruct((tokens, hid), BF16)]
+    kept, sent = side_call(
+        up_body, core, (own, theirs), anywhere, ups, shapes,
+        [pltpu.VMEM((tokens, cols), BF16)], [pltpu.SemaphoreType.DMA((2,))],
+    )
+    up_sum = kept + swapped(sent).astype(F32)
     hidden = jnp.square(jax.nn.relu(up_sum * scale)).astype(BF16)
-    other = swapped(hidden)
-    kept = side_call(
-        down_body, "down", 0, core, (hidden, hidden), downs, jax.ShapeDtypeStruct((tokens, cols), F32), []
-    )
     n = lax.axis_size("x")
     blocks = jax.ShapeDtypeStruct((n, 2, tokens // (2 * n), cols), BF16)
-    return side_call(down_body, "down", 1, core, (other, kept), downs, blocks, [])
+    return side_call(down_body, core, (hidden, swapped(hidden)), inside, downs, blocks, [], [])
 
 
 def on_device(

time: 222 us -> 215 us (0.968)
  Pallas kernels: 15.6 us -> 7.57 us
  waiting for transfers between devices: 45.3 us -> 51 us
  other arithmetic: 17.1 us -> 14.5 us
    pallas_call x4 -> x2, Pallas kernels: 15.6 us -> 7.57 us  [side_call(): pl.pallas_call(body, in_specs=[pl.BlockSpec(memory_space=pltpu.SMEM)] + [...]
    ppermute x8, waiting for transfers between devices: 33.9 us -> 40.7 us  [hop(): return lax.ppermute(x, (*RING, 'core'), pairs)]
    all_to_all x5, starting transfers between devices: 38.1 us -> 34.9 us  [exchange(): return lax.all_to_all(x, axis, split_axis=0, concat_axis=0, tiled=True)]
    another operation x3, local copies, waits for them, and re-layouts: 0.06 us -> 2.96 us  [on_device(): jnp.stack([b[:, hid:] for b in near])]
  transfers between devices with their start and end apart: 24 -> 24, of which waited for: 11 -> 11; matrix products, arithmetic and copies ran while one was open for 10% -> 10% of each run, Pallas kernels for 5% -> 2%
where the time goes in v6:
time: 215 us; the launch traced here: 213 us
  starting transfers between devices  100 us (47%)
  waiting for transfers between devices  51 us (24%)
  blocking collectives  24.5 us (11%)
  other arithmetic  14.5 us (7%)
  local copies, waits for them, and re-layouts  10.6 us (5%)
  Pallas kernels  7.57 us (4%)
  matrix products  4.29 us (2%)
    ppermute x8, waiting for transfers between devices, hop(): return lax.ppermute(x, (*RING, 'core'), pairs)  40.7 us
    ppermute x8, starting transfers between devices, swapped(): return lax.ppermute(x, 'core', [(0, 1), (1, 0)])  35.1 us
    all_to_all x5, starting transfers between devices, exchange(): return lax.all_to_all(x, axis, split_axis=0, concat_axis=0, tiled=True)  34.9 us
    all_to_all x2, blocking collectives, exchange(): return lax.all_to_all(x, axis, split_axis=0, concat_axis=0, tiled=True)  24.5 us
    ppermute x8, starting transfers between devices, hop(): return lax.ppermute(x, (*RING, 'core'), pairs)  20.6 us
    ppermute x3, starting transfers between devices, y_ring(): others[d] = lax.ppermute(block, 'y', [((i + d) % n, i) for i in range(n)])  9.5 us
    pallas_call x2, Pallas kernels, side_call(): pl.pallas_call(body, in_specs=[pl.BlockSpec(memory_space=pltpu.SMEM)] + [...  7.57 us
    all_to_all x5, waiting for transfers between devices, exchange(): return lax.all_to_all(x, axis, split_axis=0, concat_axis=0, tiled=True)  6.84 us
  transfers between devices with their start and end apart: 24, of which 11 were waited for; matrix products, arithmetic and copies ran while one was open for 10% of the time, Pallas kernels for 2%

profile of v6, /device:TPU:1, one launch (start us, length us, event | category | flops | bytes accessed | tf_op | source)
XLA Modules:
  0.0 213.5 jit_solution(5802700955246484044)
XLA Ops:
  4.0 13.1 %all-to-all-start = ((bf16[8,64,384]{2,1,0:T(8,128)(2,1)}), bf16[8,64,384]{2,1,0:T(8,128)(2,1)S(1)}, u32[]{:S(2)}, u32[]{:S(2)}) async-start(bf16[8,64,384]{2,1,0:T(8,128)(2,1)} %broadcast_in_dim.12), calls=%async_computation | async-start | bytes 786432 | tf_op jit(solution)/shard_map/all_to_all | solution.py:24
  17.2 4.6 %collective-permute-start.2 = (bf16[64,2048]{1,0:T(8,128)(2,1)S(1)}, bf16[64,2048]{1,0:T(8,128)(2,1)}, u32[]{:S(2)}, u32[]{:S(2)}) collective-permute-start(bf16[64,2048]{1,0:T(8,128)(2,1)S(1)} %pad_maximum_fusion.5), channel_id=1, source_target_pairs={{8,0},{16,8},{24,16},{0,24},{9,1},{17,9},{25,17},{1,25},{10,2},{18... | collective-permute-start | bytes 786440 | tf_op jit(solution)/shard_map/ppermute | solution.py:35
  27.6 6.8 %all-to-all-done = bf16[8,64,384]{2,1,0:T(8,128)(2,1)S(1)} async-done(((bf16[8,64,384]{2,1,0:T(8,128)(2,1)}), bf16[8,64,384]{2,1,0:T(8,128)(2,1)S(1)}, u32[]{:S(2)}, u32[]{:S(2)}) %all-to-all-start) | async-done | bytes 393248 | tf_op jit(solution)/shard_map/all_to_all | solution.py:24
  35.9 4.3 %all-to-all-start.1 = ((bf16[4,8,64,384]{3,2,1,0:T(8,128)(2,1)}), bf16[4,8,64,384]{3,2,1,0:T(8,128)(2,1)S(1)}, u32[]{:S(2)}, u32[]{:S(2)}) async-start(bf16[4,8,64,384]{3,2,1,0:T(8,128)(2,1)} %broadcast_in_dim.13), calls=%async_computation.1 | async-start | bytes 3145728 | tf_op jit(solution)/shard_map/all_to_all | solution.py:24
  45.3 8.8 %collective-permute-start.5 = (bf16[4,64,1024]{2,1,0:T(8,128)(2,1)S(1)}, bf16[4,64,1024]{2,1,0:T(8,128)(2,1)}, u32[]{:S(2)}, u32[]{:S(2)}) collective-permute-start(bf16[4,64,1024]{2,1,0:T(8,128)(2,1)S(1)} %get-tuple-element.18), channel_id=1, source_target_pairs={{0,1},{1,0},{2,3},{3,2},{4,5},{5,4},{6,7},{7,6},{8,9},{9,8},{10,11... | collective-permute-start | bytes 1572872 | tf_op jit(solution)/shard_map/ppermute | solution.py:102
  60.9 9.1 %all-to-all-start.2 = ((f32[8,2,256]{2,1,0:T(2,128)}), f32[8,2,256]{2,1,0:T(2,128)S(1)}, u32[]{:S(2)}, u32[]{:S(2)}) async-start(f32[8,2,256]{2,1,0:T(2,128)} %broadcast_in_dim.15), calls=%async_computation.2 | async-start | bytes 32768 | tf_op jit(solution)/shard_map/all_to_all | solution.py:24
  72.4 6.5 %collective-permute-start.6 = (bf16[2,4,64,1024]{3,2,1,0:T(8,128)(2,1)}, bf16[2,4,64,1024]{3,2,1,0:T(8,128)(2,1)}, u32[]{:S(2)}, u32[]{:S(2)}) collective-permute-start(bf16[2,4,64,1024]{3,2,1,0:T(8,128)(2,1)} %pad_maximum_fusion), channel_id=1, source_target_pairs={{32,0},{64,32},{96,64},{128,96},{160,128},{192,160},{224,192},{256... | collective-permute-start | bytes 3145736 | tf_op jit(solution)/shard_map/ppermute | solution.py:42
  80.4 3.9 %collective-permute-start = (bf16[128,2048]{1,0:T(8,128)(2,1)}, bf16[128,2048]{1,0:T(8,128)(2,1)}, u32[]{:S(2)}, u32[]{:S(2)}) collective-permute-start(bf16[128,2048]{1,0:T(8,128)(2,1)} %convolution_convert_fusion), channel_id=1, source_target_pairs={{0,1},{1,0},{2,3},{3,2},{4,5},{5,4},{6,7},{7,6},{8,9},{9,8},{10,11... | collective-permute-start | bytes 1572872 | tf_op jit(solution)/shard_map/ppermute | solution.py:102
  87.3 5.8 %collective-permute-done.6 = bf16[2,4,64,1024]{3,2,1,0:T(8,128)(2,1)} collective-permute-done((bf16[2,4,64,1024]{3,2,1,0:T(8,128)(2,1)}, bf16[2,4,64,1024]{3,2,1,0:T(8,128)(2,1)}, u32[]{:S(2)}, u32[]{:S(2)}) %collective-permute-start.6) | collective-permute-done | bytes 1048608 | tf_op jit(solution)/shard_map/ppermute | solution.py:42
  97.2 4.3 %all-to-all-start.3 = ((bf16[4,32,2048]{2,1,0:T(8,128)(2,1)}), bf16[4,32,2048]{2,1,0:T(8,128)(2,1)S(1)}, u32[]{:S(2)}, u32[]{:S(2)}) async-start(bf16[4,32,2048]{2,1,0:T(8,128)(2,1)} %bitcast.9), calls=%async_computation.3 | async-start | bytes 1048576 | tf_op jit(solution)/shard_map/all_to_all | solution.py:24
  101.5 2.9 %collective-permute-done.13 = bf16[2,4,64,1024]{3,2,1,0:T(8,128)(2,1)} collective-permute-done((bf16[2,4,64,1024]{3,2,1,0:T(8,128)(2,1)}, bf16[2,4,64,1024]{3,2,1,0:T(8,128)(2,1)}, u32[]{:S(2)}, u32[]{:S(2)}) %collective-permute-start.13) | collective-permute-done | bytes 1048608 | tf_op jit(solution)/shard_map/ppermute | solution.py:42
  106.3 9.3 %collective-permute-done.7 = bf16[2,4,64,1024]{3,2,1,0:T(8,128)(2,1)} collective-permute-done((bf16[2,4,64,1024]{3,2,1,0:T(8,128)(2,1)}, bf16[2,4,64,1024]{3,2,1,0:T(8,128)(2,1)}, u32[]{:S(2)}, u32[]{:S(2)}) %collective-permute-start.7) | collective-permute-done | bytes 1048608 | tf_op jit(solution)/shard_map/ppermute | solution.py:42
  120.2 4.1 %all-to-all-start.4 = ((bf16[4,2,32,1024]{3,2,1,0:T(8,128)(2,1)}), bf16[4,2,32,1024]{3,2,1,0:T(8,128)(2,1)S(1)}, u32[]{:S(2)}, u32[]{:S(2)}) async-start(bf16[4,2,32,1024]{3,2,1,0:T(8,128)(2,1)} %broadcast_in_dim.16), calls=%async_computation.4 | async-start | bytes 1048576 | tf_op jit(solution)/shard_map/all_to_all | solution.py:24
  128.8 9.2 %collective-permute-done.8 = bf16[2,4,64,1024]{3,2,1,0:T(8,128)(2,1)S(1)} collective-permute-done((bf16[2,4,64,1024]{3,2,1,0:T(8,128)(2,1)}, bf16[2,4,64,1024]{3,2,1,0:T(8,128)(2,1)S(1)}, u32[]{:S(2)}, u32[]{:S(2)}) %collective-permute-start.8) | collective-permute-done | bytes 1048608 | tf_op jit(solution)/shard_map/ppermute | solution.py:42
  140.8 6.0 %collective-permute-start.1 = (bf16[128,1024]{1,0:T(8,128)(2,1)S(1)}, bf16[128,1024]{1,0:T(8,128)(2,1)S(1)}, u32[]{:S(2)}, u32[]{:S(2)}) collective-permute-start(bf16[128,1024]{1,0:T(8,128)(2,1)S(1)} %bitcast.109), channel_id=1, source_target_pairs={{0,1},{1,0},{2,3},{3,2},{4,5},{5,4},{6,7},{7,6},{8,9},{9,8},{10,11... | collective-permute-start | bytes 786440 | tf_op jit(solution)/shard_map/ppermute | solution.py:102
  147.9 7.0 %collective-permute-done.9 = bf16[2,2,64,1024]{3,2,1,0:T(8,128)(2,1)} collective-permute-done((bf16[2,2,64,1024]{3,2,1,0:T(8,128)(2,1)}, bf16[2,2,64,1024]{3,2,1,0:T(8,128)(2,1)}, u32[]{:S(2)}, u32[]{:S(2)}) %collective-permute-start.9) | collective-permute-done | bytes 524320 | tf_op jit(solution)/shard_map/ppermute | solution.py:42
  154.9 4.1 %shard_map.145 = (f32[256,1024]{1,0:T(8,128)}, bf16[256,1024]{1,0:T(8,128)(2,1)S(1)}) custom-call(s32[1]{0:T(128)} %bitcast.10.core_ref, bf16[128,1024]{1,0:T(8,128)(2,1)S(1)} %bitcast.85, bf16[128,1024]{1,0:T(8,128)(2,1)S(1)} %collective-permute-done.1.theirs, bf16[256,1024]{1,0:T(8,128)(2,1)S(1)} %bitcast.84, bf16[256,1024]{1,0:T(8,128)(2,1)} %bitcast.21.refs_1_, ...), custom_call_target="tpu_custom_call" | custom-call | flops 1073741824 | bytes 4194304 | tf_op jit(solution)/shard_map/pallas_call | solution.py:214
  164.2 5.1 %collective-permute-start.11 = (bf16[256,1024]{1,0:T(8,128)(2,1)S(1)}, bf16[256,1024]{1,0:T(8,128)(2,1)S(1)}, u32[]{:S(2)}, u32[]{:S(2)}) collective-permute-start(bf16[256,1024]{1,0:T(8,128)(2,1)S(1)} %multiply_convert_fusion.hidden), channel_id=1, source_target_pairs={{0,1},{1,0},{2,3},{3,2},{4,5},{5,4},{6,7},{7,6},{8,9},{9,8},{10,11... | collective-permute-start | bytes 1572872 | tf_op jit(solution)/shard_map/ppermute | solution.py:102
  169.3 4.1 %collective-permute-done.16 = bf16[2,2,64,1024]{3,2,1,0:T(8,128)(2,1)S(1)} collective-permute-done((bf16[2,2,64,1024]{3,2,1,0:T(8,128)(2,1)S(1)}, bf16[2,2,64,1024]{3,2,1,0:T(8,128)(2,1)S(1)}, u32[]{:S(2)}, u32[]{:S(2)}) %collective-permute-start.16) | collective-permute-done | bytes 524320 | tf_op jit(solution)/shard_map/ppermute | solution.py:42
  174.2 3.5 %shard_map.146 = bf16[4,2,32,1024]{3,2,1,0:T(8,128)(2,1)S(1)} custom-call(s32[1]{0:T(128)} %bitcast.10.core_ref, bf16[256,1024]{1,0:T(8,128)(2,1)S(1)} %multiply_convert_fusion.hidden, bf16[256,1024]{1,0:T(8,128)(2,1)S(1)} %collective-permute-done.11.other, bf16[256,1024]{1,0:T(8,128)(2,1)} %bitcast.91, bf16[256,1024]{1,0:T(8,128)(2,1)} %bitcast.94, ...), custom_call_target="tpu_custom_call" | custom-call | flops 1073741824 | bytes 4194304 | tf_op jit(solution)/shard_map/pallas_call | solution.py:214
  177.7 12.9 %all_to_all.35 = bf16[4,2,32,1024]{3,2,1,0:T(8,128)(2,1)S(1)} all-to-all(bf16[4,2,32,1024]{3,2,1,0:T(8,128)(2,1)S(1)} %shard_map.146), channel_id=1, replica_groups=mesh['rep'=2,'z'=8,'y'=4,'x'=4,'core'=2] {'x'}, dimensions={0} | all-to-all | bytes 1048576 | tf_op jit(solution)/shard_map/all_to_all | solution.py:24
  190.8 3.8 %collective-permute-start.17 = (bf16[32,1024]{1,0:T(8,128)(2,1)S(1)}, bf16[32,1024]{1,0:T(8,128)(2,1)S(1)}, u32[]{:S(2)}, u32[]{:S(2)}) collective-permute-start(bf16[32,1024]{1,0:T(8,128)(2,1)S(1)} %fusion.30), channel_id=1, source_target_pairs={{0,1},{1,0},{2,3},{3,2},{4,5},{5,4},{6,7},{7,6},{8,9},{9,8},{10,11... | collective-permute-start | bytes 196616 | tf_op jit(solution)/shard_map/ppermute | solution.py:102
  196.0 11.6 %all_to_all.36 = bf16[4,32,2048]{2,1,0:T(8,128)(2,1)S(1)} all-to-all(bf16[4,32,2048]{2,1,0:T(8,128)(2,1)S(1)} %broadcast_in_dim.17), channel_id=1, replica_groups=mesh['rep'=2,'z'=8,'y'=4,'x'=4,'core'=2] {'x'}, dimensions={0} | all-to-all | bytes 1048576 | tf_op jit(solution)/shard_map/all_to_all | solution.py:24
  207.7 3.1 %collective-permute-start.18 = (bf16[128,2048]{1,0:T(8,128)(2,1)S(1)}, bf16[128,2048]{1,0:T(8,128)(2,1)S(1)}, u32[]{:S(2)}, u32[]{:S(2)}) collective-permute-start(bf16[128,2048]{1,0:T(8,128)(2,1)S(1)} %bitcast.92), channel_id=1, source_target_pairs={{0,1},{1,0},{2,3},{3,2},{4,5},{5,4},{6,7},{7,6},{8,9},{9,8},{10,11... | collective-permute-start | bytes 1572872 | tf_op jit(solution)/shard_map/ppermute | solution.py:102
  (157 shorter events, 58.8 us)
Async XLA Ops:
  4.0 30.5 %all-to-all-start = ((bf16[8,64,384]{2,1,0:T(8,128)(2,1)}), bf16[8,64,384]{2,1,0:T(8,128)(2,1)S(1)}, u32[]{:S(2)}, u32[]{:S(2)}) async-start(bf16[8,64,384]{2,1,0:T(8,128)(2,1)} %broadcast_in_dim.12), calls=%async_computation | async-start | bytes 786432 | tf_op jit(solution)/shard_map/all_to_all | solution.py:24
  17.2 24.2 %collective-permute-start.2 = (bf16[64,2048]{1,0:T(8,128)(2,1)S(1)}, bf16[64,2048]{1,0:T(8,128)(2,1)}, u32[]{:S(2)}, u32[]{:S(2)}) collective-permute-start(bf16[64,2048]{1,0:T(8,128)(2,1)S(1)} %pad_maximum_fusion.5), channel_id=1, source_target_pairs={{8,0},{16,8},{24,16},{0,24},{9,1},{17,9},{25,17},{1,25},{10,2},{18... | collective-permute-start | bytes 786440 | tf_op jit(solution)/shard_map/ppermute | solution.py:35
  21.9 20.5 %collective-permute-start.3 = (bf16[64,2048]{1,0:T(8,128)(2,1)S(1)}, bf16[64,2048]{1,0:T(8,128)(2,1)}, u32[]{:S(2)}, u32[]{:S(2)}) collective-permute-start(bf16[64,2048]{1,0:T(8,128)(2,1)S(1)} %pad_maximum_fusion.5), channel_id=1, source_target_pairs={{16,0},{24,8},{0,16},{8,24},{17,1},{25,9},{1,17},{9,25},{18,2},{26... | collective-permute-start | bytes 786440 | tf_op jit(solution)/shard_map/ppermute | solution.py:35
  24.1 19.3 %collective-permute-start.4 = (bf16[64,2048]{1,0:T(8,128)(2,1)S(1)}, bf16[64,2048]{1,0:T(8,128)(2,1)}, u32[]{:S(2)}, u32[]{:S(2)}) collective-permute-start(bf16[64,2048]{1,0:T(8,128)(2,1)S(1)} %pad_maximum_fusion.5), channel_id=1, source_target_pairs={{24,0},{0,8},{8,16},{16,24},{25,1},{1,9},{9,17},{17,25},{26,2},{2,... | collective-permute-start | bytes 786440 | tf_op jit(solution)/shard_map/ppermute | solution.py:35
  35.9 21.1 %all-to-all-start.1 = ((bf16[4,8,64,384]{3,2,1,0:T(8,128)(2,1)}), bf16[4,8,64,384]{3,2,1,0:T(8,128)(2,1)S(1)}, u32[]{:S(2)}, u32[]{:S(2)}) async-start(bf16[4,8,64,384]{3,2,1,0:T(8,128)(2,1)} %broadcast_in_dim.13), calls=%async_computation.1 | async-start | bytes 3145728 | tf_op jit(solution)/shard_map/all_to_all | solution.py:24
  45.3 24.8 %collective-permute-start.5 = (bf16[4,64,1024]{2,1,0:T(8,128)(2,1)S(1)}, bf16[4,64,1024]{2,1,0:T(8,128)(2,1)}, u32[]{:S(2)}, u32[]{:S(2)}) collective-permute-start(bf16[4,64,1024]{2,1,0:T(8,128)(2,1)S(1)} %get-tuple-element.18), channel_id=1, source_target_pairs={{0,1},{1,0},{2,3},{3,2},{4,5},{5,4},{6,7},{7,6},{8,9},{9,8},{10,11... | collective-permute-start | bytes 1572872 | tf_op jit(solution)/shard_map/ppermute | solution.py:102
  55.0 29.3 %collective-permute-start.12 = (bf16[4,64,1024]{2,1,0:T(8,128)(2,1)S(1)}, bf16[4,64,1024]{2,1,0:T(8,128)(2,1)S(1)}, u32[]{:S(2)}, u32[]{:S(2)}) collective-permute-start(bf16[4,64,1024]{2,1,0:T(8,128)(2,1)S(1)} %get-tuple-element.16), channel_id=1, source_target_pairs={{0,1},{1,0},{2,3},{3,2},{4,5},{5,4},{6,7},{7,6},{8,9},{9,8},{10,11... | collective-permute-start | bytes 1572872 | tf_op jit(solution)/shard_map/ppermute | solution.py:102
  60.9 18.0 %all-to-all-start.2 = ((f32[8,2,256]{2,1,0:T(2,128)}), f32[8,2,256]{2,1,0:T(2,128)S(1)}, u32[]{:S(2)}, u32[]{:S(2)}) async-start(f32[8,2,256]{2,1,0:T(2,128)} %broadcast_in_dim.15), calls=%async_computation.2 | async-start | bytes 32768 | tf_op jit(solution)/shard_map/all_to_all | solution.py:24
  72.4 20.7 %collective-permute-start.6 = (bf16[2,4,64,1024]{3,2,1,0:T(8,128)(2,1)}, bf16[2,4,64,1024]{3,2,1,0:T(8,128)(2,1)}, u32[]{:S(2)}, u32[]{:S(2)}) collective-permute-start(bf16[2,4,64,1024]{3,2,1,0:T(8,128)(2,1)} %pad_maximum_fusion), channel_id=1, source_target_pairs={{32,0},{64,32},{96,64},{128,96},{160,128},{192,160},{224,192},{256... | collective-permute-start | bytes 3145736 | tf_op jit(solution)/shard_map/ppermute | solution.py:42
  80.4 14.7 %collective-permute-start = (bf16[128,2048]{1,0:T(8,128)(2,1)}, bf16[128,2048]{1,0:T(8,128)(2,1)}, u32[]{:S(2)}, u32[]{:S(2)}) collective-permute-start(bf16[128,2048]{1,0:T(8,128)(2,1)} %convolution_convert_fusion), channel_id=1, source_target_pairs={{0,1},{1,0},{2,3},{3,2},{4,5},{5,4},{6,7},{7,6},{8,9},{9,8},{10,11... | collective-permute-start | bytes 1572872 | tf_op jit(solution)/shard_map/ppermute | solution.py:102
  85.4 18.9 %collective-permute-start.13 = (bf16[2,4,64,1024]{3,2,1,0:T(8,128)(2,1)}, bf16[2,4,64,1024]{3,2,1,0:T(8,128)(2,1)}, u32[]{:S(2)}, u32[]{:S(2)}) collective-permute-start(bf16[2,4,64,1024]{3,2,1,0:T(8,128)(2,1)} %pad_maximum_fusion.1), channel_id=1, source_target_pairs={{32,0},{64,32},{96,64},{128,96},{160,128},{192,160},{224,192},{256... | collective-permute-start | bytes 3145736 | tf_op jit(solution)/shard_map/ppermute | solution.py:42
  93.1 22.5 %collective-permute-start.7 = (bf16[2,4,64,1024]{3,2,1,0:T(8,128)(2,1)}, bf16[2,4,64,1024]{3,2,1,0:T(8,128)(2,1)}, u32[]{:S(2)}, u32[]{:S(2)}) collective-permute-start(bf16[2,4,64,1024]{3,2,1,0:T(8,128)(2,1)} %collective-permute-done.6), channel_id=1, source_target_pairs={{32,0},{64,32},{96,64},{128,96},{160,128},{192,160},{224,192},{256... | collective-permute-start | bytes 3145736 | tf_op jit(solution)/shard_map/ppermute | solution.py:42
  97.2 20.3 %all-to-all-start.3 = ((bf16[4,32,2048]{2,1,0:T(8,128)(2,1)}), bf16[4,32,2048]{2,1,0:T(8,128)(2,1)S(1)}, u32[]{:S(2)}, u32[]{:S(2)}) async-start(bf16[4,32,2048]{2,1,0:T(8,128)(2,1)} %bitcast.9), calls=%async_computation.3 | async-start | bytes 1048576 | tf_op jit(solution)/shard_map/all_to_all | solution.py:24
  104.3 22.5 %collective-permute-start.14 = (bf16[2,4,64,1024]{3,2,1,0:T(8,128)(2,1)}, bf16[2,4,64,1024]{3,2,1,0:T(8,128)(2,1)}, u32[]{:S(2)}, u32[]{:S(2)}) collective-permute-start(bf16[2,4,64,1024]{3,2,1,0:T(8,128)(2,1)} %collective-permute-done.13), channel_id=1, source_target_pairs={{32,0},{64,32},{96,64},{128,96},{160,128},{192,160},{224,192},{256... | collective-permute-start | bytes 3145736 | tf_op jit(solution)/shard_map/ppermute | solution.py:42
  115.6 22.4 %collective-permute-start.8 = (bf16[2,4,64,1024]{3,2,1,0:T(8,128)(2,1)}, bf16[2,4,64,1024]{3,2,1,0:T(8,128)(2,1)S(1)}, u32[]{:S(2)}, u32[]{:S(2)}) collective-permute-start(bf16[2,4,64,1024]{3,2,1,0:T(8,128)(2,1)} %collective-permute-done.7), channel_id=1, source_target_pairs={{32,0},{64,32},{96,64},{128,96},{160,128},{192,160},{224,192},{256... | collective-permute-start | bytes 3145736 | tf_op jit(solution)/shard_map/ppermute | solution.py:42
  120.2 20.6 %all-to-all-start.4 = ((bf16[4,2,32,1024]{3,2,1,0:T(8,128)(2,1)}), bf16[4,2,32,1024]{3,2,1,0:T(8,128)(2,1)S(1)}, u32[]{:S(2)}, u32[]{:S(2)}) async-start(bf16[4,2,32,1024]{3,2,1,0:T(8,128)(2,1)} %broadcast_in_dim.16), calls=%async_computation.4 | async-start | bytes 1048576 | tf_op jit(solution)/shard_map/all_to_all | solution.py:24
  126.8 34.7 %collective-permute-start.15 = (bf16[2,4,64,1024]{3,2,1,0:T(8,128)(2,1)}, bf16[2,4,64,1024]{3,2,1,0:T(8,128)(2,1)S(1)}, u32[]{:S(2)}, u32[]{:S(2)}) collective-permute-start(bf16[2,4,64,1024]{3,2,1,0:T(8,128)(2,1)} %collective-permute-done.14), channel_id=1, source_target_pairs={{32,0},{64,32},{96,64},{128,96},{160,128},{192,160},{224,192},{256... | collective-permute-start | bytes 3145736 | tf_op jit(solution)/shard_map/ppermute | solution.py:42
  138.8 16.1 %collective-permute-start.9 = (bf16[2,2,64,1024]{3,2,1,0:T(8,128)(2,1)}, bf16[2,2,64,1024]{3,2,1,0:T(8,128)(2,1)}, u32[]{:S(2)}, u32[]{:S(2)}) collective-permute-start(bf16[2,2,64,1024]{3,2,1,0:T(8,128)(2,1)} %constant_dynamic-slice_fusion.1), channel_id=1, source_target_pairs={{32,0},{64,32},{96,64},{128,96},{160,128},{192,160},{224,192},{256... | collective-permute-start | bytes 1572872 | tf_op jit(solution)/shard_map/ppermute | solution.py:42
  140.8 7.1 %collective-permute-start.1 = (bf16[128,1024]{1,0:T(8,128)(2,1)S(1)}, bf16[128,1024]{1,0:T(8,128)(2,1)S(1)}, u32[]{:S(2)}, u32[]{:S(2)}) collective-permute-start(bf16[128,1024]{1,0:T(8,128)(2,1)S(1)} %bitcast.109), channel_id=1, source_target_pairs={{0,1},{1,0},{2,3},{3,2},{4,5},{5,4},{6,7},{7,6},{8,9},{9,8},{10,11... | collective-permute-start | bytes 786440 | tf_op jit(solution)/shard_map/ppermute | solution.py:102
  159.0 5.0 %collective-permute-start.10 = (bf16[256,1024]{1,0:T(8,128)(2,1)S(1)}, bf16[256,1024]{1,0:T(8,128)(2,1)S(1)}, u32[]{:S(2)}, u32[]{:S(2)}) collective-permute-start(bf16[256,1024]{1,0:T(8,128)(2,1)S(1)} %get-tuple-element.8), channel_id=1, source_target_pairs={{0,1},{1,0},{2,3},{3,2},{4,5},{5,4},{6,7},{7,6},{8,9},{9,8},{10,11... | collective-permute-start | bytes 1572872 | tf_op jit(solution)/shard_map/ppermute | solution.py:102
  161.5 11.9 %collective-permute-start.16 = (bf16[2,2,64,1024]{3,2,1,0:T(8,128)(2,1)S(1)}, bf16[2,2,64,1024]{3,2,1,0:T(8,128)(2,1)S(1)}, u32[]{:S(2)}, u32[]{:S(2)}) collective-permute-start(bf16[2,2,64,1024]{3,2,1,0:T(8,128)(2,1)S(1)} %constant_dynamic-slice_fusion), channel_id=1, source_target_pairs={{32,0},{64,32},{96,64},{128,96},{160,128},{192,160},{224,192},{256... | collective-permute-start | bytes 1572872 | tf_op jit(solution)/shard_map/ppermute | solution.py:42
  164.2 9.2 %collective-permute-start.11 = (bf16[256,1024]{1,0:T(8,128)(2,1)S(1)}, bf16[256,1024]{1,0:T(8,128)(2,1)S(1)}, u32[]{:S(2)}, u32[]{:S(2)}) collective-permute-start(bf16[256,1024]{1,0:T(8,128)(2,1)S(1)} %multiply_convert_fusion.hidden), channel_id=1, source_target_pairs={{0,1},{1,0},{2,3},{3,2},{4,5},{5,4},{6,7},{7,6},{8,9},{9,8},{10,11... | collective-permute-start | bytes 1572872 | tf_op jit(solution)/shard_map/ppermute | solution.py:102
  190.8 4.6 %collective-permute-start.17 = (bf16[32,1024]{1,0:T(8,128)(2,1)S(1)}, bf16[32,1024]{1,0:T(8,128)(2,1)S(1)}, u32[]{:S(2)}, u32[]{:S(2)}) collective-permute-start(bf16[32,1024]{1,0:T(8,128)(2,1)S(1)} %fusion.30), channel_id=1, source_target_pairs={{0,1},{1,0},{2,3},{3,2},{4,5},{5,4},{6,7},{7,6},{8,9},{9,8},{10,11... | collective-permute-start | bytes 196616 | tf_op jit(solution)/shard_map/ppermute | solution.py:102
  207.7 4.6 %collective-permute-start.18 = (bf16[128,2048]{1,0:T(8,128)(2,1)S(1)}, bf16[128,2048]{1,0:T(8,128)(2,1)S(1)}, u32[]{:S(2)}, u32[]{:S(2)}) collective-permute-start(bf16[128,2048]{1,0:T(8,128)(2,1)S(1)} %bitcast.92), channel_id=1, source_target_pairs={{0,1},{1,0},{2,3},{3,2},{4,5},{5,4},{6,7},{7,6},{8,9},{9,8},{10,11... | collective-permute-start | bytes 1572872 | tf_op jit(solution)/shard_map/ppermute | solution.py:102
  (25 other events, 273.0 us)
